TPU v7x, 512 devices: a whole 4x4x16 slice. The times are simulated.
512 devices in a mesh: fs: 64 (over z, y), tp: 8 (over x, core).
Axes of the slice: x: 4, y: 4, z: 16, core: 2. Of those that a mesh axis runs over, the one named last changes fastest.
Arguments:
- tokens: bfloat16 [32768, 2048], P('fs', 'tp'), may hold values from -24 to 24
- u_weight: bfloat16 [2048, 1024], P('fs', 'tp'), may hold values from -0.125 to 0.125
- v_weight: bfloat16 [2048, 1024], P('fs', 'tp'), may hold values from -0.125 to 0.125
- sg_gain: float32 [1024], P('tp'), may hold values from 0.1 to 1.9
- spatial_weight: bfloat16 [8, 128, 128], P('tp'), may hold values from -0.5 to 0.5
- spatial_bias: float32 [8, 128], P('tp'), may hold values from 0.1 to 1.9
- out_weight: bfloat16 [1024, 2048], P('tp', 'fs'), may hold values from -0.1875 to 0.1875
- gain_one: float32 [2048], P('tp'), may hold values from 0.1 to 1.9
- gate_weight: bfloat16 [2048, 5632], P('fs', 'tp'), may hold values from -0.125 to 0.125
- up_weight: bfloat16 [2048, 5632], P('fs', 'tp'), may hold values from -0.125 to 0.125
- down_weight: bfloat16 [5632, 2048], P('tp', 'fs'), may hold values from -0.078125 to 0.078125
- gain_two: float32 [2048], P('tp'), may hold values from 0.1 to 1.9
Outputs:
- layer_out: bfloat16 [32768, 2048], P('fs', 'tp')
All inputs are finite; a program needn't handle non-finite values.
Results may differ from a plain program's by a relative error of at most 0.014.
Values may be sent and summed in bfloat16 or wider, within the bound.
No kernel may reach another device: no remote copies, remote signals or barrier semaphores. Data moves between devices by JAX's collectives and lax.ppermute only.
A program may use at most 64 MiB of HBM per device.

v0:
```python
import jax
import jax.numpy as jnp
from jax import lax
from jax.sharding import Mesh
from jax.sharding import PartitionSpec as P

FS = ("fs_0", "fs_1")


EPS = 1e-05
ALPHA = 2.0**0.25


def sent_to_all(value, axis):
    copies = jnp.broadcast_to(value, (lax.axis_size(axis), *value.shape))
    return lax.all_to_all(copies, axis, split_axis=0, concat_axis=0, tiled=True)


def in_order(pieces, dim):
    pieces = jnp.moveaxis(pieces, 0, dim)
    shape = pieces.shape
    return pieces.reshape(*shape[:dim], shape[dim] * shape[dim + 1], *shape[dim + 2 :])


def gathered_copies(value, axis, dim):
    pieces = sent_to_all(value, axis)
    return in_order(pieces, dim)


def in_one_piece(arrays, axis, dim, along):
    widths = [a.shape[along] for a in arrays]
    both = jnp.concatenate(arrays, axis=along)
    out = lax.all_gather(both, axis, axis=dim, tiled=True)
    return tuple(jnp.split(out, [sum(widths[:k]) for k in range(1, len(widths))], axis=along))


def of_everyone(value, axis):
    everything = sent_to_all(value, axis)
    return jnp.sum(everything, axis=0)


def together(arrays, axis):
    ends = [0]
    for a in arrays:
        ends.append(ends[-1] + a.size)
    so_far = of_everyone(jnp.concatenate([a.ravel() for a in arrays]), axis)
    return tuple((so_far[b:e].reshape(a.shape) for a, b, e in zip(arrays, ends, ends[1:])))


def whole_of(value, axes, dim):
    for axis in reversed(axes):
        value = lax.all_gather(value, axis, axis=dim, tiled=True)
    return value


def in_blocks(value, dim, peers):
    before, after = (value.shape[:dim], value.shape[dim + 1 :])
    return jnp.moveaxis(value.reshape(*before, peers, -1, *after), dim, 0)


def sum_at_owner(value, axis, dim):
    peers = lax.axis_size(axis)
    pieces = lax.all_to_all(in_blocks(value, dim, peers), axis, 0, 0, tiled=True)
    return jnp.sum(pieces.astype(jnp.float32), axis=0)


def add_rows(left, piece):
    return jnp.dot(left, piece, preferred_element_type=jnp.float32)


def scaled_rows(vals, sums, gain, count):
    mean = sums[0][:, None] / count
    square = sums[1][:, None] / count
    return (vals - mean) * lax.rsqrt(square - mean * mean + EPS) * gain[None, :]


def on_device(
    tokens,
    u_weight,
    v_weight,
    sg_gain,
    spatial_weight,
    spatial_bias,
    out_weight,
    gain_one,
    gate_weight,
    up_weight,
    down_weight,
    gain_two,
):
    parts = lax.axis_size("tp")
    whole = gathered_copies(tokens, "tp", 1)
    rows = whole.shape[0]
    width_sg = u_weight.shape[1]
    pieces = in_one_piece((u_weight, v_weight), FS, 0, 1)
    pre_u = add_rows(whole, pieces[0])
    pre_v = add_rows(whole, pieces[1])
    gated = jax.nn.gelu(pre_u)
    valued = jax.nn.gelu(pre_v)
    stats = together((jnp.sum(valued, axis=1), jnp.sum(valued * valued, axis=1)), "tp")
    normed = scaled_rows(valued, stats, sg_gain, width_sg * parts).astype(jnp.bfloat16)
    groups_here = spatial_weight.shape[0]
    block = spatial_weight.shape[1]
    group_width = width_sg // groups_here
    shaped = normed.reshape(rows // block, block, groups_here, group_width)
    lower = jnp.tril(jnp.ones((block, block), jnp.bool_))
    masked = jnp.where(lower[None], spatial_weight, jnp.zeros_like(spatial_weight))
    mixed = jnp.einsum("gij,njgd->nigd", masked, shaped, preferred_element_type=jnp.float32)
    mixed = mixed + spatial_bias.T[None, :, :, None]
    gated_out = (gated * mixed.reshape(rows, width_sg)).astype(jnp.bfloat16)
    terms = jnp.dot(gated_out, whole_of(out_weight, FS, 1), preferred_element_type=jnp.float32)
    mix = sum_at_owner(terms.astype(jnp.bfloat16), "tp", 1).astype(jnp.bfloat16)
    resid = ALPHA * tokens.astype(jnp.float32) + mix.astype(jnp.float32)
    first_sums = together((jnp.sum(resid, axis=1), jnp.sum(resid * resid, axis=1)), "tp")
    first = scaled_rows(resid, first_sums, gain_one, resid.shape[1] * parts).astype(jnp.bfloat16)
    collected = whole_of(down_weight, FS, 1)
    whole_first = gathered_copies(first, "tp", 1)
    pieces = in_one_piece((gate_weight, up_weight), FS, 0, 1)
    gate = add_rows(whole_first, pieces[0])
    upper = add_rows(whole_first, pieces[1])
    hidden = (jax.nn.silu(gate) * upper).astype(jnp.bfloat16)
    ffn_terms = jnp.dot(hidden, collected, preferred_element_type=jnp.float32)
    ffn = sum_at_owner(ffn_terms.astype(jnp.bfloat16), "tp", 1).astype(jnp.bfloat16)
    second = ALPHA * first.astype(jnp.float32) + ffn.astype(jnp.float32)
    last_sums = together((jnp.sum(second, axis=1), jnp.sum(second * second, axis=1)), "tp")
    return scaled_rows(second, last_sums, gain_two, second.shape[1] * parts).astype(jnp.bfloat16)


def solution(mesh):
    finer = Mesh(mesh.devices.reshape(16, 4, mesh.shape["tp"]), ("fs_0", "fs_1", "tp"))
    return jax.shard_map(
        on_device,
        mesh=finer,
        in_specs=(
            P(FS, "tp"),
            P(FS, "tp"),
            P(FS, "tp"),
            P("tp"),
            P("tp", None, None),
            P("tp", None),
            P("tp", FS),
            P("tp"),
            P(FS, "tp"),
            P(FS, "tp"),
            P("tp", FS),
            P("tp"),
        ),
        out_specs=P(FS, "tp"),
        check_vma=False,
    )
```

profile of v0, /device:TPU:1, one launch (start us, length us, event | category | flops | bytes accessed | tf_op | source)
XLA Modules:
  0.0 435.0 jit_solution(3928190341259931945)
XLA Ops:
  6.5 1.3 pad_maximum_fusion.1
  7.9 1.5 pad_maximum_fusion
  9.5 1.1 copy.31
  10.6 1.6 broadcast_in_dim.14
  12.2 10.5 %all-to-all-start = ((bf16[8,512,256]{1,2,0:T(8,128)(2,1)}), bf16[8,512,256]{1,2,0:T(8,128)(2,1)S(1)}, u32[]{:S(2)}, u32[]{:S(2)}) async-start(bf16[8,512,256]{1,2,0:T(8,128)(2,1)} %broadcast_in_dim.14), calls=%async_computation | async-start | bytes 4194304 | tf_op jit(solution)/shard_map/all_to_all | solution.py:16
  22.6 10.2 %all_gather.22 = bf16[704,128]{0,1:T(8,128)(2,1)} all-gather(bf16[704,32]{0,1:T(8,128)(2,1)S(1)} %copy-done.1), channel_id=1, replica_groups=mesh['fs_0'=16,'fs_1'=4,'tp'=8] {'fs_1'}, dimensions={1}, use_global_device_ids=true | all-gather | bytes 225280 | tf_op jit(solution)/shard_map/all_gather | solution.py:52
  32.8 9.9 %all_gather.19 = bf16[128,128]{0,1:T(8,128)(2,1)S(1)} all-gather(bf16[128,32]{0,1:T(8,128)(2,1)S(1)} %copy-done.3), channel_id=1, replica_groups=mesh['fs_0'=16,'fs_1'=4,'tp'=8] {'fs_1'}, dimensions={1}, use_global_device_ids=true | all-gather | bytes 40960 | tf_op jit(solution)/shard_map/all_gather | solution.py:52
  42.8 6.1 %all-to-all-done = bf16[8,512,256]{1,2,0:T(8,128)(2,1)S(1)} async-done(((bf16[8,512,256]{1,2,0:T(8,128)(2,1)}), bf16[8,512,256]{1,2,0:T(8,128)(2,1)S(1)}, u32[]{:S(2)}, u32[]{:S(2)}) %all-to-all-start) | async-done | bytes 2097184 | tf_op jit(solution)/shard_map/all_to_all | solution.py:16
  48.9 96.5 %all-gather.4.cloned.1.call-done = bf16[2048,256]{1,0:T(8,128)(2,1)} async-done(((bf16[32,256]{1,0:T(8,128)(2,1)}), bf16[2048,256]{1,0:T(8,128)(2,1)}) %all-gather.4.cloned.1.call-update) | async-done | bytes 1048592 | tf_op jit(solution)/shard_map/all_gather | solution.py:33
  145.4 1.6 fusion.58
  147.6 15.0 %all-to-all-start.1 = ((f32[8,1,1024]{2,1,0:T(1,128)}), f32[8,1,1024]{2,1,0:T(1,128)S(1)}, u32[]{:S(2)}, u32[]{:S(2)}) async-start(f32[8,1,1024]{2,1,0:T(1,128)} %broadcast_in_dim.15), calls=%async_computation.1 | async-start | bytes 65536 | tf_op jit(solution)/shard_map/all_to_all | solution.py:16
  162.6 24.6 %all_gather.20 = bf16[128,2048]{0,1:T(8,128)(2,1)S(1)} all-gather(bf16[128,128]{0,1:T(8,128)(2,1)S(1)} %all_gather.19), channel_id=1, replica_groups=mesh['fs_0'=16,'fs_1'=4,'tp'=8] {'fs_0'}, dimensions={1}, use_global_device_ids=true | all-gather | bytes 557056 | tf_op jit(solution)/shard_map/all_gather | solution.py:52
  187.8 3.7 convolution_convert_fusion
  191.5 1.7 copy.56
  193.2 37.2 %all_to_all.38 = bf16[8,512,256]{2,1,0:T(8,128)(2,1)S(1)} all-to-all(bf16[8,512,256]{2,1,0:T(8,128)(2,1)S(1)} %bitcast.57), channel_id=1, replica_groups=mesh['fs_0'=16,'fs_1'=4,'tp'=8] {'tp'}, dimensions={0} | all-to-all | bytes 4194304 | tf_op jit(solution)/shard_map/all_to_all | solution.py:63
  231.7 8.1 %all_to_all.39 = f32[8,1,1024]{2,1,0:T(1,128)S(1)} all-to-all(f32[8,1,1024]{2,1,0:T(1,128)S(1)} %broadcast_in_dim.17), channel_id=1, replica_groups=mesh['fs_0'=16,'fs_1'=4,'tp'=8] {'tp'}, dimensions={0} | all-to-all | bytes 65536 | tf_op jit(solution)/shard_map/all_to_all | solution.py:16
  240.4 29.4 %all_to_all.40 = bf16[8,512,256]{1,2,0:T(8,128)(2,1)S(1)} all-to-all(bf16[8,512,256]{1,2,0:T(8,128)(2,1)S(1)} %broadcast_in_dim.18), channel_id=1, replica_groups=mesh['fs_0'=16,'fs_1'=4,'tp'=8] {'tp'}, dimensions={0} | all-to-all | bytes 4194304 | tf_op jit(solution)/shard_map/all_to_all | solution.py:16
  269.8 26.1 %all-gather.6.cloned.1.call-done = bf16[2048,1408]{1,0:T(8,128)(2,1)} async-done(((bf16[32,1408]{1,0:T(8,128)(2,1)}), bf16[2048,1408]{1,0:T(8,128)(2,1)}) %all-gather.6.cloned.1.call-update) | async-done | bytes 5767184 | tf_op jit(solution)/shard_map/all_gather | solution.py:33
  295.9 4.7 %fusion.2 = f32[512,704]{0,1:T(8,128)} fusion(bf16[512,2048]{0,1:T(8,128)(2,1)S(1)} %bitcast.59, bf16[2048,1408]{1,0:T(8,128)(2,1)} %all-gather.6.cloned.1.call-done), kind=kOutput, calls=%fused_computation.2 | convolution fusion | flops 1476395008 | bytes 6684672 | tf_op jit(solution)/shard_map/dot_general | solution.py:68
  300.6 67.2 %all-gather.8.cloned.1.call-done = bf16[704,2048]{0,1:T(8,128)(2,1)} async-done(((bf16[704,128]{0,1:T(8,128)(2,1)}), bf16[704,2048]{0,1:T(8,128)(2,1)}) %all-gather.8.cloned.1.call-update) | async-done | bytes 2883600 | tf_op jit(solution)/shard_map/all_gather | solution.py:52
  367.8 9.3 %convolution_convert_fusion.1 = bf16[512,2048]{1,0:T(8,128)(2,1)} fusion(bf16[704,2048]{0,1:T(8,128)(2,1)} %all-gather.8.cloned.1.call-done, bf16[512,2048]{0,1:T(8,128)(2,1)S(1)} %bitcast.60, bf16[2048,1408]{1,0:T(8,128)(2,1)} %all-gather.6.cloned.1.call-done, f32[512,704]{0,1:T(8,128)} %fusion.2), kind=kOutput, calls=%fused_computation.5 | convolution fusion | flops 2956001280 | bytes 11927552 | tf_op jit(solution)/shard_map/dot_general | solution.py:122
  377.1 1.7 copy.55
  378.9 39.8 %all_to_all.41 = bf16[8,512,256]{2,1,0:T(8,128)(2,1)S(1)} all-to-all(bf16[8,512,256]{2,1,0:T(8,128)(2,1)S(1)} %bitcast.58), channel_id=1, replica_groups=mesh['fs_0'=16,'fs_1'=4,'tp'=8] {'tp'}, dimensions={0} | all-to-all | bytes 4194304 | tf_op jit(solution)/shard_map/all_to_all | solution.py:63
  419.3 8.1 %all_to_all.42 = f32[8,1,1024]{2,1,0:T(1,128)S(1)} all-to-all(f32[8,1,1024]{2,1,0:T(1,128)S(1)} %broadcast_in_dim.36), channel_id=1, replica_groups=mesh['fs_0'=16,'fs_1'=4,'tp'=8] {'tp'}, dimensions={0} | all-to-all | bytes 65536 | tf_op jit(solution)/shard_map/all_to_all | solution.py:16
  (47 shorter events, 4.7 us)
Async XLA Ops:
  6.5 138.8 %all-gather.4.cloned.1.call-start = ((), (), s32[]{:S(2)}) async-start(), calls=%async_computation.7 | async-start | bytes 1064960 | tf_op jit(solution)/shard_map/all_gather | solution.py:33
  7.9 288.0 %all-gather.6.cloned.1.call-start = ((), (), s32[]{:S(2)}) async-start(), calls=%async_computation.8 | async-start | bytes 5857280 | tf_op jit(solution)/shard_map/all_gather | solution.py:33
  12.2 10.5 %copy-start.1 = (bf16[704,32]{0,1:T(8,128)(2,1)S(1)}, bf16[704,32]{0,1:T(8,128)(2,1)}, u32[]{:S(2)}) copy-start(bf16[704,32]{0,1:T(8,128)(2,1)} %param.22) | copy-start | bytes 135172
  12.2 20.7 %copy-start.3 = (bf16[128,32]{0,1:T(8,128)(2,1)S(1)}, bf16[128,32]{0,1:T(8,128)(2,1)}, u32[]{:S(2)}) copy-start(bf16[128,32]{0,1:T(8,128)(2,1)} %param.18) | copy-start | bytes 24580
  12.2 36.7 %all-to-all-start = ((bf16[8,512,256]{1,2,0:T(8,128)(2,1)}), bf16[8,512,256]{1,2,0:T(8,128)(2,1)S(1)}, u32[]{:S(2)}, u32[]{:S(2)}) async-start(bf16[8,512,256]{1,2,0:T(8,128)(2,1)} %broadcast_in_dim.14), calls=%async_computation | async-start | bytes 4194304 | tf_op jit(solution)/shard_map/all_to_all | solution.py:16
  22.6 164.6 %copy-start.6 = (f32[128]{0:T(128)S(1)}, f32[128]{0:T(128)}, u32[]{:S(2)}) copy-start(f32[128]{0:T(128)} %param.15) | copy-start | bytes 1540
  22.6 345.2 %all-gather.8.cloned.1.call-start = ((), (), s32[]{:S(2)}) async-start(), calls=%async_computation.9 | async-start | bytes 3342336 | tf_op jit(solution)/shard_map/all_gather | solution.py:52
  145.4 42.1 %copy-start.2 = (bf16[1,128,128]{2,1,0:T(8,128)(2,1)S(1)}, bf16[1,128,128]{2,1,0:T(8,128)(2,1)}, u32[]{:S(2)}) copy-start(bf16[1,128,128]{2,1,0:T(8,128)(2,1)} %param.16) | copy-start | bytes 98308
  145.4 42.1 %copy-start.7 = (f32[1,128]{1,0:T(1,128)S(1)}, f32[1,128]{1,0:T(1,128)}, u32[]{:S(2)}) copy-start(f32[1,128]{1,0:T(1,128)} %param.17) | copy-start | bytes 1540
  147.6 39.6 %all-to-all-start.1 = ((f32[8,1,1024]{2,1,0:T(1,128)}), f32[8,1,1024]{2,1,0:T(1,128)S(1)}, u32[]{:S(2)}, u32[]{:S(2)}) async-start(f32[8,1,1024]{2,1,0:T(1,128)} %broadcast_in_dim.15), calls=%async_computation.1 | async-start | bytes 65536 | tf_op jit(solution)/shard_map/all_to_all | solution.py:16
  230.5 1.0 copy-start
  230.5 9.4 %copy-start.4 = (f32[256]{0:T(256)S(1)}, f32[256]{0:T(256)}, u32[]{:S(2)}) copy-start(f32[256]{0:T(256)} %param.19) | copy-start | bytes 3076
  418.7 8.8 %copy-start.5 = (f32[256]{0:T(256)S(1)}, f32[256]{0:T(256)}, u32[]{:S(2)}) copy-start(f32[256]{0:T(256)} %param.23) | copy-start | bytes 3076
Sparse Core Ops, SparseCore 0:
  10.3 135.0 all-gather.3
  148.3 147.5 all-gather.5
  298.0 69.7 all-gather.7
where the time goes:
time: 436 us; the launch traced here: 435 us
  waiting for transfers between devices  196 us (45%)
  blocking collectives  167 us (38%)
  starting transfers between devices  25.5 us (6%)
  matrix products  19.5 us (4%)
  between operations  13.3 us (3%)
  local copies, waits for them, and re-layouts  7.9 us (2%)
  other arithmetic  5.49 us (1%)
    all_gather x2, waiting for transfers between devices, in_one_piece(): out = lax.all_gather(both, axis, axis=dim, tiled=True)  123 us
    all_to_all x2, blocking collectives, sum_at_owner(): lax.all_to_all(in_blocks(value, dim, peers), axis, 0, 0, tiled=True)  77 us
    all_gather x1, waiting for transfers between devices, whole_of(): value = lax.all_gather(value, axis, axis=dim, tiled=True)  67.2 us
    all_to_all x3, blocking collectives, sent_to_all(): return lax.all_to_all(copies, axis, split_axis=0, concat_axis=0, tiled=True)  45.6 us
    all_gather x3, blocking collectives, whole_of(): value = lax.all_gather(value, axis, axis=dim, tiled=True)  44.7 us
    all_to_all x2, starting transfers between devices, sent_to_all(): return lax.all_to_all(copies, axis, split_axis=0, concat_axis=0, tiled=True)  25.5 us
    dot_general x1, matrix products, on_device(): ffn_terms = jnp.dot(hidden, collected, preferred_element_type=jnp.float32)  9.33 us
  transfers between devices with their start and end apart: 5, of which 4 were waited for; matrix products, arithmetic and copies ran while one was open for 4% of the time, Pallas kernels for 0%

commit v1 on v0

v1 whole, which is shorter than its diff:
```python
import jax
import jax.numpy as jnp
from jax import lax
from jax.sharding import Mesh
from jax.sharding import PartitionSpec as P

FS = ("z", "y")
TP = ("x", "c")

EPS = 1e-05
ALPHA = 2.0**0.25
BF16 = jnp.bfloat16
F32 = jnp.float32


def sent_to_all(value, axis):
    copies = jnp.broadcast_to(value, (lax.axis_size(axis), *value.shape))
    return lax.all_to_all(copies, axis, split_axis=0, concat_axis=0, tiled=True)


def to_partner(value):
    return lax.ppermute(value, "c", [(0, 1), (1, 0)])


def row_norm(vals, gain):
    count = vals.shape[1]
    mean = jnp.sum(vals, axis=1, keepdims=True) / count
    square = jnp.sum(vals * vals, axis=1, keepdims=True) / count
    return (vals - mean) * lax.rsqrt(square - mean * mean + EPS) * gain[None, :]


def summed_rows(own, other, peers):
    pair = own + to_partner(other.astype(BF16)).astype(F32)
    pieces = pair.astype(BF16).reshape(peers, own.shape[0] // peers, own.shape[1])
    pieces = lax.all_to_all(pieces, "x", 0, 0, tiled=True)
    return jnp.sum(pieces.astype(F32), axis=0)


def on_device(
    tokens,
    u_weight,
    v_weight,
    sg_gain,
    spatial_weight,
    spatial_bias,
    out_weight,
    gain_one,
    gate_weight,
    up_weight,
    down_weight,
    gain_two,
):
    core = lax.axis_index("c")
    chips = lax.axis_size("x")
    cores = lax.axis_size("c")
    parts = chips * cores
    rows, feats = tokens.shape
    width = feats * parts
    sg = u_weight.shape[1]
    ff = gate_weight.shape[1]
    own_rows = rows // parts

    packed = jnp.concatenate([gate_weight, up_weight, down_weight.T], axis=1)
    packed = lax.all_gather(packed, "y", axis=0, tiled=True)
    ffw = lax.all_gather(packed, "z", axis=0, tiled=True)

    small = jnp.concatenate([u_weight, v_weight, out_weight.T], axis=1)
    depth = small.shape[0]
    small = lax.all_gather(small, "z", axis=0, tiled=True)
    small = sent_to_all(small, "y")
    small = small.reshape(small.shape[0], -1, depth, small.shape[2])
    small = jnp.swapaxes(small, 0, 1).reshape(width, small.shape[3])

    gains = sent_to_all(jnp.stack([gain_one, gain_two]), TP)
    gain_1 = gains[:, 0].reshape(width)
    gain_2 = gains[:, 1].reshape(width)

    blocks = sent_to_all(tokens, TP)
    whole = jnp.moveaxis(blocks, 0, 1).reshape(rows, width)
    me = lax.axis_index(TP)
    mine = lax.dynamic_slice_in_dim(blocks, me * own_rows, own_rows, 1)
    mine = jnp.moveaxis(mine, 0, 1).reshape(own_rows, width)

    pre_u = jnp.dot(whole, small[:, :sg], preferred_element_type=F32)
    pre_v = jnp.dot(whole, small[:, sg : 2 * sg], preferred_element_type=F32)
    gated = jax.nn.gelu(pre_u)
    valued = jax.nn.gelu(pre_v)
    sums = jnp.stack([jnp.sum(valued, axis=1), jnp.sum(valued * valued, axis=1)])
    sums = jnp.sum(sent_to_all(sums, TP), axis=0)
    count = sg * parts
    mean = sums[0][:, None] / count
    square = sums[1][:, None] / count
    normed = (valued - mean) * lax.rsqrt(square - mean * mean + EPS) * sg_gain[None, :]
    normed = normed.astype(BF16)

    groups = spatial_weight.shape[0]
    block = spatial_weight.shape[1]
    shaped = normed.reshape(rows // block, block, groups, sg // groups)
    lower = jnp.tril(jnp.ones((block, block), jnp.bool_))
    masked = jnp.where(lower[None], spatial_weight, jnp.zeros_like(spatial_weight))
    mixed = jnp.einsum("gij,njgd->nigd", masked, shaped, preferred_element_type=F32)
    mixed = mixed + spatial_bias.T[None, :, :, None]
    gated_out = (gated * mixed.reshape(rows, sg)).astype(BF16)

    split = gated_out.reshape(chips, cores, own_rows, sg)
    keep = lax.dynamic_index_in_dim(split, core, 1, keepdims=False).reshape(-1, sg)
    give = lax.dynamic_index_in_dim(split, 1 - core, 1, keepdims=False).reshape(-1, sg)
    out_t = small[:, 2 * sg :]
    across = (((1,), (1,)), ((), ()))
    give = lax.dot_general(give, out_t, across, preferred_element_type=F32)
    keep = lax.dot_general(keep, out_t, across, preferred_element_type=F32)
    mix = summed_rows(keep, give, chips).astype(BF16)
    first = row_norm(ALPHA * mine.astype(F32) + mix.astype(F32), gain_1).astype(BF16)

    near = sent_to_all(first, "x").reshape(-1, width)
    far = to_partner(near)
    gate_w, up_w, down_t = ffw[:, :ff], ffw[:, ff : 2 * ff], ffw[:, 2 * ff :]

    def mixer(left):
        gate = jnp.dot(left, gate_w, preferred_element_type=F32)
        upper = jnp.dot(left, up_w, preferred_element_type=F32)
        hidden = (jax.nn.silu(gate) * upper).astype(BF16)
        return lax.dot_general(hidden, down_t, across, preferred_element_type=F32)

    both = mixer(jnp.concatenate([near, far], axis=0))
    half = near.shape[0]
    ffn = summed_rows(both[:half], both[half:], chips).astype(BF16)
    last = row_norm(ALPHA * first.astype(F32) + ffn.astype(F32), gain_2).astype(BF16)
    last = jnp.moveaxis(last.reshape(own_rows, parts, feats), 1, 0)
    return lax.all_to_all(last, TP, 0, 0, tiled=True).reshape(rows, feats)


def solution(mesh):
    tp = mesh.shape["tp"]
    finer = Mesh(mesh.devices.reshape(16, 4, tp // 2, 2), ("z", "y", "x", "c"))
    return jax.shard_map(
        on_device,
        mesh=finer,
        in_specs=(
            P(FS, TP),
            P(FS, TP),
            P(FS, TP),
            P(TP),
            P(TP, None, None),
            P(TP, None),
            P(TP, FS),
            P(TP),
            P(FS, TP),
            P(FS, TP),
            P(TP, FS),
            P(TP),
        ),
        out_specs=P(FS, TP),
        check_vma=False,
    )
```

time: 436 us -> 254 us (0.58)
  waiting for transfers between devices: 196 us -> 72.8 us
  blocking collectives: 167 us -> 71.5 us
  starting transfers between devices: 25.5 us -> 44.2 us
  local copies, waits for them, and re-layouts: 7.9 us -> 16.2 us
  other arithmetic: 5.49 us -> 10.3 us
    all_gather x3 -> x1, waiting for transfers between devices: 190 us -> 0.01 us  [on_device(): ffw = lax.all_gather(packed, 'z', axis=0, tiled=True)]
    all_to_all x2 -> x1, blocking collectives: 77 us -> 10.1 us  [on_device(): return lax.all_to_all(last, TP, 0, 0, tiled=True).reshape(rows, feats)]
    all_to_all x2 -> x4, waiting for transfers between devices: 6.09 us -> 42.4 us  [sent_to_all(): return lax.all_to_all(copies, axis, split_axis=0, concat_axis=0, tiled=True)]
    all_to_all x3 -> x1, blocking collectives: 45.6 us -> 15.9 us  [sent_to_all(): return lax.all_to_all(copies, axis, split_axis=0, concat_axis=0, tiled=True)]
    all_to_all x0 -> x2, waiting for transfers between devices: none -> 25.7 us  [summed_rows(): pieces = lax.all_to_all(pieces, 'x', 0, 0, tiled=True)]
    ppermute x0 -> x3, starting transfers between devices: none -> 9.33 us  [to_partner(): return lax.ppermute(value, 'c', [(0, 1), (1, 0)])]
    all_to_all x0 -> x2, starting transfers between devices: none -> 7.76 us  [summed_rows(): pieces = lax.all_to_all(pieces, 'x', 0, 0, tiled=True)]
    ppermute x0 -> x3, waiting for transfers between devices: none -> 4.66 us  [to_partner(): return lax.ppermute(value, 'c', [(0, 1), (1, 0)])]
  transfers between devices with their start and end apart: 5 -> 10, of which waited for: 4 -> 8; matrix products, arithmetic and copies ran while one was open for 4% -> 9% of each run, Pallas kernels for 0% -> 0%
where the time goes in v1:
time: 254 us; the launch traced here: 253 us
  waiting for transfers between devices  72.8 us (29%)
  blocking collectives  71.5 us (28%)
  starting transfers between devices  44.2 us (17%)
  matrix products  23.7 us (9%)
  local copies, waits for them, and re-layouts  16.2 us (6%)
  between operations  13.7 us (5%)
  other arithmetic  10.3 us (4%)
    all_to_all x4, waiting for transfers between devices, sent_to_all(): return lax.all_to_all(copies, axis, split_axis=0, concat_axis=0, tiled=True)  42.4 us
    all_gather x1, blocking collectives, on_device(): small = lax.all_gather(small, 'z', axis=0, tiled=True)  32.9 us
    all_to_all x4, starting transfers between devices, sent_to_all(): return lax.all_to_all(copies, axis, split_axis=0, concat_axis=0, tiled=True)  27.2 us
    all_to_all x2, waiting for transfers between devices, summed_rows(): pieces = lax.all_to_all(pieces, 'x', 0, 0, tiled=True)  25.7 us
    all_to_all x1, blocking collectives, sent_to_all(): return lax.all_to_all(copies, axis, split_axis=0, concat_axis=0, tiled=True)  15.9 us
    all_gather x1, blocking collectives, on_device(): packed = lax.all_gather(packed, 'y', axis=0, tiled=True)  12.7 us
    dot_general x1, matrix products, mixer(): return lax.dot_general(hidden, down_t, across, preferred_element_type=F32)  10.7 us
    all_to_all x1, blocking collectives, on_device(): return lax.all_to_all(last, TP, 0, 0, tiled=True).reshape(rows, feats)  10.1 us
  transfers between devices with their start and end apart: 10, of which 8 were waited for; matrix products, arithmetic and copies ran while one was open for 9% of the time, Pallas kernels for 0%

profile of v1, /device:TPU:1, one launch (start us, length us, event | category | flops | bytes accessed | tf_op | source)
XLA Modules:
  0.0 252.5 jit_solution(10627825997509619518)
XLA Ops:
  7.5 12.7 %all_gather.10 = bf16[128,2112]{1,0:T(8,128)(2,1)} all-gather(bf16[32,2112]{1,0:T(8,128)(2,1)S(1)} %concatenate.11), channel_id=1, replica_groups=mesh['z'=16,'y'=4,'x'=4,'c'=2] {'y'}, dimensions={0}, use_global_device_ids=true | all-gather | bytes 675840 | tf_op jit(solution)/shard_map/all_gather | solution.py:64
  20.9 32.9 %all_gather.9 = bf16[512,384]{1,0:T(8,128)(2,1)S(1)} all-gather(bf16[32,384]{1,0:T(8,128)(2,1)S(1)} %pad_maximum_fusion.7), channel_id=1, replica_groups=mesh['z'=16,'y'=4,'x'=4,'c'=2] {'z'}, dimensions={0}, use_global_device_ids=true | all-gather | bytes 417792 | tf_op jit(solution)/shard_map/all_gather | solution.py:69
  55.1 3.6 %all-to-all-start.1 = ((bf16[4,512,384]{2,1,0:T(8,128)(2,1)}), bf16[4,512,384]{2,1,0:T(8,128)(2,1)S(1)}, u32[]{:S(2)}, u32[]{:S(2)}) async-start(bf16[4,512,384]{2,1,0:T(8,128)(2,1)} %broadcast_in_dim.28), calls=%async_computation.1 | async-start | bytes 3145728 | tf_op jit(solution)/shard_map/all_to_all | solution.py:18
  58.8 12.4 %all-to-all-done.1 = bf16[4,512,384]{2,1,0:T(8,128)(2,1)S(1)} async-done(((bf16[4,512,384]{2,1,0:T(8,128)(2,1)}), bf16[4,512,384]{2,1,0:T(8,128)(2,1)S(1)}, u32[]{:S(2)}, u32[]{:S(2)}) %all-to-all-start.1) | async-done | bytes 1572896 | tf_op jit(solution)/shard_map/all_to_all | solution.py:18
  73.1 16.1 %all-to-all-start = ((bf16[8,512,256]{1,2,0:T(8,128)(2,1)}), bf16[8,512,256]{1,2,0:T(8,128)(2,1)S(1)}, u32[]{:S(2)}, u32[]{:S(2)}) async-start(bf16[8,512,256]{1,2,0:T(8,128)(2,1)} %broadcast_in_dim.14), calls=%async_computation | async-start | bytes 4194304 | tf_op jit(solution)/shard_map/all_to_all | solution.py:18
  89.2 2.8 %copy.50 = bf16[16,4,32,384]{3,2,1,0:T(8,128)(2,1)} copy(bf16[16,4,32,384]{3,2,0,1:T(8,128)(2,1)} %bitcast.85) | data formatting | bytes 3145728 | tf_op jit(solution)/shard_map/transpose | solution.py:72
  92.0 23.4 %all-to-all-done = bf16[8,512,256]{1,2,0:T(8,128)(2,1)S(1)} async-done(((bf16[8,512,256]{1,2,0:T(8,128)(2,1)}), bf16[8,512,256]{1,2,0:T(8,128)(2,1)S(1)}, u32[]{:S(2)}, u32[]{:S(2)}) %all-to-all-start) | async-done | bytes 2097184 | tf_op jit(solution)/shard_map/all_to_all | solution.py:18
  117.6 4.2 %all-to-all-start.2 = ((f32[8,2,512]{2,1,0:T(2,128)}), f32[8,2,512]{2,1,0:T(2,128)S(1)}, u32[]{:S(2)}, u32[]{:S(2)}) async-start(f32[8,2,512]{2,1,0:T(2,128)} %broadcast_in_dim.29), calls=%async_computation.2 | async-start | bytes 65536 | tf_op jit(solution)/shard_map/all_to_all | solution.py:18
  121.8 4.8 %all-to-all-done.2 = f32[8,2,512]{2,1,0:T(2,128)S(1)} async-done(((f32[8,2,512]{2,1,0:T(2,128)}), f32[8,2,512]{2,1,0:T(2,128)S(1)}, u32[]{:S(2)}, u32[]{:S(2)}) %all-to-all-start.2) | async-done | bytes 32800 | tf_op jit(solution)/shard_map/all_to_all | solution.py:18
  130.5 2.6 %collective-permute-start = (bf16[256,2048]{1,0:T(8,128)(2,1)S(1)}, bf16[256,2048]{1,0:T(8,128)(2,1)}, u32[]{:S(2)}, u32[]{:S(2)}) collective-permute-start(bf16[256,2048]{1,0:T(8,128)(2,1)S(1)} %convolution_convert_fusion), channel_id=1, source_target_pairs={{0,1},{1,0},{2,3},{3,2},{4,5},{5,4},{6,7},{7,6},{8,9},{9,8},{10,11... | collective-permute-start | bytes 3145736 | tf_op jit(solution)/shard_map/ppermute | solution.py:22
  133.7 3.3 %all-to-all-start.4 = ((f32[8,2,256]{2,1,0:T(2,128)}), f32[8,2,256]{2,1,0:T(2,128)S(1)}, u32[]{:S(2)}, u32[]{:S(2)}) async-start(f32[8,2,256]{2,1,0:T(2,128)} %broadcast_in_dim.31), calls=%async_computation.4 | async-start | bytes 32768 | tf_op jit(solution)/shard_map/all_to_all | solution.py:18
  137.1 2.8 %add_convert_fusion = bf16[256,2048]{1,0:T(8,128)(2,1)} fusion(bf16[256,2048]{1,0:T(8,128)(2,1)} %collective-permute-done, bf16[256,128]{1,0:T(8,128)(2,1)S(1)} %bitcast.97, bf16[2048,384]{1,0:T(8,128)(2,1)} %bitcast.84), kind=kOutput, calls=%fused_computation.11 | convolution fusion | flops 135790592 | bytes 2686976 | tf_op jit(solution)/shard_map/dot_general | solution.py:111
  141.7 3.5 %all-to-all-start.3 = ((bf16[4,64,2048]{2,1,0:T(8,128)(2,1)}), bf16[4,64,2048]{2,1,0:T(8,128)(2,1)S(1)}, u32[]{:S(2)}, u32[]{:S(2)}) async-start(bf16[4,64,2048]{2,1,0:T(8,128)(2,1)} %bitcast.87), calls=%async_computation.3 | async-start | bytes 2097152 | tf_op jit(solution)/shard_map/all_to_all | solution.py:35
  146.4 2.4 copy.62
  148.8 10.9 %all-to-all-done.3 = bf16[4,64,2048]{2,1,0:T(8,128)(2,1)S(1)} async-done(((bf16[4,64,2048]{2,1,0:T(8,128)(2,1)}), bf16[4,64,2048]{2,1,0:T(8,128)(2,1)S(1)}, u32[]{:S(2)}, u32[]{:S(2)}) %all-to-all-start.3) | async-done | bytes 1048608 | tf_op jit(solution)/shard_map/all_to_all | solution.py:35
  161.7 15.9 %all_to_all.40 = bf16[4,64,2048]{2,1,0:T(8,128)(2,1)S(1)} all-to-all(bf16[4,64,2048]{2,1,0:T(8,128)(2,1)S(1)} %broadcast_in_dim.32), channel_id=1, replica_groups=mesh['z'=16,'y'=4,'x'=4,'c'=2] {'x'}, dimensions={0} | all-to-all | bytes 2097152 | tf_op jit(solution)/shard_map/all_to_all | solution.py:18
  178.6 4.5 %collective-permute-start.1 = (bf16[256,2048]{1,0:T(8,128)(2,1)S(1)}, bf16[256,2048]{1,0:T(8,128)(2,1)}, u32[]{:S(2)}, u32[]{:S(2)}) collective-permute-start(bf16[256,2048]{1,0:T(8,128)(2,1)S(1)} %bitcast.89), channel_id=1, source_target_pairs={{0,1},{1,0},{2,3},{3,2},{4,5},{5,4},{6,7},{7,6},{8,9},{9,8},{10,11... | collective-permute-start | bytes 3145736 | tf_op jit(solution)/shard_map/ppermute | solution.py:22
  183.1 2.4 collective-permute-done.1
  185.5 5.4 %fusion.4 = f32[512,704]{0,1:T(8,128)} fusion(bf16[2048,2112]{1,0:T(8,128)(2,1)} %all-gather.2.cloned.1.call-done, bf16[256,2048]{1,0:T(8,128)(2,1)} %collective-permute-done.1, bf16[256,2048]{1,0:T(8,128)(2,1)} %bitcast.90), kind=kOutput, calls=%fused_computation.4 | convolution fusion | flops 1480589312 | bytes 6684672 | tf_op jit(solution)/shard_map/dot_general | solution.py:120
  190.9 10.7 %fusion = f32[512,2048]{1,0:T(8,128)} fusion(bf16[2048,2112]{1,0:T(8,128)(2,1)} %all-gather.2.cloned.1.call-done, f32[512,704]{0,1:T(8,128)} %fusion.4, bf16[256,2048]{1,0:T(8,128)(2,1)} %collective-permute-done.1, bf16[256,2048]{1,0:T(8,128)(2,1)} %bitcast.91), kind=kOutput, calls=%fused_computation | convolution fusion | flops 2959147008 | bytes 14024704 | tf_op jit(solution)/shard_map/dot_general | solution.py:123
  207.9 2.9 %fusion.6 = bf16[256,2048]{1,0:T(8,128)(2,1)} fusion(f32[512,2048]{1,0:T(8,128)} %fusion, bf16[256,2048]{1,0:T(8,128)(2,1)S(1)} %collective-permute-done.2), kind=kLoop, calls=%fused_computation.9 | loop fusion | flops 1572864 | bytes 4194304 | tf_op jit(solution)/shard_map/convert_element_type | solution.py:34
  210.8 4.2 %all-to-all-start.6 = ((bf16[4,64,2048]{2,1,0:T(8,128)(2,1)}), bf16[4,64,2048]{2,1,0:T(8,128)(2,1)}, u32[]{:S(2)}, u32[]{:S(2)}) async-start(bf16[4,64,2048]{2,1,0:T(8,128)(2,1)} %bitcast.88), calls=%async_computation.6 | async-start | bytes 2097152 | tf_op jit(solution)/shard_map/all_to_all | solution.py:35
  215.0 14.9 %all-to-all-done.6 = bf16[4,64,2048]{2,1,0:T(8,128)(2,1)} async-done(((bf16[4,64,2048]{2,1,0:T(8,128)(2,1)}), bf16[4,64,2048]{2,1,0:T(8,128)(2,1)}, u32[]{:S(2)}, u32[]{:S(2)}) %all-to-all-start.6) | async-done | bytes 1048608 | tf_op jit(solution)/shard_map/all_to_all | solution.py:35
  234.9 10.1 %all_to_all.41 = bf16[8,64,256]{2,1,0:T(8,128)(2,1)S(1)} all-to-all(bf16[8,64,256]{2,1,0:T(8,128)(2,1)S(1)} %copy.58), channel_id=1, replica_groups=mesh['z'=16,'y'=4,'x'=4,'c'=2] {'x','c'}, dimensions={0} | all-to-all | bytes 524288 | tf_op jit(solution)/shard_map/all_to_all | solution.py:130
  (62 shorter events, 29.7 us)
Async XLA Ops:
  6.5 179.0 %all-gather.2.cloned.1.call-start = ((), (), s32[]{:S(2)}) async-start(), calls=%async_computation.8 | async-start | bytes 9469952 | tf_op jit(solution)/shard_map/all_gather | solution.py:65
  53.8 4.9 %copy-start.2 = (bf16[512,256]{1,0:T(8,128)(2,1)S(1)}, bf16[512,256]{1,0:T(8,128)(2,1)}, u32[]{:S(2)}) copy-start(bf16[512,256]{1,0:T(8,128)(2,1)} %param.12) | copy-start | bytes 786436
  55.1 16.1 %all-to-all-start.1 = ((bf16[4,512,384]{2,1,0:T(8,128)(2,1)}), bf16[4,512,384]{2,1,0:T(8,128)(2,1)S(1)}, u32[]{:S(2)}, u32[]{:S(2)}) async-start(bf16[4,512,384]{2,1,0:T(8,128)(2,1)} %broadcast_in_dim.28), calls=%async_computation.1 | async-start | bytes 3145728 | tf_op jit(solution)/shard_map/all_to_all | solution.py:18
  71.3 1.8 copy-start
  73.1 42.3 %all-to-all-start = ((bf16[8,512,256]{1,2,0:T(8,128)(2,1)}), bf16[8,512,256]{1,2,0:T(8,128)(2,1)S(1)}, u32[]{:S(2)}, u32[]{:S(2)}) async-start(bf16[8,512,256]{1,2,0:T(8,128)(2,1)} %broadcast_in_dim.14), calls=%async_computation | async-start | bytes 4194304 | tf_op jit(solution)/shard_map/all_to_all | solution.py:18
  92.0 34.7 %copy-start.6 = (f32[128]{0:T(128)S(1)}, f32[128]{0:T(128)}, u32[]{:S(2)}) copy-start(f32[128]{0:T(128)} %param.15) | copy-start | bytes 1540
  92.0 34.9 %copy-start.3 = (bf16[1,128,128]{2,1,0:T(8,128)(2,1)S(1)}, bf16[1,128,128]{2,1,0:T(8,128)(2,1)}, u32[]{:S(2)}) copy-start(bf16[1,128,128]{2,1,0:T(8,128)(2,1)} %param.16) | copy-start | bytes 98308
  92.0 34.9 %copy-start.7 = (f32[1,128]{1,0:T(1,128)S(1)}, f32[1,128]{1,0:T(1,128)}, u32[]{:S(2)}) copy-start(f32[1,128]{1,0:T(1,128)} %param.17) | copy-start | bytes 1540
  117.6 9.0 %all-to-all-start.2 = ((f32[8,2,512]{2,1,0:T(2,128)}), f32[8,2,512]{2,1,0:T(2,128)S(1)}, u32[]{:S(2)}, u32[]{:S(2)}) async-start(f32[8,2,512]{2,1,0:T(2,128)} %broadcast_in_dim.29), calls=%async_computation.2 | async-start | bytes 65536 | tf_op jit(solution)/shard_map/all_to_all | solution.py:18
  127.3 5.8 %copy-start.4 = (f32[256]{0:T(256)S(1)}, f32[256]{0:T(256)}, u32[]{:S(2)}) copy-start(f32[256]{0:T(256)} %param.23) | copy-start | bytes 3076
  127.3 5.8 %copy-start.5 = (f32[256]{0:T(256)S(1)}, f32[256]{0:T(256)}, u32[]{:S(2)}) copy-start(f32[256]{0:T(256)} %param.19) | copy-start | bytes 3076
  130.5 6.5 %collective-permute-start = (bf16[256,2048]{1,0:T(8,128)(2,1)S(1)}, bf16[256,2048]{1,0:T(8,128)(2,1)}, u32[]{:S(2)}, u32[]{:S(2)}) collective-permute-start(bf16[256,2048]{1,0:T(8,128)(2,1)S(1)} %convolution_convert_fusion), channel_id=1, source_target_pairs={{0,1},{1,0},{2,3},{3,2},{4,5},{5,4},{6,7},{7,6},{8,9},{9,8},{10,11... | collective-permute-start | bytes 3145736 | tf_op jit(solution)/shard_map/ppermute | solution.py:22
  133.7 7.9 %all-to-all-start.4 = ((f32[8,2,256]{2,1,0:T(2,128)}), f32[8,2,256]{2,1,0:T(2,128)S(1)}, u32[]{:S(2)}, u32[]{:S(2)}) async-start(f32[8,2,256]{2,1,0:T(2,128)} %broadcast_in_dim.31), calls=%async_computation.4 | async-start | bytes 32768 | tf_op jit(solution)/shard_map/all_to_all | solution.py:18
  141.7 18.0 %all-to-all-start.3 = ((bf16[4,64,2048]{2,1,0:T(8,128)(2,1)}), bf16[4,64,2048]{2,1,0:T(8,128)(2,1)S(1)}, u32[]{:S(2)}, u32[]{:S(2)}) async-start(bf16[4,64,2048]{2,1,0:T(8,128)(2,1)} %bitcast.87), calls=%async_computation.3 | async-start | bytes 2097152 | tf_op jit(solution)/shard_map/all_to_all | solution.py:35
  177.6 1.0 copy-start.1
  178.6 6.9 %collective-permute-start.1 = (bf16[256,2048]{1,0:T(8,128)(2,1)S(1)}, bf16[256,2048]{1,0:T(8,128)(2,1)}, u32[]{:S(2)}, u32[]{:S(2)}) collective-permute-start(bf16[256,2048]{1,0:T(8,128)(2,1)S(1)} %bitcast.89), channel_id=1, source_target_pairs={{0,1},{1,0},{2,3},{3,2},{4,5},{5,4},{6,7},{7,6},{8,9},{9,8},{10,11... | collective-permute-start | bytes 3145736 | tf_op jit(solution)/shard_map/ppermute | solution.py:22
  203.3 4.6 %collective-permute-start.2 = (bf16[256,2048]{1,0:T(8,128)(2,1)S(1)}, bf16[256,2048]{1,0:T(8,128)(2,1)S(1)}, u32[]{:S(2)}, u32[]{:S(2)}) collective-permute-start(bf16[256,2048]{1,0:T(8,128)(2,1)S(1)} %slice.95), channel_id=1, source_target_pairs={{0,1},{1,0},{2,3},{3,2},{4,5},{5,4},{6,7},{7,6},{8,9},{9,8},{10,11... | collective-permute-start | bytes 3145736 | tf_op jit(solution)/shard_map/ppermute | solution.py:22
  210.8 19.1 %all-to-all-start.6 = ((bf16[4,64,2048]{2,1,0:T(8,128)(2,1)}), bf16[4,64,2048]{2,1,0:T(8,128)(2,1)}, u32[]{:S(2)}, u32[]{:S(2)}) async-start(bf16[4,64,2048]{2,1,0:T(8,128)(2,1)} %bitcast.88), calls=%async_computation.6 | async-start | bytes 2097152 | tf_op jit(solution)/shard_map/all_to_all | solution.py:35
Sparse Core Ops, SparseCore 0:
  20.3 119.2 all-gather.1

commit v2 on v1

--- a/solution.py
+++ b/solution.py
@@ -1,6 +1,8 @@
 import jax
 import jax.numpy as jnp
 from jax import lax
+from jax.experimental import pallas as pl
+from jax.experimental.pallas import tpu as pltpu
 from jax.sharding import Mesh
 from jax.sharding import PartitionSpec as P
 
@@ -22,18 +24,100 @@
     return lax.ppermute(value, "c", [(0, 1), (1, 0)])
 
 
-def row_norm(vals, gain):
-    count = vals.shape[1]
-    mean = jnp.sum(vals, axis=1, keepdims=True) / count
-    square = jnp.sum(vals * vals, axis=1, keepdims=True) / count
-    return (vals - mean) * lax.rsqrt(square - mean * mean + EPS) * gain[None, :]
-
-
 def summed_rows(own, other, peers):
     pair = own + to_partner(other.astype(BF16)).astype(F32)
     pieces = pair.astype(BF16).reshape(peers, own.shape[0] // peers, own.shape[1])
-    pieces = lax.all_to_all(pieces, "x", 0, 0, tiled=True)
-    return jnp.sum(pieces.astype(F32), axis=0)
+    return lax.all_to_all(pieces, "x", 0, 0, tiled=True)
+
+
+def whole_vmem():
+    return pl.BlockSpec(memory_space=pltpu.VMEM)
+
+
+def residual_norm(pieces, base, gain, parts, to_everyone):
+    peers, rows, width = pieces.shape
+
+    def body(pieces_ref, base_ref, gain_ref, out_ref):
+        added = pieces_ref[0].astype(F32)
+        for k in range(1, peers):
+            added = added + pieces_ref[k].astype(F32)
+        vals = ALPHA * base_ref[...].astype(F32) + added.astype(BF16).astype(F32)
+        mean = jnp.sum(vals, axis=1, keepdims=True) / width
+        square = jnp.sum(vals * vals, axis=1, keepdims=True) / width
+        done = (vals - mean) * lax.rsqrt(square - mean * mean + EPS) * gain_ref[...]
+        done = done.astype(BF16)
+        for k in range(parts):
+            if to_everyone:
+                out_ref[k] = done
+            else:
+                out_ref[k] = done[:, k * (width // parts) : (k + 1) * (width // parts)]
+
+    shape = (parts, rows, width if to_everyone else width // parts)
+    return pl.pallas_call(
+        body,
+        out_shape=jax.ShapeDtypeStruct(shape, BF16),
+        in_specs=[whole_vmem()] * 3,
+        out_specs=whole_vmem(),
+        name="first_norm" if to_everyone else "last_norm",
+    )(pieces, base, gain.reshape(1, width))
+
+
+def packed_ffw(gate, up, down):
+    cut = gate.shape[1] // 128 * 128
+    return jnp.concatenate([gate[:, :cut], up[:, :cut], gate[:, cut:], up[:, cut:], down.T], axis=1)
+
+
+def mixer(near, far, ffw, ff):
+    half, width = near.shape
+    cut = ff // 128 * 128
+    tail = ff - cut
+    steps = 8
+    depth = width // steps
+    columns = ffw.shape[1]
+    across = (((1,), (1,)), ((), ()))
+
+    def body(near_ref, far_ref, ffw_ref, keep_ref, give_ref, acc, down):
+        k = pl.program_id(0)
+        at = pl.ds(k * depth, depth)
+        weights = ffw_ref[:, : 2 * ff]
+        low = jnp.dot(near_ref[:, at], weights, preferred_element_type=F32)
+        high = jnp.dot(far_ref[:, at], weights, preferred_element_type=F32)
+        down[at, :] = ffw_ref[:, 2 * ff :]
+
+        @pl.when(k == 0)
+        def _():
+            acc[:half] = low
+            acc[half:] = high
+
+        @pl.when(k > 0)
+        def _():
+            acc[:half] += low
+            acc[half:] += high
+
+        @pl.when(k == steps - 1)
+        def _():
+            def rows(begin, count):
+                at = slice(begin, begin + count)
+                gate = acc[at, :cut]
+                main = (gate * lax.logistic(gate) * acc[at, cut : 2 * cut]).astype(BF16)
+                last = acc[at, 2 * cut :]
+                ends = (last[:, :tail] * lax.logistic(last[:, :tail]) * last[:, tail:]).astype(BF16)
+                out = lax.dot_general(main, down[:, :cut], across, preferred_element_type=F32)
+                return out + lax.dot_general(ends, down[:, cut:], across, preferred_element_type=F32)
+
+            give_ref[...] = rows(half, half).astype(BF16)
+            keep_ref[...] = rows(0, half)
+
+    return pl.pallas_call(
+        body,
+        grid=(steps,),
+        out_shape=(jax.ShapeDtypeStruct((half, width), F32), jax.ShapeDtypeStruct((half, width), BF16)),
+        in_specs=[whole_vmem(), whole_vmem(), pl.BlockSpec((depth, columns), lambda k: (k, 0))],
+        out_specs=(whole_vmem(), whole_vmem()),
+        scratch_shapes=[pltpu.VMEM((2 * half, 2 * ff), F32), pltpu.VMEM((width, ff), BF16)],
+        cost_estimate=pl.CostEstimate(flops=12 * half * width * ff, bytes_accessed=ffw.size * 2, transcendentals=2 * half * ff),
+        name="mixer",
+    )(near, far, ffw)
 
 
 def on_device(
@@ -57,11 +141,11 @@
     rows, feats = tokens.shape
     width = feats * parts
     sg = u_weight.shape[1]
-    ff = gate_weight.shape[1]
     own_rows = rows // parts
 
-    packed = jnp.concatenate([gate_weight, up_weight, down_weight.T], axis=1)
-    packed = lax.all_gather(packed, "y", axis=0, tiled=True)
+    blocks = sent_to_all(tokens, TP)
+
+    packed = lax.all_gather(packed_ffw(gate_weight, up_weight, down_weight), "y", axis=0, tiled=True)
     ffw = lax.all_gather(packed, "z", axis=0, tiled=True)
 
     small = jnp.concatenate([u_weight, v_weight, out_weight.T], axis=1)
@@ -71,11 +155,6 @@
     small = small.reshape(small.shape[0], -1, depth, small.shape[2])
     small = jnp.swapaxes(small, 0, 1).reshape(width, small.shape[3])
 
-    gains = sent_to_all(jnp.stack([gain_one, gain_two]), TP)
-    gain_1 = gains[:, 0].reshape(width)
-    gain_2 = gains[:, 1].reshape(width)
-
-    blocks = sent_to_all(tokens, TP)
     whole = jnp.moveaxis(blocks, 0, 1).reshape(rows, width)
     me = lax.axis_index(TP)
     mine = lax.dynamic_slice_in_dim(blocks, me * own_rows, own_rows, 1)
@@ -86,7 +165,12 @@
     gated = jax.nn.gelu(pre_u)
     valued = jax.nn.gelu(pre_v)
     sums = jnp.stack([jnp.sum(valued, axis=1), jnp.sum(valued * valued, axis=1)])
-    sums = jnp.sum(sent_to_all(sums, TP), axis=0)
+    gains = jnp.concatenate([gain_one, gain_two]).reshape(-1, rows)
+    known = sent_to_all(jnp.concatenate([sums, gains], axis=0), TP)
+    gains = known[:, 2:].reshape(parts, 2, feats)
+    gain_1 = gains[:, 0].reshape(width)
+    gain_2 = gains[:, 1].reshape(width)
+    sums = jnp.sum(known[:, :2], axis=0)
     count = sg * parts
     mean = sums[0][:, None] / count
     square = sums[1][:, None] / count
@@ -109,24 +193,13 @@
     across = (((1,), (1,)), ((), ()))
     give = lax.dot_general(give, out_t, across, preferred_element_type=F32)
     keep = lax.dot_general(keep, out_t, across, preferred_element_type=F32)
-    mix = summed_rows(keep, give, chips).astype(BF16)
-    first = row_norm(ALPHA * mine.astype(F32) + mix.astype(F32), gain_1).astype(BF16)
-
-    near = sent_to_all(first, "x").reshape(-1, width)
-    far = to_partner(near)
-    gate_w, up_w, down_t = ffw[:, :ff], ffw[:, ff : 2 * ff], ffw[:, 2 * ff :]
-
-    def mixer(left):
-        gate = jnp.dot(left, gate_w, preferred_element_type=F32)
-        upper = jnp.dot(left, up_w, preferred_element_type=F32)
-        hidden = (jax.nn.silu(gate) * upper).astype(BF16)
-        return lax.dot_general(hidden, down_t, across, preferred_element_type=F32)
-
-    both = mixer(jnp.concatenate([near, far], axis=0))
-    half = near.shape[0]
-    ffn = summed_rows(both[:half], both[half:], chips).astype(BF16)
-    last = row_norm(ALPHA * first.astype(F32) + ffn.astype(F32), gain_2).astype(BF16)
-    last = jnp.moveaxis(last.reshape(own_rows, parts, feats), 1, 0)
+    mix = summed_rows(keep, give, chips)
+    first = residual_norm(mix, mine, gain_1, chips, True)
+
+    near = lax.all_to_all(first, "x", 0, 0, tiled=True).reshape(-1, width)
+    keep, give = mixer(near, to_partner(near), ffw, gate_weight.shape[1])
+    ffn = summed_rows(keep, give, chips)
+    last = residual_norm(ffn, first[0], gain_2, parts, False)
     return lax.all_to_all(last, TP, 0, 0, tiled=True).reshape(rows, feats)
 
 

time: 254 us -> 253 us (level)
  Pallas kernels: 0 us -> 19.2 us
  blocking collectives: 71.5 us -> 89 us
  matrix products: 23.7 us -> 7.32 us
  waiting for transfers between devices: 72.8 us -> 62.3 us
  starting transfers between devices: 44.2 us -> 37.3 us
  other arithmetic: 10.3 us -> 3.78 us
    pallas_call x0 -> x3, Pallas kernels: none -> 19.2 us  [the longest x1 14.1 us: mixer(): pl.pallas_call(body, grid=(steps,), out_shape=(jax.ShapeDtypeStruct((half...]
    all_to_all x0 -> x1, blocking collectives: none -> 17.4 us  [on_device(): near = lax.all_to_all(first, 'x', 0, 0, tiled=True).reshape(-1, width)]
    dot_general x2 -> x0, matrix products: 16.1 us -> none  [the longest x1 10.7 us: mixer(): return lax.dot_general(hidden, down_t, across, preferred_element_type=F32)]
    all_to_all x4 -> x2, waiting for transfers between devices: 42.4 us -> 29.8 us  [sent_to_all(): return lax.all_to_all(copies, axis, split_axis=0, concat_axis=0, tiled=True)]
    all_to_all x4 -> x2, starting transfers between devices: 27.2 us -> 21.3 us  [sent_to_all(): return lax.all_to_all(copies, axis, split_axis=0, concat_axis=0, tiled=True)]
    reduce_sum x5 -> x1, other arithmetic: 3.82 us -> 0.02 us  [on_device(): sums = jnp.sum(known[:, :2], axis=0)]
    all_to_all x0 -> x1, local copies, waits for them, and re-layouts: none -> 2.88 us  [sent_to_all(): return lax.all_to_all(copies, axis, split_axis=0, concat_axis=0, tiled=True)]
    unnamed x20 -> x22, local copies, waits for them, and re-layouts: 2.03 us -> 4.64 us
  transfers between devices with their start and end apart: 10 -> 8, of which waited for: 8 -> 7; matrix products, arithmetic and copies ran while one was open for 9% -> 8% of each run, Pallas kernels for 0% -> 1%
where the time goes in v2:
time: 253 us; the launch traced here: 251 us
  blocking collectives  89 us (35%)
  waiting for transfers between devices  62.3 us (25%)
  starting transfers between devices  37.3 us (15%)
  Pallas kernels  19.2 us (8%)
  local copies, waits for them, and re-layouts  18.6 us (7%)
  between operations  13.6 us (5%)
  matrix products  7.32 us (3%)
  other arithmetic  3.78 us (1%)
    all_gather x1, blocking collectives, on_device(): small = lax.all_gather(small, 'z', axis=0, tiled=True)  32.9 us
    all_to_all x2, waiting for transfers between devices, sent_to_all(): return lax.all_to_all(copies, axis, split_axis=0, concat_axis=0, tiled=True)  29.8 us
    all_to_all x2, waiting for transfers between devices, summed_rows(): return lax.all_to_all(pieces, 'x', 0, 0, tiled=True)  25.5 us
    all_to_all x2, starting transfers between devices, sent_to_all(): return lax.all_to_all(copies, axis, split_axis=0, concat_axis=0, tiled=True)  21.3 us
    all_to_all x1, blocking collectives, on_device(): near = lax.all_to_all(first, 'x', 0, 0, tiled=True).reshape(-1, width)  17.4 us
    all_to_all x1, blocking collectives, sent_to_all(): return lax.all_to_all(copies, axis, split_axis=0, concat_axis=0, tiled=True)  15.1 us
    pallas_call x1, Pallas kernels, mixer(): pl.pallas_call(body, grid=(steps,), out_shape=(jax.ShapeDtypeStruct((half...  14.1 us
    all_gather x1, blocking collectives, on_device(): lax.all_gather(packed_ffw(gate_weight, up_weight, down_weight), 'y', axis...  12.7 us
  transfers between devices with their start and end apart: 8, of which 7 were waited for; matrix products, arithmetic and copies ran while one was open for 8% of the time, Pallas kernels for 1%

profile of v2, /device:TPU:1, one launch (start us, length us, event | category | flops | bytes accessed | tf_op | source)
XLA Modules:
  0.0 251.1 jit_solution(10726654086823701885)
XLA Ops:
  10.4 12.7 %all_gather.10 = bf16[128,2112]{1,0:T(8,128)(2,1)} all-gather(bf16[32,2112]{1,0:T(8,128)(2,1)S(1)} %concatenate.15), channel_id=1, replica_groups=mesh['z'=16,'y'=4,'x'=4,'c'=2] {'y'}, dimensions={0}, use_global_device_ids=true | all-gather | bytes 675840 | tf_op jit(solution)/shard_map/all_gather | solution.py:148
  23.8 32.9 %all_gather.9 = bf16[512,384]{1,0:T(8,128)(2,1)S(1)} all-gather(bf16[32,384]{1,0:T(8,128)(2,1)S(1)} %pad_maximum_fusion), channel_id=1, replica_groups=mesh['z'=16,'y'=4,'x'=4,'c'=2] {'z'}, dimensions={0}, use_global_device_ids=true | all-gather | bytes 417792 | tf_op jit(solution)/shard_map/all_gather | solution.py:153
  56.8 15.1 %all_to_all.35 = bf16[4,512,384]{2,1,0:T(8,128)(2,1)S(1)} all-to-all(bf16[4,512,384]{2,1,0:T(8,128)(2,1)S(1)} %broadcast_in_dim.17), channel_id=1, replica_groups=mesh['z'=16,'y'=4,'x'=4,'c'=2] {'y'}, dimensions={0} | all-to-all | bytes 3145728 | tf_op jit(solution)/shard_map/all_to_all | solution.py:20
  73.5 17.1 %all-to-all-start.1 = ((bf16[8,512,256]{2,1,0:T(8,128)(2,1)}), bf16[8,512,256]{2,1,0:T(8,128)(2,1)}, u32[]{:S(2)}, u32[]{:S(2)}) async-start(bf16[8,512,256]{2,1,0:T(8,128)(2,1)} %broadcast_in_dim.18), calls=%async_computation.1 | async-start | bytes 4194304 | tf_op jit(solution)/shard_map/all_to_all | solution.py:20
  92.0 24.9 %all-to-all-done.1 = bf16[8,512,256]{2,1,0:T(8,128)(2,1)} async-done(((bf16[8,512,256]{2,1,0:T(8,128)(2,1)}), bf16[8,512,256]{2,1,0:T(8,128)(2,1)}, u32[]{:S(2)}, u32[]{:S(2)}) %all-to-all-start.1) | async-done | bytes 2097184 | tf_op jit(solution)/shard_map/all_to_all | solution.py:20
  116.9 2.9 %copy.28 = bf16[8,512,256]{1,2,0:T(8,128)(2,1)S(1)} copy(bf16[8,512,256]{2,1,0:T(8,128)(2,1)} %all-to-all-done.1) | data formatting | bytes 4194304 | tf_op jit(solution)/shard_map/all_to_all | solution.py:20
  122.1 4.2 %all-to-all-start.2 = ((f32[8,3,512]{2,1,0:T(4,128)}), f32[8,3,512]{2,1,0:T(4,128)S(1)}, u32[]{:S(2)}, u32[]{:S(2)}) async-start(f32[8,3,512]{2,1,0:T(4,128)} %broadcast_in_dim.19), calls=%async_computation.2 | async-start | bytes 131072 | tf_op jit(solution)/shard_map/all_to_all | solution.py:20
  126.3 4.9 %all-to-all-done.2 = f32[8,3,512]{2,1,0:T(4,128)S(1)} async-done(((f32[8,3,512]{2,1,0:T(4,128)}), f32[8,3,512]{2,1,0:T(4,128)S(1)}, u32[]{:S(2)}, u32[]{:S(2)}) %all-to-all-start.2) | async-done | bytes 49184 | tf_op jit(solution)/shard_map/all_to_all | solution.py:20
  135.1 2.6 %collective-permute-start = (bf16[256,2048]{1,0:T(8,128)(2,1)S(1)}, bf16[256,2048]{1,0:T(8,128)(2,1)S(1)}, u32[]{:S(2)}, u32[]{:S(2)}) collective-permute-start(bf16[256,2048]{1,0:T(8,128)(2,1)S(1)} %convolution_convert_fusion), channel_id=1, source_target_pairs={{0,1},{1,0},{2,3},{3,2},{4,5},{5,4},{6,7},{7,6},{8,9},{9,8},{10,11... | collective-permute-start | bytes 3145736 | tf_op jit(solution)/shard_map/ppermute | solution.py:24
  137.7 2.3 collective-permute-done
  140.0 2.4 add_convert_fusion.1
  142.4 3.5 %all-to-all-start.3 = ((bf16[4,64,2048]{2,1,0:T(8,128)(2,1)}), bf16[4,64,2048]{2,1,0:T(8,128)(2,1)S(1)}, u32[]{:S(2)}, u32[]{:S(2)}) async-start(bf16[4,64,2048]{2,1,0:T(8,128)(2,1)} %bitcast.24), calls=%async_computation.3 | async-start | bytes 2097152 | tf_op jit(solution)/shard_map/all_to_all | solution.py:30
  148.4 12.4 %all-to-all-done.3.pieces_ref = bf16[4,64,2048]{2,1,0:T(8,128)(2,1)S(1)} async-done(((bf16[4,64,2048]{2,1,0:T(8,128)(2,1)}), bf16[4,64,2048]{2,1,0:T(8,128)(2,1)S(1)}, u32[]{:S(2)}, u32[]{:S(2)}) %all-to-all-start.3) | async-done | bytes 1048608 | tf_op jit(solution)/shard_map/all_to_all | solution.py:30
  161.7 2.7 %first_norm.1 = bf16[4,64,2048]{2,1,0:T(8,128)(2,1)} custom-call(bf16[4,64,2048]{2,1,0:T(8,128)(2,1)} %copy-done, bf16[64,2048]{1,0:T(8,128)(2,1)} %bitcast.66, f32[1,2048]{1,0:T(1,128)} %bitcast.77), custom_call_target="tpu_custom_call" | custom-call | tf_op jit(solution)/shard_map/first_norm/pallas_call | solution.py:56
  164.4 17.4 %all_to_all.36 = bf16[4,64,2048]{2,1,0:T(8,128)(2,1)S(1)} all-to-all(bf16[4,64,2048]{2,1,0:T(8,128)(2,1)} %first_norm.1), channel_id=1, replica_groups=mesh['z'=16,'y'=4,'x'=4,'c'=2] {'x'}, dimensions={0} | all-to-all | bytes 2097152 | tf_op jit(solution)/shard_map/all_to_all | solution.py:199
  181.9 4.0 %collective-permute-start.1 = (bf16[256,2048]{1,0:T(8,128)(2,1)S(1)}, bf16[256,2048]{1,0:T(8,128)(2,1)S(1)}, u32[]{:S(2)}, u32[]{:S(2)}) collective-permute-start(bf16[256,2048]{1,0:T(8,128)(2,1)S(1)} %bitcast.67), channel_id=1, source_target_pairs={{0,1},{1,0},{2,3},{3,2},{4,5},{5,4},{6,7},{7,6},{8,9},{9,8},{10,11... | collective-permute-start | bytes 3145736 | tf_op jit(solution)/shard_map/ppermute | solution.py:24
  189.1 14.1 %mixer.1 = (f32[256,2048]{1,0:T(8,128)}, bf16[256,2048]{1,0:T(8,128)(2,1)}) custom-call(bf16[256,2048]{1,0:T(8,128)(2,1)} %bitcast.68, bf16[256,2048]{1,0:T(8,128)(2,1)} %copy-done.9, bf16[2048,2112]{1,0:T(8,128)(2,1)} %all-gather.2.cloned.1.call-done.ffw_ref), custom_call_target="tpu_custom_call" | custom-call | flops 4429185024 | bytes 8650752 | tf_op jit(solution)/shard_map/mixer/pallas_call | solution.py:111
  203.2 2.3 collective-permute-start.2
  205.5 2.5 collective-permute-done.2
  207.9 2.9 %add_convert_fusion = bf16[256,2048]{1,0:T(8,128)(2,1)} fusion(f32[256,2048]{1,0:T(8,128)} %get-tuple-element.7, bf16[256,2048]{1,0:T(8,128)(2,1)S(1)} %collective-permute-done.2), kind=kLoop, calls=%fused_computation.1 | loop fusion | flops 1572864 | bytes 4194304 | tf_op jit(solution)/shard_map/convert_element_type | solution.py:29
  210.8 3.5 %all-to-all-start.5 = ((bf16[4,64,2048]{2,1,0:T(8,128)(2,1)}), bf16[4,64,2048]{2,1,0:T(8,128)(2,1)S(1)}, u32[]{:S(2)}, u32[]{:S(2)}) async-start(bf16[4,64,2048]{2,1,0:T(8,128)(2,1)} %bitcast.29), calls=%async_computation.5 | async-start | bytes 2097152 | tf_op jit(solution)/shard_map/all_to_all | solution.py:30
  216.0 13.1 %all-to-all-done.5.pieces_ref = bf16[4,64,2048]{2,1,0:T(8,128)(2,1)S(1)} async-done(((bf16[4,64,2048]{2,1,0:T(8,128)(2,1)}), bf16[4,64,2048]{2,1,0:T(8,128)(2,1)S(1)}, u32[]{:S(2)}, u32[]{:S(2)}) %all-to-all-start.5) | async-done | bytes 1048608 | tf_op jit(solution)/shard_map/all_to_all | solution.py:30
  230.1 2.4 last_norm.1
  232.6 11.0 %all_to_all.37 = bf16[8,64,256]{2,1,0:T(8,128)(2,1)S(1)} all-to-all(bf16[8,64,256]{2,1,0:T(8,128)(2,1)} %last_norm.1), channel_id=1, replica_groups=mesh['z'=16,'y'=4,'x'=4,'c'=2] {'x','c'}, dimensions={0} | all-to-all | bytes 524288 | tf_op jit(solution)/shard_map/all_to_all | solution.py:203
  (55 shorter events, 23.7 us)
Async XLA Ops:
  6.5 181.6 %all-gather.2.cloned.1.call-start = ((), (), s32[]{:S(2)}) async-start(), calls=%async_computation.7 | async-start | bytes 9469952 | tf_op jit(solution)/shard_map/all_gather | solution.py:149
  56.7 15.2 %copy-start.3 = (bf16[512,256]{1,0:T(8,128)(2,1)S(1)}, bf16[512,256]{1,0:T(8,128)(2,1)}, u32[]{:S(2)}) copy-start(bf16[512,256]{1,0:T(8,128)(2,1)} %param.12) | copy-start | bytes 786436
  73.4 17.1 %copy-start.5 = (f32[256]{0:T(256)S(1)}, f32[256]{0:T(256)}, u32[]{:S(2)}) copy-start(f32[256]{0:T(256)} %param.23) | copy-start | bytes 3076
  73.5 17.1 %copy-start.6 = (f32[256]{0:T(256)S(1)}, f32[256]{0:T(256)}, u32[]{:S(2)}) copy-start(f32[256]{0:T(256)} %param.19) | copy-start | bytes 3076
  73.5 43.4 %all-to-all-start.1 = ((bf16[8,512,256]{2,1,0:T(8,128)(2,1)}), bf16[8,512,256]{2,1,0:T(8,128)(2,1)}, u32[]{:S(2)}, u32[]{:S(2)}) async-start(bf16[8,512,256]{2,1,0:T(8,128)(2,1)} %broadcast_in_dim.18), calls=%async_computation.1 | async-start | bytes 4194304 | tf_op jit(solution)/shard_map/all_to_all | solution.py:20
  119.8 11.5 %copy-start.7 = (f32[128]{0:T(128)S(1)}, f32[128]{0:T(128)}, u32[]{:S(2)}) copy-start(f32[128]{0:T(128)} %param.15) | copy-start | bytes 1540
  119.8 11.7 %copy-start.4 = (bf16[1,128,128]{2,1,0:T(8,128)(2,1)S(1)}, bf16[1,128,128]{2,1,0:T(8,128)(2,1)}, u32[]{:S(2)}) copy-start(bf16[1,128,128]{2,1,0:T(8,128)(2,1)} %param.16) | copy-start | bytes 98308
  119.8 11.7 %copy-start.8 = (f32[1,128]{1,0:T(1,128)S(1)}, f32[1,128]{1,0:T(1,128)}, u32[]{:S(2)}) copy-start(f32[1,128]{1,0:T(1,128)} %param.17) | copy-start | bytes 1540
  122.1 9.2 %all-to-all-start.2 = ((f32[8,3,512]{2,1,0:T(4,128)}), f32[8,3,512]{2,1,0:T(4,128)S(1)}, u32[]{:S(2)}, u32[]{:S(2)}) async-start(f32[8,3,512]{2,1,0:T(4,128)} %broadcast_in_dim.19), calls=%async_computation.2 | async-start | bytes 131072 | tf_op jit(solution)/shard_map/all_to_all | solution.py:20
  135.1 4.9 %collective-permute-start = (bf16[256,2048]{1,0:T(8,128)(2,1)S(1)}, bf16[256,2048]{1,0:T(8,128)(2,1)S(1)}, u32[]{:S(2)}, u32[]{:S(2)}) collective-permute-start(bf16[256,2048]{1,0:T(8,128)(2,1)S(1)} %convolution_convert_fusion), channel_id=1, source_target_pairs={{0,1},{1,0},{2,3},{3,2},{4,5},{5,4},{6,7},{7,6},{8,9},{9,8},{10,11... | collective-permute-start | bytes 3145736 | tf_op jit(solution)/shard_map/ppermute | solution.py:24
  142.4 18.3 %all-to-all-start.3 = ((bf16[4,64,2048]{2,1,0:T(8,128)(2,1)}), bf16[4,64,2048]{2,1,0:T(8,128)(2,1)S(1)}, u32[]{:S(2)}, u32[]{:S(2)}) async-start(bf16[4,64,2048]{2,1,0:T(8,128)(2,1)} %bitcast.24), calls=%async_computation.3 | async-start | bytes 2097152 | tf_op jit(solution)/shard_map/all_to_all | solution.py:30
  160.7 1.0 copy-start
  181.9 6.3 %copy-start.2 = (bf16[4,64,2048]{2,1,0:T(8,128)(2,1)}, bf16[4,64,2048]{2,1,0:T(8,128)(2,1)S(1)}, u32[]{:S(2)}) copy-start(bf16[4,64,2048]{2,1,0:T(8,128)(2,1)S(1)} %all_to_all.36) | copy-start | bytes 3145732
  181.9 6.3 %collective-permute-start.1 = (bf16[256,2048]{1,0:T(8,128)(2,1)S(1)}, bf16[256,2048]{1,0:T(8,128)(2,1)S(1)}, u32[]{:S(2)}, u32[]{:S(2)}) collective-permute-start(bf16[256,2048]{1,0:T(8,128)(2,1)S(1)} %bitcast.67), channel_id=1, source_target_pairs={{0,1},{1,0},{2,3},{3,2},{4,5},{5,4},{6,7},{7,6},{8,9},{9,8},{10,11... | collective-permute-start | bytes 3145736 | tf_op jit(solution)/shard_map/ppermute | solution.py:24
  188.2 1.0 copy-start.9
  203.2 4.8 %collective-permute-start.2 = (bf16[256,2048]{1,0:T(8,128)(2,1)}, bf16[256,2048]{1,0:T(8,128)(2,1)S(1)}, u32[]{:S(2)}, u32[]{:S(2)}) collective-permute-start(bf16[256,2048]{1,0:T(8,128)(2,1)} %get-tuple-element.8), channel_id=1, source_target_pairs={{0,1},{1,0},{2,3},{3,2},{4,5},{5,4},{6,7},{7,6},{8,9},{9,8},{10,11... | collective-permute-start | bytes 3145736 | tf_op jit(solution)/shard_map/ppermute | solution.py:24
  210.8 18.3 %all-to-all-start.5 = ((bf16[4,64,2048]{2,1,0:T(8,128)(2,1)}), bf16[4,64,2048]{2,1,0:T(8,128)(2,1)S(1)}, u32[]{:S(2)}, u32[]{:S(2)}) async-start(bf16[4,64,2048]{2,1,0:T(8,128)(2,1)} %bitcast.29), calls=%async_computation.5 | async-start | bytes 2097152 | tf_op jit(solution)/shard_map/all_to_all | solution.py:30
  229.2 1.0 copy-start.1
Sparse Core Ops, SparseCore 0:
  23.2 119.2 all-gather.1

commit v3 on v2

v3 whole, which is shorter than its diff:
```python
import jax
import jax.numpy as jnp
from jax import lax
from jax.experimental import pallas as pl
from jax.experimental.pallas import tpu as pltpu
from jax.sharding import Mesh
from jax.sharding import PartitionSpec as P

FS = ("z", "y")
TP = ("x", "c")

EPS = 1e-05
ALPHA = 2.0**0.25
BF16 = jnp.bfloat16
F32 = jnp.float32
ACROSS = (((1,), (1,)), ((), ()))


def sent_to_all(value, axis):
    copies = jnp.broadcast_to(value, (lax.axis_size(axis), *value.shape))
    return lax.all_to_all(copies, axis, split_axis=0, concat_axis=0, tiled=True)


def to_partner(value):
    return lax.ppermute(value, "c", [(0, 1), (1, 0)])


def row_norm(vals, gain):
    count = vals.shape[1]
    mean = jnp.sum(vals, axis=1, keepdims=True) / count
    square = jnp.sum(vals * vals, axis=1, keepdims=True) / count
    return (vals - mean) * lax.rsqrt(square - mean * mean + EPS) * gain


def summed_rows(own, other, peers):
    pair = own + to_partner(other.astype(BF16)).astype(F32)
    pieces = pair.astype(BF16).reshape(peers, own.shape[0] // peers, own.shape[1])
    return lax.all_to_all(pieces, "x", 0, 0, tiled=True)


def whole_vmem():
    return pl.BlockSpec(memory_space=pltpu.VMEM)


def last_norm(pieces, base, gain, parts):
    peers, rows, width = pieces.shape

    def body(pieces_ref, base_ref, gain_ref, out_ref):
        added = pieces_ref[0].astype(F32)
        for k in range(1, peers):
            added = added + pieces_ref[k].astype(F32)
        vals = ALPHA * base_ref[...].astype(F32) + added.astype(BF16).astype(F32)
        done = row_norm(vals, gain_ref[...]).astype(BF16)
        for k in range(parts):
            out_ref[k] = done[:, k * (width // parts) : (k + 1) * (width // parts)]

    return pl.pallas_call(
        body,
        out_shape=jax.ShapeDtypeStruct((parts, rows, width // parts), BF16),
        in_specs=[whole_vmem()] * 3,
        out_specs=whole_vmem(),
        name="last_norm",
    )(pieces, base, gain.reshape(1, width))


def first_rows(place, gated, blocks, gain, near, far):
    parts, rows, channels = gated.shape
    feats = blocks.shape[2]
    width = parts * feats
    peers = len(near)
    cores = 2
    chips = parts // cores
    depth = 32
    zs = near[0].shape[0] // depth
    wide = near[0].shape[1]
    step = 128

    def body(place_ref, gated_ref, blocks_ref, gain_ref, *rest):
        pieces, out_ref, weights, left, sems = rest[: 2 * peers], rest[-4], rest[-3], rest[-2], rest[-1]
        core = place_ref[0]
        y = place_ref[1]
        copies = []
        for n in range(2 * peers):
            which = core if n < peers else 1 - core
            at = lax.rem(y + 2 * peers - n, peers)
            copies.append(pltpu.make_async_copy(pieces[n], weights.at[which, :, at], sems.at[n]))
        for c in copies:
            c.start()
        for k in range(parts):
            at = (k % cores * chips + k // cores) * channels
            left[:, at : at + channels] = gated_ref[k]
        for c in copies:
            c.wait()
        for r in range(0, rows, step):
            mix = jnp.zeros((step, width), F32)
            for k in range(cores):
                right = weights[k].reshape(width, wide)
                mix += lax.dot_general(left[r : r + step, k * wide : (k + 1) * wide], right, ACROSS, preferred_element_type=F32)
            base = jnp.concatenate([blocks_ref[k, r : r + step] for k in range(parts)], axis=1)
            vals = ALPHA * base.astype(F32) + mix.astype(BF16).astype(F32)
            out_ref[r : r + step] = row_norm(vals, gain_ref[...]).astype(BF16)

    given = [p.reshape(zs, depth, wide) for p in (*near, *far)]
    return pl.pallas_call(
        body,
        out_shape=jax.ShapeDtypeStruct((rows, width), BF16),
        in_specs=[pl.BlockSpec(memory_space=pltpu.SMEM)] + [whole_vmem()] * 3 + [pl.BlockSpec(memory_space=pl.ANY)] * len(given),
        out_specs=whole_vmem(),
        scratch_shapes=[
            pltpu.VMEM((cores, zs, peers, depth, wide), BF16),
            pltpu.VMEM((rows, parts * channels), BF16),
            pltpu.SemaphoreType.DMA((len(given),)),
        ],
        cost_estimate=pl.CostEstimate(flops=2 * rows * width * parts * channels, bytes_accessed=6 << 20, transcendentals=rows),
        name="first_rows",
    )(place, gated, blocks, gain.reshape(1, width), *given)


def packed_weights(gate, up, down):
    cut = gate.shape[1] // 128 * 128
    low = cut - 128
    down = down.T
    big = jnp.concatenate([gate[:, :cut], up[:, :cut], gate[:, cut:], up[:, cut:], down[:, low:]], axis=1)
    return big, down[:, :low]


def mixer(place, first, big, downs, ff):
    rows, width = first.shape
    half = rows // 2
    cut = ff // 128 * 128
    tail = ff - cut
    low = cut - 128
    peers = len(downs)
    depth = 32
    zs = width // peers // depth
    edges = [0, 384, 768, 1152, big.shape[1]]
    chunks = len(edges) - 1

    def body(place_ref, first_ref, big_ref, *rest):
        pieces = rest[:peers]
        keep_ref, give_ref = rest[peers : peers + 2]
        weights = rest[peers + 2 : -3]
        down, acc, sems = rest[-3:]
        core = place_ref[0]
        y = place_ref[1]
        copies = []
        for n in range(chunks):
            at = pl.ds(edges[n], edges[n + 1] - edges[n])
            copies.append(pltpu.make_async_copy(big_ref.at[:, at], weights[n], sems.at[n]))
        for n in range(peers):
            at = lax.rem(y + peers - n, peers)
            copies.append(pltpu.make_async_copy(pieces[n], down.at[:, at], sems.at[chunks + n]))
        for c in copies:
            c.start()
        for n in range(chunks):
            copies[n].wait()
            begin, count = edges[n], min(edges[n + 1], 2 * ff) - edges[n]
            acc[:, begin : begin + count] = jnp.dot(first_ref[...], weights[n][:, :count], preferred_element_type=F32)
        for c in copies[chunks:]:
            c.wait()
        gate = acc[:, :cut]
        main = (gate * lax.logistic(gate) * acc[:, cut : 2 * cut]).astype(BF16)
        last = acc[:, 2 * cut :]
        ends = (last[:, :tail] * lax.logistic(last[:, :tail]) * last[:, tail:]).astype(BF16)
        rest = jnp.concatenate([main[:, low:], ends], axis=1)
        acc_out = lax.dot_general(main[:, :low], down[...].reshape(width, low), ACROSS, preferred_element_type=F32)
        acc_out += lax.dot_general(rest, weights[-1][:, 2 * ff - edges[-2] :], ACROSS, preferred_element_type=F32)

        @pl.when(core == 0)
        def _():
            keep_ref[...] = acc_out[:half]
            give_ref[...] = acc_out[half:].astype(BF16)

        @pl.when(core == 1)
        def _():
            keep_ref[...] = acc_out[half:]
            give_ref[...] = acc_out[:half].astype(BF16)

    given = [p.reshape(zs, depth, p.shape[1]) for p in downs]
    return pl.pallas_call(
        body,
        out_shape=(jax.ShapeDtypeStruct((half, width), F32), jax.ShapeDtypeStruct((half, width), BF16)),
        in_specs=[pl.BlockSpec(memory_space=pltpu.SMEM), whole_vmem()] + [pl.BlockSpec(memory_space=pl.ANY)] * (1 + peers),
        out_specs=(whole_vmem(), whole_vmem()),
        scratch_shapes=[
            *(pltpu.VMEM((width, edges[n + 1] - edges[n]), BF16) for n in range(chunks)),
            pltpu.VMEM((zs, peers, depth, low), BF16),
            pltpu.VMEM((rows, 2 * ff), F32),
            pltpu.SemaphoreType.DMA((chunks + peers,)),
        ],
        cost_estimate=pl.CostEstimate(flops=6 * rows * width * ff, bytes_accessed=12 << 20, transcendentals=rows * ff),
        name="mixer",
    )(place, first, big, *given)


def from_each(value, axis):
    size = lax.axis_size(axis)
    return [value] + [lax.ppermute(value, axis, [(i, (i + k) % size) for i in range(size)]) for k in range(1, size)]


def on_device(
    tokens,
    u_weight,
    v_weight,
    sg_gain,
    spatial_weight,
    spatial_bias,
    out_weight,
    gain_one,
    gate_weight,
    up_weight,
    down_weight,
    gain_two,
):
    core = lax.axis_index("c")
    chips = lax.axis_size("x")
    cores = lax.axis_size("c")
    parts = chips * cores
    rows, feats = tokens.shape
    width = feats * parts
    sg = u_weight.shape[1]
    own_rows = rows // parts

    blocks = sent_to_all(tokens, TP)

    big, rest = packed_weights(gate_weight, up_weight, down_weight)
    big = lax.all_gather(big, "y", axis=0, tiled=True)
    big = lax.all_gather(big, "z", axis=0, tiled=True)

    small = jnp.concatenate([u_weight, v_weight, out_weight.T, rest], axis=1)
    depth = small.shape[0]
    small = lax.all_gather(small, "z", axis=0, tiled=True)
    gates = sent_to_all(small[:, : 2 * sg], "y")
    gates = gates.reshape(gates.shape[0], -1, depth, 2 * sg)
    gates = jnp.swapaxes(gates, 0, 1).reshape(width, 2 * sg)
    out_x = lax.all_gather(small[:, 2 * sg : 3 * sg], "x", axis=1, tiled=True)
    out_near = from_each(out_x, "y")
    out_far = [to_partner(piece) for piece in out_near]
    downs = from_each(small[:, 3 * sg :], "y")

    whole = jnp.moveaxis(blocks, 0, 1).reshape(rows, width)

    pre_u = jnp.dot(whole, gates[:, :sg], preferred_element_type=F32)
    pre_v = jnp.dot(whole, gates[:, sg:], preferred_element_type=F32)
    gated = jax.nn.gelu(pre_u)
    valued = jax.nn.gelu(pre_v)
    sums = jnp.stack([jnp.sum(valued, axis=1), jnp.sum(valued * valued, axis=1)])
    gains = jnp.concatenate([gain_one, gain_two]).reshape(-1, rows)
    known = sent_to_all(jnp.concatenate([sums, gains], axis=0), TP)
    gains = known[:, 2:].reshape(parts, 2, feats)
    gain_1 = gains[:, 0].reshape(width)
    gain_2 = gains[:, 1].reshape(width)
    sums = jnp.sum(known[:, :2], axis=0)
    count = sg * parts
    mean = sums[0][:, None] / count
    square = sums[1][:, None] / count
    normed = (valued - mean) * lax.rsqrt(square - mean * mean + EPS) * sg_gain[None, :]
    normed = normed.astype(BF16)

    groups = spatial_weight.shape[0]
    block = spatial_weight.shape[1]
    shaped = normed.reshape(rows // block, block, groups, sg // groups)
    lower = jnp.tril(jnp.ones((block, block), jnp.bool_))
    masked = jnp.where(lower[None], spatial_weight, jnp.zeros_like(spatial_weight))
    mixed = jnp.einsum("gij,njgd->nigd", masked, shaped, preferred_element_type=F32)
    mixed = mixed + spatial_bias.T[None, :, :, None]
    gated_out = (gated * mixed.reshape(rows, sg)).astype(BF16)

    everyone = sent_to_all(gated_out, TP)
    chip = lax.axis_index("x")
    place = jnp.stack([core, lax.axis_index("y")]).astype(jnp.int32)
    first = first_rows(place, everyone, blocks, gain_1, out_near, out_far)
    keep, give = mixer(place, first, big, downs, gate_weight.shape[1])
    ffn = summed_rows(keep, give, chips)
    mine = lax.dynamic_slice_in_dim(first, (core * chips + chip) * own_rows, own_rows, 0)
    last = last_norm(ffn, mine, gain_2, parts)
    last = lax.all_to_all(last, TP, 0, 0, tiled=True)
    return jnp.swapaxes(last.reshape(chips, cores, own_rows, feats), 0, 1).reshape(rows, feats)


def solution(mesh):
    tp = mesh.shape["tp"]
    finer = Mesh(mesh.devices.reshape(16, 4, tp // 2, 2), ("z", "y", "x", "c"))
    return jax.shard_map(
        on_device,
        mesh=finer,
        in_specs=(
            P(FS, TP),
            P(FS, TP),
            P(FS, TP),
            P(TP),
            P(TP, None, None),
            P(TP, None),
            P(TP, FS),
            P(TP),
            P(FS, TP),
            P(FS, TP),
            P(TP, FS),
            P(TP),
        ),
        out_specs=P(FS, TP),
        check_vma=False,
    )
```

time: 253 us -> 277 us (1.095)
  starting transfers between devices: 37.3 us -> 65.5 us
  waiting for transfers between devices: 62.3 us -> 48.2 us
  Pallas kernels: 19.2 us -> 28.4 us
  matrix products: 7.32 us -> 2.73 us
  local copies, waits for them, and re-layouts: 18.6 us -> 22.4 us
    all_to_all x2 -> x1, blocking collectives: 28.4 us -> 11 us  [on_device(): last = lax.all_to_all(last, TP, 0, 0, tiled=True)]
    ppermute x0 -> x6, starting transfers between devices: none -> 17 us  [from_each(): lax.ppermute(value, axis, [(i, (i + k) % size) for i in range(size)])]
    all_to_all x2 -> x1, waiting for transfers between devices: 25.5 us -> 13.1 us  [summed_rows(): return lax.all_to_all(pieces, 'x', 0, 0, tiled=True)]
    all_gather x1 -> x2, blocking collectives: 12.7 us -> 24.6 us  [the longest x1 12.5 us: on_device(): out_x = lax.all_gather(small[:, 2 * sg:3 * sg], 'x', axis=1, tiled=True)]
    pallas_call x3, Pallas kernels: 19.2 us -> 28.4 us  [the longest x1 14.4 us: mixer(): pl.pallas_call(body, out_shape=(jax.ShapeDtypeStruct((half, width), F32),...]
    all_gather x1, blocking collectives: 32.9 us -> 41.2 us  [on_device(): small = lax.all_gather(small, 'z', axis=0, tiled=True)]
    ppermute x3 -> x5, starting transfers between devices: 8.88 us -> 16.8 us  [to_partner(): return lax.ppermute(value, 'c', [(0, 1), (1, 0)])]
    ppermute x0 -> x6, waiting for transfers between devices: none -> 7.51 us  [from_each(): lax.ppermute(value, axis, [(i, (i + k) % size) for i in range(size)])]
  transfers between devices with their start and end apart: 8 -> 16, of which waited for: 7 -> 5; matrix products, arithmetic and copies ran while one was open for 8% -> 7% of each run, Pallas kernels for 1% -> 4%
where the time goes in v3:
time: 277 us; the launch traced here: 275 us
  blocking collectives  89 us (32%)
  starting transfers between devices  65.5 us (24%)
  waiting for transfers between devices  48.2 us (17%)
  Pallas kernels  28.4 us (10%)
  local copies, waits for them, and re-layouts  22.4 us (8%)
  between operations  13.8 us (5%)
  other arithmetic  5.18 us (2%)
    all_gather x1, blocking collectives, on_device(): small = lax.all_gather(small, 'z', axis=0, tiled=True)  41.2 us
    all_to_all x3, starting transfers between devices, sent_to_all(): return lax.all_to_all(copies, axis, split_axis=0, concat_axis=0, tiled=True)  28.1 us
    all_to_all x3, waiting for transfers between devices, sent_to_all(): return lax.all_to_all(copies, axis, split_axis=0, concat_axis=0, tiled=True)  25.1 us
    ppermute x6, starting transfers between devices, from_each(): lax.ppermute(value, axis, [(i, (i + k) % size) for i in range(size)])  17 us
    ppermute x5, starting transfers between devices, to_partner(): return lax.ppermute(value, 'c', [(0, 1), (1, 0)])  16.8 us
    pallas_call x1, Pallas kernels, mixer(): pl.pallas_call(body, out_shape=(jax.ShapeDtypeStruct((half, width), F32),...  14.4 us
    all_to_all x1, waiting for transfers between devices, summed_rows(): return lax.all_to_all(pieces, 'x', 0, 0, tiled=True)  13.1 us
    all_gather x1, blocking collectives, on_device(): out_x = lax.all_gather(small[:, 2 * sg:3 * sg], 'x', axis=1, tiled=True)  12.5 us
  transfers between devices with their start and end apart: 16, of which 5 were waited for; matrix products, arithmetic and copies ran while one was open for 7% of the time, Pallas kernels for 4%

profile of v3, /device:TPU:1, one launch (start us, length us, event | category | flops | bytes accessed | tf_op | source)
XLA Modules:
  0.0 275.2 jit_solution(3316177400463534756)
XLA Ops:
  10.3 12.2 %all_gather.14 = bf16[128,1600]{1,0:T(8,128)(2,1)} all-gather(bf16[32,1600]{1,0:T(8,128)(2,1)S(1)} %concatenate.15), channel_id=1, replica_groups=mesh['z'=16,'y'=4,'x'=4,'c'=2] {'y'}, dimensions={0}, use_global_device_ids=true | all-gather | bytes 512000 | tf_op jit(solution)/shard_map/all_gather | solution.py:227
  24.0 41.2 %all_gather.12 = bf16[512,896]{1,0:T(8,128)(2,1)S(1)} all-gather(bf16[32,896]{1,0:T(8,128)(2,1)S(1)} %pad_maximum_fusion), channel_id=1, replica_groups=mesh['z'=16,'y'=4,'x'=4,'c'=2] {'z'}, dimensions={0}, use_global_device_ids=true | all-gather | bytes 974848 | tf_op jit(solution)/shard_map/all_gather | solution.py:232
  66.3 12.2 %all_to_all.30 = bf16[4,512,256]{2,1,0:T(8,128)(2,1)S(1)} all-to-all(bf16[4,512,256]{2,1,0:T(8,128)(2,1)S(1)} %broadcast_in_dim.20), channel_id=1, replica_groups=mesh['z'=16,'y'=4,'x'=4,'c'=2] {'y'}, dimensions={0} | all-to-all | bytes 2097152 | tf_op jit(solution)/shard_map/all_to_all | solution.py:21
  80.0 16.0 %all-to-all-start.1 = ((bf16[8,512,256]{2,1,0:T(8,128)(2,1)}), bf16[8,512,256]{2,1,0:T(8,128)(2,1)S(1)}, u32[]{:S(2)}, u32[]{:S(2)}) async-start(bf16[8,512,256]{2,1,0:T(8,128)(2,1)} %broadcast_in_dim.21), calls=%async_computation.1 | async-start | bytes 4194304 | tf_op jit(solution)/shard_map/all_to_all | solution.py:21
  97.1 25.1 %all-to-all-done.1.blocks_ref = bf16[8,512,256]{2,1,0:T(8,128)(2,1)S(1)} async-done(((bf16[8,512,256]{2,1,0:T(8,128)(2,1)}), bf16[8,512,256]{2,1,0:T(8,128)(2,1)S(1)}, u32[]{:S(2)}, u32[]{:S(2)}) %all-to-all-start.1) | async-done | bytes 2097184 | tf_op jit(solution)/shard_map/all_to_all | solution.py:21
  123.5 2.9 %copy.29 = bf16[512,8,256]{0,2,1:T(8,128)(2,1)S(1)} copy(bf16[512,8,256]{2,0,1:T(8,128)(2,1)} %bitcast.64) | data formatting | bytes 4194304 | tf_op jit(solution)/shard_map/transpose | solution.py:241
  127.8 4.8 %all-to-all-start.2 = ((f32[8,3,512]{2,1,0:T(4,128)}), f32[8,3,512]{2,1,0:T(4,128)}, u32[]{:S(2)}, u32[]{:S(2)}) async-start(f32[8,3,512]{2,1,0:T(4,128)} %broadcast_in_dim.22), calls=%async_computation.2 | async-start | bytes 131072 | tf_op jit(solution)/shard_map/all_to_all | solution.py:21
  132.6 12.5 %all_gather.13 = bf16[512,512]{1,0:T(8,128)(2,1)} all-gather(bf16[512,128]{1,0:T(8,128)(2,1)S(1)} %slice-done), channel_id=1, replica_groups=mesh['z'=16,'y'=4,'x'=4,'c'=2] {'x'}, dimensions={1}, use_global_device_ids=true | all-gather | bytes 655360 | tf_op jit(solution)/shard_map/all_gather | solution.py:236
  147.2 3.7 %collective-permute-start.1 = (bf16[512,512]{1,0:T(8,128)(2,1)}, bf16[512,512]{1,0:T(8,128)(2,1)}, u32[]{:S(2)}, u32[]{:S(2)}) collective-permute-start(bf16[512,512]{1,0:T(8,128)(2,1)} %all_gather.13), channel_id=1, source_target_pairs={{0,16},{8,24},{16,0},{24,8},{1,17},{9,25},{17,1},{25,9},{2,18},{10... | collective-permute-start | bytes 1572872 | tf_op jit(solution)/shard_map/ppermute | solution.py:198
  150.9 2.5 collective-permute-start.2
  159.1 7.3 %all-to-all-start.3 = ((bf16[8,512,128]{2,1,0:T(8,128)(2,1)}), bf16[8,512,128]{2,1,0:T(8,128)(2,1)S(1)}, u32[]{:S(2)}, u32[]{:S(2)}) async-start(bf16[8,512,128]{2,1,0:T(8,128)(2,1)} %broadcast_in_dim.24), calls=%async_computation.3 | async-start | bytes 2097152 | tf_op jit(solution)/shard_map/all_to_all | solution.py:21
  168.3 7.6 %collective-permute-start.4 = (bf16[512,512]{1,0:T(8,128)(2,1)}, bf16[512,512]{1,0:T(8,128)(2,1)S(1)}, u32[]{:S(2)}, u32[]{:S(2)}) collective-permute-start(bf16[512,512]{1,0:T(8,128)(2,1)} %collective-permute-done), channel_id=1, source_target_pairs={{0,1},{1,0},{2,3},{3,2},{4,5},{5,4},{6,7},{7,6},{8,9},{9,8},{10,11... | collective-permute-start | bytes 1572872 | tf_op jit(solution)/shard_map/ppermute | solution.py:25
  183.6 3.6 %collective-permute-start.8 = (bf16[512,512]{1,0:T(8,128)(2,1)}, bf16[512,512]{1,0:T(8,128)(2,1)}, u32[]{:S(2)}, u32[]{:S(2)}) collective-permute-start(bf16[512,512]{1,0:T(8,128)(2,1)} %slice.79), channel_id=1, source_target_pairs={{0,16},{8,24},{16,0},{24,8},{1,17},{9,25},{17,1},{25,9},{2,18},{10... | collective-permute-start | bytes 1572872 | tf_op jit(solution)/shard_map/ppermute | solution.py:198
  187.3 3.1 %collective-permute-start.9 = (bf16[512,512]{1,0:T(8,128)(2,1)}, bf16[512,512]{1,0:T(8,128)(2,1)}, u32[]{:S(2)}, u32[]{:S(2)}) collective-permute-start(bf16[512,512]{1,0:T(8,128)(2,1)} %slice.79), channel_id=1, source_target_pairs={{0,24},{8,0},{16,8},{24,16},{1,25},{9,1},{17,9},{25,17},{2,26},{10... | collective-permute-start | bytes 1572872 | tf_op jit(solution)/shard_map/ppermute | solution.py:198
  193.0 11.5 %first_rows.1.first_ref = bf16[512,2048]{1,0:T(8,128)(2,1)} custom-call(s32[2]{0:T(128)} %pad_add_fusion.place_ref, bf16[8,512,128]{2,1,0:T(8,128)(2,1)} %copy-done.3, bf16[8,512,256]{2,1,0:T(8,128)(2,1)} %copy-done, f32[1,2048]{1,0:T(1,128)} %bitcast.77, bf16[16,32,512]{2,1,0:T(8,128)(2,1)} %bitcast.24.rest_0_, bf16[16,32,512]{2,1,0:T(8,128)(2,1)} %bitcast.25.rest_1_, ...), custom_call_target="tpu_custom_call" | custom-call | flops 2147483648 | bytes 6291456 | tf_op jit(solution)/shard_map/first_rows/pallas_call | solution.py:104
  204.6 4.6 %collective-permute-done.7 = bf16[512,512]{1,0:T(8,128)(2,1)S(1)} collective-permute-done((bf16[512,512]{1,0:T(8,128)(2,1)}, bf16[512,512]{1,0:T(8,128)(2,1)S(1)}, u32[]{:S(2)}, u32[]{:S(2)}) %collective-permute-start.7) | collective-permute-done | bytes 524320 | tf_op jit(solution)/shard_map/ppermute | solution.py:198
  209.2 2.9 %collective-permute-done.9 = bf16[512,512]{1,0:T(8,128)(2,1)} collective-permute-done((bf16[512,512]{1,0:T(8,128)(2,1)}, bf16[512,512]{1,0:T(8,128)(2,1)}, u32[]{:S(2)}, u32[]{:S(2)}) %collective-permute-start.9) | collective-permute-done | bytes 524320 | tf_op jit(solution)/shard_map/ppermute | solution.py:198
  212.1 14.4 %mixer.1 = (f32[256,2048]{1,0:T(8,128)}, bf16[256,2048]{1,0:T(8,128)(2,1)}) custom-call(s32[2]{0:T(128)} %pad_add_fusion.place_ref, bf16[512,2048]{1,0:T(8,128)(2,1)} %first_rows.1.first_ref, bf16[2048,1600]{1,0:T(8,128)(2,1)} %all-gather.2.cloned.1.call-done.big_ref, bf16[16,32,512]{2,1,0:T(8,128)(2,1)} %bitcast.32.rest_0_, bf16[16,32,512]{2,1,0:T(8,128)(2,1)} %bitcast.86, ...), custom_call_target="tpu_custom_call" | custom-call | flops 4429185024 | bytes 12582912 | tf_op jit(solution)/shard_map/mixer/pallas_call | solution.py:180
  226.5 3.0 %collective-permute-start.10 = (bf16[256,2048]{1,0:T(8,128)(2,1)}, bf16[256,2048]{1,0:T(8,128)(2,1)S(1)}, u32[]{:S(2)}, u32[]{:S(2)}) collective-permute-start(bf16[256,2048]{1,0:T(8,128)(2,1)} %get-tuple-element.8), channel_id=1, source_target_pairs={{0,1},{1,0},{2,3},{3,2},{4,5},{5,4},{6,7},{7,6},{8,9},{9,8},{10,11... | collective-permute-start | bytes 3145736 | tf_op jit(solution)/shard_map/ppermute | solution.py:25
  229.6 2.5 collective-permute-done.10
  232.1 2.9 %add_convert_fusion = bf16[256,2048]{1,0:T(8,128)(2,1)} fusion(f32[256,2048]{1,0:T(8,128)} %get-tuple-element.7, bf16[256,2048]{1,0:T(8,128)(2,1)S(1)} %collective-permute-done.10), kind=kLoop, calls=%fused_computation | loop fusion | flops 1572864 | bytes 4194304 | tf_op jit(solution)/shard_map/convert_element_type | solution.py:37
  235.0 3.5 %all-to-all-start.4 = ((bf16[4,64,2048]{2,1,0:T(8,128)(2,1)}), bf16[4,64,2048]{2,1,0:T(8,128)(2,1)S(1)}, u32[]{:S(2)}, u32[]{:S(2)}) async-start(bf16[4,64,2048]{2,1,0:T(8,128)(2,1)} %bitcast.36), calls=%async_computation.4 | async-start | bytes 2097152 | tf_op jit(solution)/shard_map/all_to_all | solution.py:38
  240.2 13.1 %all-to-all-done.4.pieces_ref = bf16[4,64,2048]{2,1,0:T(8,128)(2,1)S(1)} async-done(((bf16[4,64,2048]{2,1,0:T(8,128)(2,1)}), bf16[4,64,2048]{2,1,0:T(8,128)(2,1)S(1)}, u32[]{:S(2)}, u32[]{:S(2)}) %all-to-all-start.4) | async-done | bytes 1048608 | tf_op jit(solution)/shard_map/all_to_all | solution.py:38
  256.7 11.0 %all_to_all.31 = bf16[8,64,256]{2,1,0:T(8,128)(2,1)S(1)} all-to-all(bf16[8,64,256]{2,1,0:T(8,128)(2,1)} %last_norm.1), channel_id=1, replica_groups=mesh['z'=16,'y'=4,'x'=4,'c'=2] {'x','c'}, dimensions={0} | all-to-all | bytes 524288 | tf_op jit(solution)/shard_map/all_to_all | solution.py:277
  (84 shorter events, 37.3 us)
Async XLA Ops:
  6.5 205.5 %all-gather.2.cloned.1.call-start = ((), (), s32[]{:S(2)}) async-start(), calls=%async_computation.6 | async-start | bytes 7241728 | tf_op jit(solution)/shard_map/all_gather | solution.py:228
  66.2 12.3 %copy-start.9 = (bf16[512,256]{1,0:T(8,128)(2,1)S(1)}, bf16[512,256]{1,0:T(8,128)(2,1)}, u32[]{:S(2)}) copy-start(bf16[512,256]{1,0:T(8,128)(2,1)} %param.12) | copy-start | bytes 786436
  80.0 16.0 %copy-start.10 = (f32[256]{0:T(256)S(1)}, f32[256]{0:T(256)}, u32[]{:S(2)}) copy-start(f32[256]{0:T(256)} %param.23) | copy-start | bytes 3076
  80.0 16.0 %copy-start.11 = (f32[256]{0:T(256)S(1)}, f32[256]{0:T(256)}, u32[]{:S(2)}) copy-start(f32[256]{0:T(256)} %param.19) | copy-start | bytes 3076
  80.0 42.2 %all-to-all-start.1 = ((bf16[8,512,256]{2,1,0:T(8,128)(2,1)}), bf16[8,512,256]{2,1,0:T(8,128)(2,1)S(1)}, u32[]{:S(2)}, u32[]{:S(2)}) async-start(bf16[8,512,256]{2,1,0:T(8,128)(2,1)} %broadcast_in_dim.21), calls=%async_computation.1 | async-start | bytes 4194304 | tf_op jit(solution)/shard_map/all_to_all | solution.py:21
  126.5 6.1 %slice-start = ((bf16[512,896]{1,0:T(8,128)(2,1)}), bf16[512,128]{1,0:T(8,128)(2,1)S(1)}, s32[]{:S(2)}) async-start(bf16[512,896]{1,0:T(8,128)(2,1)} %copy-done.4), calls=%async_computation.7 | async-start | bytes 262144 | tf_op jit(solution)/shard_map/slice | solution.py:236
  126.5 27.9 %copy-start.12 = (f32[128]{0:T(128)S(1)}, f32[128]{0:T(128)}, u32[]{:S(2)}) copy-start(f32[128]{0:T(128)} %param.15) | copy-start | bytes 1540
  126.5 28.1 %copy-start.13 = (f32[1,128]{1,0:T(1,128)S(1)}, f32[1,128]{1,0:T(1,128)}, u32[]{:S(2)}) copy-start(f32[1,128]{1,0:T(1,128)} %param.17) | copy-start | bytes 1540
  127.8 25.7 %all-to-all-start.2 = ((f32[8,3,512]{2,1,0:T(4,128)}), f32[8,3,512]{2,1,0:T(4,128)}, u32[]{:S(2)}, u32[]{:S(2)}) async-start(f32[8,3,512]{2,1,0:T(4,128)} %broadcast_in_dim.22), calls=%async_computation.2 | async-start | bytes 131072 | tf_op jit(solution)/shard_map/all_to_all | solution.py:21
  145.0 23.3 %collective-permute-start = (bf16[512,512]{1,0:T(8,128)(2,1)}, bf16[512,512]{1,0:T(8,128)(2,1)}, u32[]{:S(2)}, u32[]{:S(2)}) collective-permute-start(bf16[512,512]{1,0:T(8,128)(2,1)} %all_gather.13), channel_id=1, source_target_pairs={{0,8},{8,16},{16,24},{24,0},{1,9},{9,17},{17,25},{25,1},{2,10},{10... | collective-permute-start | bytes 1572872 | tf_op jit(solution)/shard_map/ppermute | solution.py:198
  147.2 28.7 %collective-permute-start.1 = (bf16[512,512]{1,0:T(8,128)(2,1)}, bf16[512,512]{1,0:T(8,128)(2,1)}, u32[]{:S(2)}, u32[]{:S(2)}) collective-permute-start(bf16[512,512]{1,0:T(8,128)(2,1)} %all_gather.13), channel_id=1, source_target_pairs={{0,16},{8,24},{16,0},{24,8},{1,17},{9,25},{17,1},{25,9},{2,18},{10... | collective-permute-start | bytes 1572872 | tf_op jit(solution)/shard_map/ppermute | solution.py:198
  150.9 26.9 %collective-permute-start.2 = (bf16[512,512]{1,0:T(8,128)(2,1)}, bf16[512,512]{1,0:T(8,128)(2,1)}, u32[]{:S(2)}, u32[]{:S(2)}) collective-permute-start(bf16[512,512]{1,0:T(8,128)(2,1)} %all_gather.13), channel_id=1, source_target_pairs={{0,24},{8,0},{16,8},{24,16},{1,25},{9,1},{17,9},{25,17},{2,26},{10... | collective-permute-start | bytes 1572872 | tf_op jit(solution)/shard_map/ppermute | solution.py:198
  157.9 22.4 %copy-start.5 = (bf16[512,896]{1,0:T(8,128)(2,1)S(1)}, bf16[512,896]{1,0:T(8,128)(2,1)}, u32[]{:S(2)}) copy-start(bf16[512,896]{1,0:T(8,128)(2,1)} %copy-done.4) | copy-start | bytes 2752516
  159.1 32.8 %all-to-all-start.3 = ((bf16[8,512,128]{2,1,0:T(8,128)(2,1)}), bf16[8,512,128]{2,1,0:T(8,128)(2,1)S(1)}, u32[]{:S(2)}, u32[]{:S(2)}) async-start(bf16[8,512,128]{2,1,0:T(8,128)(2,1)} %broadcast_in_dim.24), calls=%async_computation.3 | async-start | bytes 2097152 | tf_op jit(solution)/shard_map/all_to_all | solution.py:21
  166.4 17.2 %collective-permute-start.3 = (bf16[512,512]{1,0:T(8,128)(2,1)}, bf16[512,512]{1,0:T(8,128)(2,1)S(1)}, u32[]{:S(2)}, u32[]{:S(2)}) collective-permute-start(bf16[512,512]{1,0:T(8,128)(2,1)} %all_gather.13), channel_id=1, source_target_pairs={{0,1},{1,0},{2,3},{3,2},{4,5},{5,4},{6,7},{7,6},{8,9},{9,8},{10,11... | collective-permute-start | bytes 1572872 | tf_op jit(solution)/shard_map/ppermute | solution.py:25
  168.3 18.9 %collective-permute-start.4 = (bf16[512,512]{1,0:T(8,128)(2,1)}, bf16[512,512]{1,0:T(8,128)(2,1)S(1)}, u32[]{:S(2)}, u32[]{:S(2)}) collective-permute-start(bf16[512,512]{1,0:T(8,128)(2,1)} %collective-permute-done), channel_id=1, source_target_pairs={{0,1},{1,0},{2,3},{3,2},{4,5},{5,4},{6,7},{7,6},{8,9},{9,8},{10,11... | collective-permute-start | bytes 1572872 | tf_op jit(solution)/shard_map/ppermute | solution.py:25
  175.9 15.9 %collective-permute-start.5 = (bf16[512,512]{1,0:T(8,128)(2,1)}, bf16[512,512]{1,0:T(8,128)(2,1)S(1)}, u32[]{:S(2)}, u32[]{:S(2)}) collective-permute-start(bf16[512,512]{1,0:T(8,128)(2,1)} %collective-permute-done.1), channel_id=1, source_target_pairs={{0,1},{1,0},{2,3},{3,2},{4,5},{5,4},{6,7},{7,6},{8,9},{9,8},{10,11... | collective-permute-start | bytes 1572872 | tf_op jit(solution)/shard_map/ppermute | solution.py:25
  177.9 14.0 %collective-permute-start.6 = (bf16[512,512]{1,0:T(8,128)(2,1)}, bf16[512,512]{1,0:T(8,128)(2,1)}, u32[]{:S(2)}, u32[]{:S(2)}) collective-permute-start(bf16[512,512]{1,0:T(8,128)(2,1)} %collective-permute-done.2), channel_id=1, source_target_pairs={{0,1},{1,0},{2,3},{3,2},{4,5},{5,4},{6,7},{7,6},{8,9},{9,8},{10,11... | collective-permute-start | bytes 1572872 | tf_op jit(solution)/shard_map/ppermute | solution.py:25
  181.2 28.0 %collective-permute-start.7 = (bf16[512,512]{1,0:T(8,128)(2,1)}, bf16[512,512]{1,0:T(8,128)(2,1)S(1)}, u32[]{:S(2)}, u32[]{:S(2)}) collective-permute-start(bf16[512,512]{1,0:T(8,128)(2,1)} %slice.79), channel_id=1, source_target_pairs={{0,8},{8,16},{16,24},{24,0},{1,9},{9,17},{17,25},{25,1},{2,10},{10... | collective-permute-start | bytes 1572872 | tf_op jit(solution)/shard_map/ppermute | solution.py:198
  183.6 8.3 %copy-start.6 = (bf16[512,512]{1,0:T(8,128)(2,1)}, bf16[512,512]{1,0:T(8,128)(2,1)S(1)}, u32[]{:S(2)}) copy-start(bf16[512,512]{1,0:T(8,128)(2,1)S(1)} %collective-permute-done.3) | copy-start | bytes 1572868
  183.6 25.5 %collective-permute-start.8 = (bf16[512,512]{1,0:T(8,128)(2,1)}, bf16[512,512]{1,0:T(8,128)(2,1)}, u32[]{:S(2)}, u32[]{:S(2)}) collective-permute-start(bf16[512,512]{1,0:T(8,128)(2,1)} %slice.79), channel_id=1, source_target_pairs={{0,16},{8,24},{16,0},{24,8},{1,17},{9,25},{17,1},{25,9},{2,18},{10... | collective-permute-start | bytes 1572872 | tf_op jit(solution)/shard_map/ppermute | solution.py:198
  187.3 24.8 %collective-permute-start.9 = (bf16[512,512]{1,0:T(8,128)(2,1)}, bf16[512,512]{1,0:T(8,128)(2,1)}, u32[]{:S(2)}, u32[]{:S(2)}) collective-permute-start(bf16[512,512]{1,0:T(8,128)(2,1)} %slice.79), channel_id=1, source_target_pairs={{0,24},{8,0},{16,8},{24,16},{1,25},{9,1},{17,9},{25,17},{2,26},{10... | collective-permute-start | bytes 1572872 | tf_op jit(solution)/shard_map/ppermute | solution.py:198
  226.5 5.5 %collective-permute-start.10 = (bf16[256,2048]{1,0:T(8,128)(2,1)}, bf16[256,2048]{1,0:T(8,128)(2,1)S(1)}, u32[]{:S(2)}, u32[]{:S(2)}) collective-permute-start(bf16[256,2048]{1,0:T(8,128)(2,1)} %get-tuple-element.8), channel_id=1, source_target_pairs={{0,1},{1,0},{2,3},{3,2},{4,5},{5,4},{6,7},{7,6},{8,9},{9,8},{10,11... | collective-permute-start | bytes 3145736 | tf_op jit(solution)/shard_map/ppermute | solution.py:25
  235.0 18.3 %all-to-all-start.4 = ((bf16[4,64,2048]{2,1,0:T(8,128)(2,1)}), bf16[4,64,2048]{2,1,0:T(8,128)(2,1)S(1)}, u32[]{:S(2)}, u32[]{:S(2)}) async-start(bf16[4,64,2048]{2,1,0:T(8,128)(2,1)} %bitcast.36), calls=%async_computation.4 | async-start | bytes 2097152 | tf_op jit(solution)/shard_map/all_to_all | solution.py:38
  (8 other events, 15.8 us)
Sparse Core Ops, SparseCore 0:
  22.6 101.5 all-gather.1

commit v4 on v3

--- a/solution.py
+++ b/solution.py
@@ -73,124 +73,145 @@
     depth = 32
     zs = near[0].shape[0] // depth
     wide = near[0].shape[1]
-    step = 128
+    deep = zs // parts
+    ahead = 3
 
     def body(place_ref, gated_ref, blocks_ref, gain_ref, *rest):
-        pieces, out_ref, weights, left, sems = rest[: 2 * peers], rest[-4], rest[-3], rest[-2], rest[-1]
+        pieces = rest[: 2 * peers]
+        out_ref, weights, left, base, vals, left_sems, sems = rest[2 * peers :]
         core = place_ref[0]
         y = place_ref[1]
+        first = []
+        for k in range(parts):
+            at = pl.ds((k % cores * chips + k // cores) * channels, channels)
+            first.append(pltpu.make_async_copy(gated_ref.at[k], left.at[:, at], left_sems.at[k]))
+            first[k].start()
         copies = []
-        for n in range(2 * peers):
-            which = core if n < peers else 1 - core
-            at = lax.rem(y + 2 * peers - n, peers)
-            copies.append(pltpu.make_async_copy(pieces[n], weights.at[which, :, at], sems.at[n]))
-        for c in copies:
-            c.start()
-        for k in range(parts):
-            at = (k % cores * chips + k // cores) * channels
-            left[:, at : at + channels] = gated_ref[k]
-        for c in copies:
+        for j in range(parts):
+            at_z = pl.ds(j * deep, deep)
+            some = [pltpu.make_async_copy(blocks_ref.at[j], base.at[j], sems.at[j, 2 * peers])]
+            for n in range(2 * peers):
+                which = core if n < peers else 1 - core
+                at_y = lax.rem(y + 2 * peers - n, peers)
+                some.append(pltpu.make_async_copy(pieces[n].at[at_z], weights.at[which, at_z, at_y], sems.at[j, n]))
+            copies.append(some)
+        for some in copies[:ahead]:
+            for c in some:
+                c.start()
+        for c in first:
             c.wait()
-        for r in range(0, rows, step):
-            mix = jnp.zeros((step, width), F32)
+        total = jnp.zeros((rows, 1), F32)
+        squares = jnp.zeros((rows, 1), F32)
+        for j in range(parts):
+            for c in copies[j]:
+                c.wait()
+            if j + ahead < parts:
+                for c in copies[j + ahead]:
+                    c.start()
+            mix = jnp.zeros((rows, feats), F32)
             for k in range(cores):
-                right = weights[k].reshape(width, wide)
-                mix += lax.dot_general(left[r : r + step, k * wide : (k + 1) * wide], right, ACROSS, preferred_element_type=F32)
-            base = jnp.concatenate([blocks_ref[k, r : r + step] for k in range(parts)], axis=1)
-            vals = ALPHA * base.astype(F32) + mix.astype(BF16).astype(F32)
-            out_ref[r : r + step] = row_norm(vals, gain_ref[...]).astype(BF16)
+                right = weights[k, j * deep : (j + 1) * deep].reshape(feats, wide)
+                mix += lax.dot_general(left[:, k * wide : (k + 1) * wide], right, ACROSS, preferred_element_type=F32)
+            these = ALPHA * base[j].astype(F32) + mix.astype(BF16).astype(F32)
+            vals[j] = these
+            total += jnp.sum(these, axis=1, keepdims=True)
+            squares += jnp.sum(these * these, axis=1, keepdims=True)
+        mean = total / width
+        scale = lax.rsqrt(squares / width - mean * mean + EPS)
+        for j in range(parts):
+            at = slice(j * feats, (j + 1) * feats)
+            out_ref[:, at] = ((vals[j] - mean) * scale * gain_ref[:, at]).astype(BF16)
 
     given = [p.reshape(zs, depth, wide) for p in (*near, *far)]
+    anywhere = pl.BlockSpec(memory_space=pl.ANY)
     return pl.pallas_call(
         body,
         out_shape=jax.ShapeDtypeStruct((rows, width), BF16),
-        in_specs=[pl.BlockSpec(memory_space=pltpu.SMEM)] + [whole_vmem()] * 3 + [pl.BlockSpec(memory_space=pl.ANY)] * len(given),
+        in_specs=[pl.BlockSpec(memory_space=pltpu.SMEM), anywhere, anywhere, whole_vmem()] + [anywhere] * len(given),
         out_specs=whole_vmem(),
         scratch_shapes=[
             pltpu.VMEM((cores, zs, peers, depth, wide), BF16),
             pltpu.VMEM((rows, parts * channels), BF16),
-            pltpu.SemaphoreType.DMA((len(given),)),
+            pltpu.VMEM((parts, rows, feats), BF16),
+            pltpu.VMEM((parts, rows, feats), F32),
+            pltpu.SemaphoreType.DMA((parts,)),
+            pltpu.SemaphoreType.DMA((parts, 2 * peers + 1)),
         ],
-        cost_estimate=pl.CostEstimate(flops=2 * rows * width * parts * channels, bytes_accessed=6 << 20, transcendentals=rows),
+        cost_estimate=pl.CostEstimate(flops=2 * rows * width * parts * channels, bytes_accessed=9 << 20, transcendentals=rows),
         name="first_rows",
     )(place, gated, blocks, gain.reshape(1, width), *given)
 
 
-def packed_weights(gate, up, down):
+def packed_ffw(gate, up, down):
     cut = gate.shape[1] // 128 * 128
-    low = cut - 128
-    down = down.T
-    big = jnp.concatenate([gate[:, :cut], up[:, :cut], gate[:, cut:], up[:, cut:], down[:, low:]], axis=1)
-    return big, down[:, :low]
-
-
-def mixer(place, first, big, downs, ff):
+    return jnp.concatenate([gate[:, :cut], up[:, :cut], gate[:, cut:], up[:, cut:], down.T], axis=1)
+
+
+def mixer(place, first, ffw, ff):
     rows, width = first.shape
     half = rows // 2
     cut = ff // 128 * 128
     tail = ff - cut
-    low = cut - 128
-    peers = len(downs)
-    depth = 32
-    zs = width // peers // depth
-    edges = [0, 384, 768, 1152, big.shape[1]]
-    chunks = len(edges) - 1
-
-    def body(place_ref, first_ref, big_ref, *rest):
-        pieces = rest[:peers]
-        keep_ref, give_ref = rest[peers : peers + 2]
-        weights = rest[peers + 2 : -3]
-        down, acc, sems = rest[-3:]
+    edges = [0, 384, 768, 1152, 2 * ff, 3 * ff]
+    spans = [e - b for b, e in zip(edges, edges[1:])]
+    chunks = len(spans)
+    ahead = 2
+    step = 256
+
+    def body(place_ref, first_ref, ffw_ref, keep_ref, give_ref, *rest):
+        weights, left, acc, left_sem, sems = rest[:chunks], rest[-4], rest[-3], rest[-2], rest[-1]
         core = place_ref[0]
-        y = place_ref[1]
         copies = []
         for n in range(chunks):
-            at = pl.ds(edges[n], edges[n + 1] - edges[n])
-            copies.append(pltpu.make_async_copy(big_ref.at[:, at], weights[n], sems.at[n]))
-        for n in range(peers):
-            at = lax.rem(y + peers - n, peers)
-            copies.append(pltpu.make_async_copy(pieces[n], down.at[:, at], sems.at[chunks + n]))
-        for c in copies:
+            at = pl.ds(edges[n], spans[n])
+            copies.append(pltpu.make_async_copy(ffw_ref.at[:, at], weights[n], sems.at[n]))
+        lead = pltpu.make_async_copy(first_ref, left, left_sem.at[0])
+        lead.start()
+        for c in copies[:ahead]:
             c.start()
-        for n in range(chunks):
+        lead.wait()
+        for n in range(chunks - 1):
             copies[n].wait()
-            begin, count = edges[n], min(edges[n + 1], 2 * ff) - edges[n]
-            acc[:, begin : begin + count] = jnp.dot(first_ref[...], weights[n][:, :count], preferred_element_type=F32)
-        for c in copies[chunks:]:
-            c.wait()
+            if n + ahead < chunks:
+                copies[n + ahead].start()
+            acc[:, edges[n] : edges[n + 1]] = jnp.dot(left[...], weights[n][...], preferred_element_type=F32)
         gate = acc[:, :cut]
         main = (gate * lax.logistic(gate) * acc[:, cut : 2 * cut]).astype(BF16)
         last = acc[:, 2 * cut :]
         ends = (last[:, :tail] * lax.logistic(last[:, :tail]) * last[:, tail:]).astype(BF16)
-        rest = jnp.concatenate([main[:, low:], ends], axis=1)
-        acc_out = lax.dot_general(main[:, :low], down[...].reshape(width, low), ACROSS, preferred_element_type=F32)
-        acc_out += lax.dot_general(rest, weights[-1][:, 2 * ff - edges[-2] :], ACROSS, preferred_element_type=F32)
+        hidden = jnp.concatenate([main, ends], axis=1)
+        copies[-1].wait()
+
+        def out(keep_at, give_at):
+            for b in range(0, width, step):
+                done = lax.dot_general(hidden, weights[-1][b : b + step], ACROSS, preferred_element_type=F32)
+                keep_ref[:, b : b + step] = done[keep_at : keep_at + half]
+                give_ref[:, b : b + step] = done[give_at : give_at + half].astype(BF16)
 
         @pl.when(core == 0)
         def _():
-            keep_ref[...] = acc_out[:half]
-            give_ref[...] = acc_out[half:].astype(BF16)
+            out(0, half)
 
         @pl.when(core == 1)
         def _():
-            keep_ref[...] = acc_out[half:]
-            give_ref[...] = acc_out[:half].astype(BF16)
-
-    given = [p.reshape(zs, depth, p.shape[1]) for p in downs]
+            out(half, 0)
+
+    anywhere = pl.BlockSpec(memory_space=pl.ANY)
     return pl.pallas_call(
         body,
         out_shape=(jax.ShapeDtypeStruct((half, width), F32), jax.ShapeDtypeStruct((half, width), BF16)),
-        in_specs=[pl.BlockSpec(memory_space=pltpu.SMEM), whole_vmem()] + [pl.BlockSpec(memory_space=pl.ANY)] * (1 + peers),
+        in_specs=[pl.BlockSpec(memory_space=pltpu.SMEM), anywhere, anywhere],
         out_specs=(whole_vmem(), whole_vmem()),
         scratch_shapes=[
-            *(pltpu.VMEM((width, edges[n + 1] - edges[n]), BF16) for n in range(chunks)),
-            pltpu.VMEM((zs, peers, depth, low), BF16),
+            *(pltpu.VMEM((width, n), BF16) for n in spans),
+            pltpu.VMEM((rows, width), BF16),
             pltpu.VMEM((rows, 2 * ff), F32),
-            pltpu.SemaphoreType.DMA((chunks + peers,)),
+            pltpu.SemaphoreType.DMA((1,)),
+            pltpu.SemaphoreType.DMA((chunks,)),
         ],
-        cost_estimate=pl.CostEstimate(flops=6 * rows * width * ff, bytes_accessed=12 << 20, transcendentals=rows * ff),
+        cost_estimate=pl.CostEstimate(flops=6 * rows * width * ff, bytes_accessed=14 << 20, transcendentals=rows * ff),
         name="mixer",
-    )(place, first, big, *given)
+    )(place, first, ffw)
 
 
 def from_each(value, axis):
@@ -223,20 +244,18 @@
 
     blocks = sent_to_all(tokens, TP)
 
-    big, rest = packed_weights(gate_weight, up_weight, down_weight)
-    big = lax.all_gather(big, "y", axis=0, tiled=True)
-    big = lax.all_gather(big, "z", axis=0, tiled=True)
-
-    small = jnp.concatenate([u_weight, v_weight, out_weight.T, rest], axis=1)
+    ffw = lax.all_gather(packed_ffw(gate_weight, up_weight, down_weight), "y", axis=0, tiled=True)
+    ffw = lax.all_gather(ffw, "z", axis=0, tiled=True)
+
+    small = jnp.concatenate([u_weight, v_weight, out_weight.T], axis=1)
     depth = small.shape[0]
     small = lax.all_gather(small, "z", axis=0, tiled=True)
     gates = sent_to_all(small[:, : 2 * sg], "y")
     gates = gates.reshape(gates.shape[0], -1, depth, 2 * sg)
     gates = jnp.swapaxes(gates, 0, 1).reshape(width, 2 * sg)
-    out_x = lax.all_gather(small[:, 2 * sg : 3 * sg], "x", axis=1, tiled=True)
+    out_x = lax.all_gather(small[:, 2 * sg :], "x", axis=1, tiled=True)
     out_near = from_each(out_x, "y")
     out_far = [to_partner(piece) for piece in out_near]
-    downs = from_each(small[:, 3 * sg :], "y")
 
     whole = jnp.moveaxis(blocks, 0, 1).reshape(rows, width)
 
@@ -270,7 +289,7 @@
     chip = lax.axis_index("x")
     place = jnp.stack([core, lax.axis_index("y")]).astype(jnp.int32)
     first = first_rows(place, everyone, blocks, gain_1, out_near, out_far)
-    keep, give = mixer(place, first, big, downs, gate_weight.shape[1])
+    keep, give = mixer(place, first, ffw, gate_weight.shape[1])
     ffn = summed_rows(keep, give, chips)
     mine = lax.dynamic_slice_in_dim(first, (core * chips + chip) * own_rows, own_rows, 0)
     last = last_norm(ffn, mine, gain_2, parts)

time: 277 us -> 250 us (0.903)
  starting transfers between devices: 65.5 us -> 57.1 us
  blocking collectives: 89 us -> 81.4 us
  waiting for transfers between devices: 48.2 us -> 41.3 us
    ppermute x6 -> x3, starting transfers between devices: 17 us -> 8.41 us  [from_each(): lax.ppermute(value, axis, [(i, (i + k) % size) for i in range(size)])]
    all_gather x1, blocking collectives: 41.2 us -> 33 us  [on_device(): small = lax.all_gather(small, 'z', axis=0, tiled=True)]
    ppermute x6 -> x3, waiting for transfers between devices: 7.51 us -> 0.01 us  [from_each(): lax.ppermute(value, axis, [(i, (i + k) % size) for i in range(size)])]
  transfers between devices with their start and end apart: 16 -> 13, of which waited for: 5 -> 3; matrix products, arithmetic and copies ran while one was open for 7% -> 7% of each run, Pallas kernels for 4% -> 5%
where the time goes in v4:
time: 250 us; the launch traced here: 248 us
  blocking collectives  81.4 us (33%)
  starting transfers between devices  57.1 us (23%)
  waiting for transfers between devices  41.3 us (17%)
  Pallas kernels  26.4 us (11%)
  local copies, waits for them, and re-layouts  20.4 us (8%)
  between operations  13.8 us (6%)
  other arithmetic  5.3 us (2%)
  matrix products  2.73 us (1%)
    all_gather x1, blocking collectives, on_device(): small = lax.all_gather(small, 'z', axis=0, tiled=True)  33 us
    all_to_all x3, starting transfers between devices, sent_to_all(): return lax.all_to_all(copies, axis, split_axis=0, concat_axis=0, tiled=True)  28.8 us
    all_to_all x3, waiting for transfers between devices, sent_to_all(): return lax.all_to_all(copies, axis, split_axis=0, concat_axis=0, tiled=True)  25.1 us
    ppermute x5, starting transfers between devices, to_partner(): return lax.ppermute(value, 'c', [(0, 1), (1, 0)])  16.4 us
    all_to_all x1, waiting for transfers between devices, summed_rows(): return lax.all_to_all(pieces, 'x', 0, 0, tiled=True)  13.3 us
    all_gather x1, blocking collectives, on_device(): out_x = lax.all_gather(small[:, 2 * sg:], 'x', axis=1, tiled=True)  12.8 us
    all_gather x1, blocking collectives, on_device(): lax.all_gather(packed_ffw(gate_weight, up_weight, down_weight), 'y', axis...  12.7 us
    all_to_all x1, blocking collectives, sent_to_all(): return lax.all_to_all(copies, axis, split_axis=0, concat_axis=0, tiled=True)  12.2 us
  transfers between devices with their start and end apart: 13, of which 3 were waited for; matrix products, arithmetic and copies ran while one was open for 7% of the time, Pallas kernels for 5%

profile of v4, /device:TPU:1, one launch (start us, length us, event | category | flops | bytes accessed | tf_op | source)
XLA Modules:
  0.0 248.5 jit_solution(9853470454917153949)
XLA Ops:
  10.4 12.7 %all_gather.14 = bf16[128,2112]{1,0:T(8,128)(2,1)} all-gather(bf16[32,2112]{1,0:T(8,128)(2,1)S(1)} %concatenate.15), channel_id=1, replica_groups=mesh['z'=16,'y'=4,'x'=4,'c'=2] {'y'}, dimensions={0}, use_global_device_ids=true | all-gather | bytes 675840 | tf_op jit(solution)/shard_map/all_gather | solution.py:247
  23.8 33.0 %all_gather.12 = bf16[512,384]{1,0:T(8,128)(2,1)S(1)} all-gather(bf16[32,384]{1,0:T(8,128)(2,1)S(1)} %pad_maximum_fusion), channel_id=1, replica_groups=mesh['z'=16,'y'=4,'x'=4,'c'=2] {'z'}, dimensions={0}, use_global_device_ids=true | all-gather | bytes 417792 | tf_op jit(solution)/shard_map/all_gather | solution.py:252
  56.9 12.2 %all_to_all.30 = bf16[4,512,256]{2,1,0:T(8,128)(2,1)S(1)} all-to-all(bf16[4,512,256]{2,1,0:T(8,128)(2,1)S(1)} %broadcast_in_dim.20), channel_id=1, replica_groups=mesh['z'=16,'y'=4,'x'=4,'c'=2] {'y'}, dimensions={0} | all-to-all | bytes 2097152 | tf_op jit(solution)/shard_map/all_to_all | solution.py:21
  70.6 17.2 %all-to-all-start.1 = ((bf16[8,512,256]{2,1,0:T(8,128)(2,1)}), bf16[8,512,256]{2,1,0:T(8,128)(2,1)S(1)}, u32[]{:S(2)}, u32[]{:S(2)}) async-start(bf16[8,512,256]{2,1,0:T(8,128)(2,1)} %broadcast_in_dim.21), calls=%async_computation.1 | async-start | bytes 4194304 | tf_op jit(solution)/shard_map/all_to_all | solution.py:21
  88.9 25.1 %all-to-all-done.1.blocks_ref = bf16[8,512,256]{2,1,0:T(8,128)(2,1)S(1)} async-done(((bf16[8,512,256]{2,1,0:T(8,128)(2,1)}), bf16[8,512,256]{2,1,0:T(8,128)(2,1)S(1)}, u32[]{:S(2)}, u32[]{:S(2)}) %all-to-all-start.1) | async-done | bytes 2097184 | tf_op jit(solution)/shard_map/all_to_all | solution.py:21
  115.3 3.0 %copy.29 = bf16[512,8,256]{0,2,1:T(8,128)(2,1)S(1)} copy(bf16[512,8,256]{2,0,1:T(8,128)(2,1)} %bitcast.60) | data formatting | bytes 4194304 | tf_op jit(solution)/shard_map/transpose | solution.py:260
  119.6 4.8 %all-to-all-start.2 = ((f32[8,3,512]{2,1,0:T(4,128)}), f32[8,3,512]{2,1,0:T(4,128)}, u32[]{:S(2)}, u32[]{:S(2)}) async-start(f32[8,3,512]{2,1,0:T(4,128)} %broadcast_in_dim.22), calls=%async_computation.2 | async-start | bytes 131072 | tf_op jit(solution)/shard_map/all_to_all | solution.py:21
  124.4 12.8 %all_gather.13 = bf16[512,512]{1,0:T(8,128)(2,1)} all-gather(bf16[512,128]{1,0:T(8,128)(2,1)S(1)} %slice-done), channel_id=1, replica_groups=mesh['z'=16,'y'=4,'x'=4,'c'=2] {'x'}, dimensions={1}, use_global_device_ids=true | all-gather | bytes 655360 | tf_op jit(solution)/shard_map/all_gather | solution.py:256
  137.1 2.2 collective-permute-start
  139.3 3.7 %collective-permute-start.1 = (bf16[512,512]{1,0:T(8,128)(2,1)}, bf16[512,512]{1,0:T(8,128)(2,1)}, u32[]{:S(2)}, u32[]{:S(2)}) collective-permute-start(bf16[512,512]{1,0:T(8,128)(2,1)} %all_gather.13), channel_id=1, source_target_pairs={{0,16},{8,24},{16,0},{24,8},{1,17},{9,25},{17,1},{25,9},{2,18},{10... | collective-permute-start | bytes 1572872 | tf_op jit(solution)/shard_map/ppermute | solution.py:219
  143.0 2.5 %collective-permute-start.2 = (bf16[512,512]{1,0:T(8,128)(2,1)}, bf16[512,512]{1,0:T(8,128)(2,1)}, u32[]{:S(2)}, u32[]{:S(2)}) collective-permute-start(bf16[512,512]{1,0:T(8,128)(2,1)} %all_gather.13), channel_id=1, source_target_pairs={{0,24},{8,0},{16,8},{24,16},{1,25},{9,1},{17,9},{25,17},{2,26},{10... | collective-permute-start | bytes 1572872 | tf_op jit(solution)/shard_map/ppermute | solution.py:219
  151.2 6.9 %all-to-all-start.3 = ((bf16[8,512,128]{2,1,0:T(8,128)(2,1)}), bf16[8,512,128]{2,1,0:T(8,128)(2,1)S(1)}, u32[]{:S(2)}, u32[]{:S(2)}) async-start(bf16[8,512,128]{2,1,0:T(8,128)(2,1)} %broadcast_in_dim.24), calls=%async_computation.3 | async-start | bytes 2097152 | tf_op jit(solution)/shard_map/all_to_all | solution.py:21
  160.0 8.0 %collective-permute-start.4 = (bf16[512,512]{1,0:T(8,128)(2,1)}, bf16[512,512]{1,0:T(8,128)(2,1)S(1)}, u32[]{:S(2)}, u32[]{:S(2)}) collective-permute-start(bf16[512,512]{1,0:T(8,128)(2,1)} %collective-permute-done), channel_id=1, source_target_pairs={{0,1},{1,0},{2,3},{3,2},{4,5},{5,4},{6,7},{7,6},{8,9},{9,8},{10,11... | collective-permute-start | bytes 1572872 | tf_op jit(solution)/shard_map/ppermute | solution.py:25
  168.0 1.9 collective-permute-start.5
  170.0 2.6 %collective-permute-start.6 = (bf16[512,512]{1,0:T(8,128)(2,1)}, bf16[512,512]{1,0:T(8,128)(2,1)S(1)}, u32[]{:S(2)}, u32[]{:S(2)}) collective-permute-start(bf16[512,512]{1,0:T(8,128)(2,1)} %collective-permute-done.2), channel_id=1, source_target_pairs={{0,1},{1,0},{2,3},{3,2},{4,5},{5,4},{6,7},{7,6},{8,9},{9,8},{10,11... | collective-permute-start | bytes 1572872 | tf_op jit(solution)/shard_map/ppermute | solution.py:25
  176.5 11.9 %first_rows.1.first_ref = bf16[512,2048]{1,0:T(8,128)(2,1)} custom-call(s32[2]{0:T(128)} %pad_add_fusion.place_ref, bf16[8,512,128]{2,1,0:T(8,128)(2,1)} %copy-done.3, bf16[8,512,256]{2,1,0:T(8,128)(2,1)} %copy-done, f32[1,2048]{1,0:T(1,128)} %bitcast.73, bf16[16,32,512]{2,1,0:T(8,128)(2,1)} %bitcast.23.rest_0_, bf16[16,32,512]{2,1,0:T(8,128)(2,1)} %bitcast.24.rest_1_, ...), custom_call_target="tpu_custom_call" | custom-call | flops 2147483648 | bytes 9437184 | tf_op jit(solution)/shard_map/first_rows/pallas_call | solution.py:127
  188.4 12.1 %mixer.1 = (f32[256,2048]{1,0:T(8,128)}, bf16[256,2048]{1,0:T(8,128)(2,1)}) custom-call(s32[2]{0:T(128)} %pad_add_fusion.place_ref, bf16[512,2048]{1,0:T(8,128)(2,1)} %first_rows.1.first_ref, bf16[2048,2112]{1,0:T(8,128)(2,1)} %all-gather.2.cloned.1.call-done.ffw_ref), custom_call_target="tpu_custom_call" | custom-call | flops 4429185024 | bytes 14680064 | tf_op jit(solution)/shard_map/mixer/pallas_call | solution.py:200
  200.5 1.9 collective-permute-start.7
  202.4 2.8 %collective-permute-done.7 = bf16[256,2048]{1,0:T(8,128)(2,1)S(1)} collective-permute-done((bf16[256,2048]{1,0:T(8,128)(2,1)}, bf16[256,2048]{1,0:T(8,128)(2,1)S(1)}, u32[]{:S(2)}, u32[]{:S(2)}) %collective-permute-start.7) | collective-permute-done | bytes 1048608 | tf_op jit(solution)/shard_map/ppermute | solution.py:25
  205.3 2.9 %add_convert_fusion = bf16[256,2048]{1,0:T(8,128)(2,1)} fusion(f32[256,2048]{1,0:T(8,128)} %get-tuple-element.7, bf16[256,2048]{1,0:T(8,128)(2,1)S(1)} %collective-permute-done.7), kind=kLoop, calls=%fused_computation | loop fusion | flops 1572864 | bytes 4194304 | tf_op jit(solution)/shard_map/convert_element_type | solution.py:37
  208.2 3.5 %all-to-all-start.4 = ((bf16[4,64,2048]{2,1,0:T(8,128)(2,1)}), bf16[4,64,2048]{2,1,0:T(8,128)(2,1)S(1)}, u32[]{:S(2)}, u32[]{:S(2)}) async-start(bf16[4,64,2048]{2,1,0:T(8,128)(2,1)} %bitcast.32), calls=%async_computation.4 | async-start | bytes 2097152 | tf_op jit(solution)/shard_map/all_to_all | solution.py:38
  213.4 13.3 %all-to-all-done.4.pieces_ref = bf16[4,64,2048]{2,1,0:T(8,128)(2,1)S(1)} async-done(((bf16[4,64,2048]{2,1,0:T(8,128)(2,1)}), bf16[4,64,2048]{2,1,0:T(8,128)(2,1)S(1)}, u32[]{:S(2)}, u32[]{:S(2)}) %all-to-all-start.4) | async-done | bytes 1048608 | tf_op jit(solution)/shard_map/all_to_all | solution.py:38
  227.7 2.4 last_norm.1
  230.1 10.8 %all_to_all.31 = bf16[8,64,256]{2,1,0:T(8,128)(2,1)S(1)} all-to-all(bf16[8,64,256]{2,1,0:T(8,128)(2,1)} %last_norm.1), channel_id=1, replica_groups=mesh['z'=16,'y'=4,'x'=4,'c'=2] {'x','c'}, dimensions={0} | all-to-all | bytes 524288 | tf_op jit(solution)/shard_map/all_to_all | solution.py:296
  (73 shorter events, 24.5 us)
Async XLA Ops:
  6.5 181.9 %all-gather.2.cloned.1.call-start = ((), (), s32[]{:S(2)}) async-start(), calls=%async_computation.6 | async-start | bytes 9469952 | tf_op jit(solution)/shard_map/all_gather | solution.py:248
  23.8 45.3 %copy-start.9 = (bf16[512,256]{1,0:T(8,128)(2,1)S(1)}, bf16[512,256]{1,0:T(8,128)(2,1)}, u32[]{:S(2)}) copy-start(bf16[512,256]{1,0:T(8,128)(2,1)} %param.12) | copy-start | bytes 786436
  56.8 31.0 %copy-start.4 = (bf16[512,384]{1,0:T(8,128)(2,1)}, bf16[512,384]{1,0:T(8,128)(2,1)S(1)}, u32[]{:S(2)}) copy-start(bf16[512,384]{1,0:T(8,128)(2,1)S(1)} %all_gather.12) | copy-start | bytes 1179652
  70.6 17.2 %copy-start.10 = (f32[256]{0:T(256)S(1)}, f32[256]{0:T(256)}, u32[]{:S(2)}) copy-start(f32[256]{0:T(256)} %param.23) | copy-start | bytes 3076
  70.6 17.2 %copy-start.11 = (f32[256]{0:T(256)S(1)}, f32[256]{0:T(256)}, u32[]{:S(2)}) copy-start(f32[256]{0:T(256)} %param.19) | copy-start | bytes 3076
  70.6 43.4 %all-to-all-start.1 = ((bf16[8,512,256]{2,1,0:T(8,128)(2,1)}), bf16[8,512,256]{2,1,0:T(8,128)(2,1)S(1)}, u32[]{:S(2)}, u32[]{:S(2)}) async-start(bf16[8,512,256]{2,1,0:T(8,128)(2,1)} %broadcast_in_dim.21), calls=%async_computation.1 | async-start | bytes 4194304 | tf_op jit(solution)/shard_map/all_to_all | solution.py:21
  114.0 1.3 copy-start
  115.3 3.0 %copy-start.2 = (bf16[16,4,32,256]{3,2,1,0:T(8,128)(2,1)S(1)}, bf16[16,4,32,256]{3,2,1,0:T(8,128)(2,1)}, u32[]{:S(2)}) copy-start(bf16[16,4,32,256]{3,2,1,0:T(8,128)(2,1)} %copy.28) | copy-start | bytes 3145732
  118.3 6.1 %slice-start = ((bf16[512,384]{1,0:T(8,128)(2,1)}), bf16[512,128]{1,0:T(8,128)(2,1)S(1)}, s32[]{:S(2)}) async-start(bf16[512,384]{1,0:T(8,128)(2,1)} %copy-done.4), calls=%async_computation.7 | async-start | bytes 262144 | tf_op jit(solution)/shard_map/slice | solution.py:256
  118.3 28.2 %copy-start.12 = (f32[128]{0:T(128)S(1)}, f32[128]{0:T(128)}, u32[]{:S(2)}) copy-start(f32[128]{0:T(128)} %param.15) | copy-start | bytes 1540
  118.3 28.4 %copy-start.13 = (f32[1,128]{1,0:T(1,128)S(1)}, f32[1,128]{1,0:T(1,128)}, u32[]{:S(2)}) copy-start(f32[1,128]{1,0:T(1,128)} %param.17) | copy-start | bytes 1540
  119.6 26.0 %all-to-all-start.2 = ((f32[8,3,512]{2,1,0:T(4,128)}), f32[8,3,512]{2,1,0:T(4,128)}, u32[]{:S(2)}, u32[]{:S(2)}) async-start(f32[8,3,512]{2,1,0:T(4,128)} %broadcast_in_dim.22), calls=%async_computation.2 | async-start | bytes 131072 | tf_op jit(solution)/shard_map/all_to_all | solution.py:21
  137.1 22.8 %collective-permute-start = (bf16[512,512]{1,0:T(8,128)(2,1)}, bf16[512,512]{1,0:T(8,128)(2,1)}, u32[]{:S(2)}, u32[]{:S(2)}) collective-permute-start(bf16[512,512]{1,0:T(8,128)(2,1)} %all_gather.13), channel_id=1, source_target_pairs={{0,8},{8,16},{16,24},{24,0},{1,9},{9,17},{17,25},{25,1},{2,10},{10... | collective-permute-start | bytes 1572872 | tf_op jit(solution)/shard_map/ppermute | solution.py:219
  139.3 28.7 %collective-permute-start.1 = (bf16[512,512]{1,0:T(8,128)(2,1)}, bf16[512,512]{1,0:T(8,128)(2,1)}, u32[]{:S(2)}, u32[]{:S(2)}) collective-permute-start(bf16[512,512]{1,0:T(8,128)(2,1)} %all_gather.13), channel_id=1, source_target_pairs={{0,16},{8,24},{16,0},{24,8},{1,17},{9,25},{17,1},{25,9},{2,18},{10... | collective-permute-start | bytes 1572872 | tf_op jit(solution)/shard_map/ppermute | solution.py:219
  143.0 26.9 %collective-permute-start.2 = (bf16[512,512]{1,0:T(8,128)(2,1)}, bf16[512,512]{1,0:T(8,128)(2,1)}, u32[]{:S(2)}, u32[]{:S(2)}) collective-permute-start(bf16[512,512]{1,0:T(8,128)(2,1)} %all_gather.13), channel_id=1, source_target_pairs={{0,24},{8,0},{16,8},{24,16},{1,25},{9,1},{17,9},{25,17},{2,26},{10... | collective-permute-start | bytes 1572872 | tf_op jit(solution)/shard_map/ppermute | solution.py:219
  151.2 23.6 %all-to-all-start.3 = ((bf16[8,512,128]{2,1,0:T(8,128)(2,1)}), bf16[8,512,128]{2,1,0:T(8,128)(2,1)S(1)}, u32[]{:S(2)}, u32[]{:S(2)}) async-start(bf16[8,512,128]{2,1,0:T(8,128)(2,1)} %broadcast_in_dim.24), calls=%async_computation.3 | async-start | bytes 2097152 | tf_op jit(solution)/shard_map/all_to_all | solution.py:21
  158.1 16.7 %collective-permute-start.3 = (bf16[512,512]{1,0:T(8,128)(2,1)}, bf16[512,512]{1,0:T(8,128)(2,1)S(1)}, u32[]{:S(2)}, u32[]{:S(2)}) collective-permute-start(bf16[512,512]{1,0:T(8,128)(2,1)} %all_gather.13), channel_id=1, source_target_pairs={{0,1},{1,0},{2,3},{3,2},{4,5},{5,4},{6,7},{7,6},{8,9},{9,8},{10,11... | collective-permute-start | bytes 1572872 | tf_op jit(solution)/shard_map/ppermute | solution.py:25
  160.0 14.8 %collective-permute-start.4 = (bf16[512,512]{1,0:T(8,128)(2,1)}, bf16[512,512]{1,0:T(8,128)(2,1)S(1)}, u32[]{:S(2)}, u32[]{:S(2)}) collective-permute-start(bf16[512,512]{1,0:T(8,128)(2,1)} %collective-permute-done), channel_id=1, source_target_pairs={{0,1},{1,0},{2,3},{3,2},{4,5},{5,4},{6,7},{7,6},{8,9},{9,8},{10,11... | collective-permute-start | bytes 1572872 | tf_op jit(solution)/shard_map/ppermute | solution.py:25
  168.0 6.7 %collective-permute-start.5 = (bf16[512,512]{1,0:T(8,128)(2,1)}, bf16[512,512]{1,0:T(8,128)(2,1)S(1)}, u32[]{:S(2)}, u32[]{:S(2)}) collective-permute-start(bf16[512,512]{1,0:T(8,128)(2,1)} %collective-permute-done.1), channel_id=1, source_target_pairs={{0,1},{1,0},{2,3},{3,2},{4,5},{5,4},{6,7},{7,6},{8,9},{9,8},{10,11... | collective-permute-start | bytes 1572872 | tf_op jit(solution)/shard_map/ppermute | solution.py:25
  170.0 4.8 %collective-permute-start.6 = (bf16[512,512]{1,0:T(8,128)(2,1)}, bf16[512,512]{1,0:T(8,128)(2,1)S(1)}, u32[]{:S(2)}, u32[]{:S(2)}) collective-permute-start(bf16[512,512]{1,0:T(8,128)(2,1)} %collective-permute-done.2), channel_id=1, source_target_pairs={{0,1},{1,0},{2,3},{3,2},{4,5},{5,4},{6,7},{7,6},{8,9},{9,8},{10,11... | collective-permute-start | bytes 1572872 | tf_op jit(solution)/shard_map/ppermute | solution.py:25
  174.8 1.3 copy-start.8
  174.8 1.6 copy-start.3
  200.5 4.8 %collective-permute-start.7 = (bf16[256,2048]{1,0:T(8,128)(2,1)}, bf16[256,2048]{1,0:T(8,128)(2,1)S(1)}, u32[]{:S(2)}, u32[]{:S(2)}) collective-permute-start(bf16[256,2048]{1,0:T(8,128)(2,1)} %get-tuple-element.8), channel_id=1, source_target_pairs={{0,1},{1,0},{2,3},{3,2},{4,5},{5,4},{6,7},{7,6},{8,9},{9,8},{10,11... | collective-permute-start | bytes 3145736 | tf_op jit(solution)/shard_map/ppermute | solution.py:25
  208.2 18.5 %all-to-all-start.4 = ((bf16[4,64,2048]{2,1,0:T(8,128)(2,1)}), bf16[4,64,2048]{2,1,0:T(8,128)(2,1)S(1)}, u32[]{:S(2)}, u32[]{:S(2)}) async-start(bf16[4,64,2048]{2,1,0:T(8,128)(2,1)} %bitcast.32), calls=%async_computation.4 | async-start | bytes 2097152 | tf_op jit(solution)/shard_map/all_to_all | solution.py:38
  (4 other events, 4.0 us)
Sparse Core Ops, SparseCore 0:
  23.2 119.2 all-gather.1

commit v5 on v4

v5 whole, which is shorter than its diff:
```python
import jax
import jax.numpy as jnp
from jax import lax
from jax.experimental import pallas as pl
from jax.experimental.pallas import tpu as pltpu
from jax.sharding import Mesh
from jax.sharding import PartitionSpec as P

FS = ("z", "y")
TP = ("x", "c")

EPS = 1e-05
ALPHA = 2.0**0.25
BF16 = jnp.bfloat16
F32 = jnp.float32
ACROSS = (((1,), (1,)), ((), ()))


def sent_to_all(value, axis):
    copies = jnp.broadcast_to(value, (lax.axis_size(axis), *value.shape))
    return lax.all_to_all(copies, axis, split_axis=0, concat_axis=0, tiled=True)


def to_partner(value):
    return lax.ppermute(value, "c", [(0, 1), (1, 0)])


def row_norm(vals, gain):
    count = vals.shape[1]
    mean = jnp.sum(vals, axis=1, keepdims=True) / count
    square = jnp.sum(vals * vals, axis=1, keepdims=True) / count
    return (vals - mean) * lax.rsqrt(square - mean * mean + EPS) * gain


def whole_vmem():
    return pl.BlockSpec(memory_space=pltpu.VMEM)


def last_norm(pieces, base, gain, parts):
    peers, rows, width = pieces.shape

    def body(pieces_ref, base_ref, gain_ref, out_ref):
        added = pieces_ref[0].astype(F32)
        for k in range(1, peers):
            added = added + pieces_ref[k].astype(F32)
        vals = ALPHA * base_ref[...].astype(F32) + added.astype(BF16).astype(F32)
        done = row_norm(vals, gain_ref[...]).astype(BF16)
        for k in range(parts):
            out_ref[k] = done[:, k * (width // parts) : (k + 1) * (width // parts)]

    return pl.pallas_call(
        body,
        out_shape=jax.ShapeDtypeStruct((parts, rows, width // parts), BF16),
        in_specs=[whole_vmem()] * 3,
        out_specs=whole_vmem(),
        name="last_norm",
    )(pieces, base, gain.reshape(1, width))


def projected(place, gated, pieces):
    chips, rows, channels = gated.shape
    peers = len(pieces)
    depth = 32
    zs = pieces[0].shape[0] // depth
    wide = pieces[0].shape[1]
    width = zs * peers * depth
    steps = 8
    deep = zs // steps
    span = width // steps
    ahead = 3

    def body(place_ref, gated_ref, *rest):
        pieces = rest[:peers]
        out_ref, weights, left, left_sems, sems = rest[peers:]
        y = place_ref[2]
        first = []
        for k in range(chips):
            first.append(pltpu.make_async_copy(gated_ref.at[k], left.at[:, pl.ds(k * channels, channels)], left_sems.at[k]))
            first[k].start()
        copies = []
        for j in range(steps):
            at_z = pl.ds(j * deep, deep)
            some = []
            for n in range(peers):
                at_y = lax.rem(y + peers - n, peers)
                some.append(pltpu.make_async_copy(pieces[n].at[at_z], weights.at[at_z, at_y], sems.at[j, n]))
            copies.append(some)
        for some in copies[:ahead]:
            for c in some:
                c.start()
        for c in first:
            c.wait()
        for j in range(steps):
            for c in copies[j]:
                c.wait()
            if j + ahead < steps:
                for c in copies[j + ahead]:
                    c.start()
            right = weights[j * deep : (j + 1) * deep].reshape(span, wide)
            part = lax.dot_general(left[...], right, ACROSS, preferred_element_type=F32)
            out_ref[:, j * span : (j + 1) * span] = part.astype(BF16)

    given = [p.reshape(zs, depth, wide) for p in pieces]
    anywhere = pl.BlockSpec(memory_space=pl.ANY)
    return pl.pallas_call(
        body,
        out_shape=jax.ShapeDtypeStruct((rows, width), BF16),
        in_specs=[pl.BlockSpec(memory_space=pltpu.SMEM)] + [anywhere] * (1 + peers),
        out_specs=whole_vmem(),
        scratch_shapes=[
            pltpu.VMEM((zs, peers, depth, wide), BF16),
            pltpu.VMEM((rows, chips * channels), BF16),
            pltpu.SemaphoreType.DMA((chips,)),
            pltpu.SemaphoreType.DMA((steps, peers)),
        ],
        cost_estimate=pl.CostEstimate(flops=2 * rows * width * wide, bytes_accessed=6 << 20, transcendentals=0),
        name="projected",
    )(place, gated, *given)


def mixer(place, own, other, blocks, gain, ffw, ff):
    rows, width = own.shape
    parts, _, feats = blocks.shape
    chips = parts // 2
    half = rows // 2
    few = rows // parts
    edges = [0, 384, 768, 1152, 2 * ff, 3 * ff]
    spans = [e - b for b, e in zip(edges, edges[1:])]
    chunks = len(spans)
    ahead = 2
    step = 256

    def body(place_ref, own_ref, other_ref, blocks_ref, gain_ref, ffw_ref, mine_ref, keep_ref, give_ref, *rest):
        weights = rest[:chunks]
        base, low, high, vals, left, acc, in_sems, sems = rest[chunks:]
        core = place_ref[0]
        me = place_ref[1]
        inputs = []
        for j in range(parts):
            at = pl.ds(j * feats, feats)
            inputs.append(
                [
                    pltpu.make_async_copy(own_ref.at[:, at], low.at[j], in_sems.at[j, 0]),
                    pltpu.make_async_copy(other_ref.at[:, at], high.at[j], in_sems.at[j, 1]),
                    pltpu.make_async_copy(blocks_ref.at[j], base.at[j], in_sems.at[j, 2]),
                ]
            )
            for c in inputs[j]:
                c.start()
        copies = []
        for n in range(chunks):
            at = pl.ds(edges[n], spans[n])
            copies.append(pltpu.make_async_copy(ffw_ref.at[:, at], weights[n], sems.at[n]))
        for c in copies[:ahead]:
            c.start()
        total = jnp.zeros((rows, 1), F32)
        squares = jnp.zeros((rows, 1), F32)
        for j in range(parts):
            for c in inputs[j]:
                c.wait()
            mix = (low[j].astype(F32) + high[j].astype(F32)).astype(BF16)
            these = ALPHA * base[j].astype(F32) + mix.astype(F32)
            vals[j] = these
            total += jnp.sum(these, axis=1, keepdims=True)
            squares += jnp.sum(these * these, axis=1, keepdims=True)
        mean = total / width
        scale = lax.rsqrt(squares / width - mean * mean + EPS)
        for j in range(parts):
            at = slice(j * feats, (j + 1) * feats)
            left[:, at] = ((vals[j] - mean) * scale * gain_ref[:, at]).astype(BF16)
        mine_ref[...] = left[pl.ds(pl.multiple_of(me * few, few), few), :]
        for n in range(chunks - 1):
            copies[n].wait()
            if n + ahead < chunks:
                copies[n + ahead].start()
            acc[:, edges[n] : edges[n + 1]] = jnp.dot(left[...], weights[n][...], preferred_element_type=F32)
        gate = acc[:, :ff]
        hidden = (gate * lax.logistic(gate) * acc[:, ff:]).astype(BF16)
        copies[-1].wait()

        def out(keep_core):
            for b in range(0, width, step):
                done = lax.dot_general(hidden, weights[-1][b : b + step], ACROSS, preferred_element_type=F32).astype(BF16)
                for x in range(chips):
                    here = slice(x * few, (x + 1) * few)
                    keep = (2 * x + keep_core) * few
                    give = (2 * x + 1 - keep_core) * few
                    keep_ref[here, b : b + step] = done[keep : keep + few]
                    give_ref[here, b : b + step] = done[give : give + few]

        @pl.when(core == 0)
        def _():
            out(0)

        @pl.when(core == 1)
        def _():
            out(1)

    anywhere = pl.BlockSpec(memory_space=pl.ANY)
    return pl.pallas_call(
        body,
        out_shape=(
            jax.ShapeDtypeStruct((few, width), BF16),
            jax.ShapeDtypeStruct((half, width), BF16),
            jax.ShapeDtypeStruct((half, width), BF16),
        ),
        in_specs=[pl.BlockSpec(memory_space=pltpu.SMEM), anywhere, anywhere, anywhere, whole_vmem(), anywhere],
        out_specs=(whole_vmem(),) * 3,
        scratch_shapes=[
            *(pltpu.VMEM((width, n), BF16) for n in spans),
            pltpu.VMEM((parts, rows, feats), BF16),
            pltpu.VMEM((parts, rows, feats), BF16),
            pltpu.VMEM((parts, rows, feats), BF16),
            pltpu.VMEM((parts, rows, feats), F32),
            pltpu.VMEM((rows, width), BF16),
            pltpu.VMEM((rows, 2 * ff), F32),
            pltpu.SemaphoreType.DMA((parts, 3)),
            pltpu.SemaphoreType.DMA((chunks,)),
        ],
        cost_estimate=pl.CostEstimate(flops=6 * rows * width * ff, bytes_accessed=18 << 20, transcendentals=rows * ff),
        name="mixer",
    )(place, own, other, blocks, gain.reshape(1, width), ffw)


def from_each(value, axis):
    size = lax.axis_size(axis)
    return [value] + [lax.ppermute(value, axis, [(i, (i + k) % size) for i in range(size)]) for k in range(1, size)]


def on_device(
    tokens,
    u_weight,
    v_weight,
    sg_gain,
    spatial_weight,
    spatial_bias,
    out_weight,
    gain_one,
    gate_weight,
    up_weight,
    down_weight,
    gain_two,
):
    core = lax.axis_index("c")
    chips = lax.axis_size("x")
    parts = chips * lax.axis_size("c")
    rows, feats = tokens.shape
    width = feats * parts
    sg = u_weight.shape[1]
    own_rows = rows // parts

    blocks = sent_to_all(tokens, TP)

    ffw = lax.all_gather(jnp.concatenate([gate_weight, up_weight, down_weight.T], axis=1), "y", axis=0, tiled=True)
    ffw = lax.all_gather(ffw, "z", axis=0, tiled=True)

    small = jnp.concatenate([u_weight, v_weight, out_weight.T], axis=1)
    depth = small.shape[0]
    small = lax.all_gather(small, "z", axis=0, tiled=True)
    gates = sent_to_all(small[:, : 2 * sg], "y")
    gates = gates.reshape(gates.shape[0], -1, depth, 2 * sg)
    gates = jnp.swapaxes(gates, 0, 1).reshape(width, 2 * sg)
    out_x = lax.all_gather(small[:, 2 * sg :], "x", axis=1, tiled=True)
    out_rows = from_each(out_x, "y")

    whole = jnp.moveaxis(blocks, 0, 1).reshape(rows, width)

    pre_u = jnp.dot(whole, gates[:, :sg], preferred_element_type=F32)
    pre_v = jnp.dot(whole, gates[:, sg:], preferred_element_type=F32)
    gated = jax.nn.gelu(pre_u)
    valued = jax.nn.gelu(pre_v)
    sums = jnp.stack([jnp.sum(valued, axis=1), jnp.sum(valued * valued, axis=1)])
    gains = jnp.concatenate([gain_one, gain_two]).reshape(-1, rows)
    known = sent_to_all(jnp.concatenate([sums, gains], axis=0), TP)
    gains = known[:, 2:].reshape(parts, 2, feats)
    gain_1 = gains[:, 0].reshape(width)
    gain_2 = gains[:, 1].reshape(width)
    sums = jnp.sum(known[:, :2], axis=0)
    count = sg * parts
    mean = sums[0][:, None] / count
    square = sums[1][:, None] / count
    normed = (valued - mean) * lax.rsqrt(square - mean * mean + EPS) * sg_gain[None, :]
    normed = normed.astype(BF16)

    groups = spatial_weight.shape[0]
    block = spatial_weight.shape[1]
    shaped = normed.reshape(rows // block, block, groups, sg // groups)
    lower = jnp.tril(jnp.ones((block, block), jnp.bool_))
    masked = jnp.where(lower[None], spatial_weight, jnp.zeros_like(spatial_weight))
    mixed = jnp.einsum("gij,njgd->nigd", masked, shaped, preferred_element_type=F32)
    mixed = mixed + spatial_bias.T[None, :, :, None]
    gated_out = (gated * mixed.reshape(rows, sg)).astype(BF16)

    together = sent_to_all(gated_out, "x")
    place = jnp.stack([core, lax.axis_index(TP), lax.axis_index("y")]).astype(jnp.int32)
    own = projected(place, together, out_rows)
    mine, keep, give = mixer(place, own, to_partner(own), blocks, gain_1, ffw, gate_weight.shape[1])
    pair = (keep.astype(F32) + to_partner(give).astype(F32)).astype(BF16)
    pieces = lax.all_to_all(pair.reshape(chips, own_rows, width), "x", 0, 0, tiled=True)
    last = last_norm(pieces, mine, gain_2, parts)
    return lax.all_to_all(last, TP, 0, 0, tiled=True).reshape(rows, feats)


def solution(mesh):
    tp = mesh.shape["tp"]
    finer = Mesh(mesh.devices.reshape(16, 4, tp // 2, 2), ("z", "y", "x", "c"))
    return jax.shard_map(
        on_device,
        mesh=finer,
        in_specs=(
            P(FS, TP),
            P(FS, TP),
            P(FS, TP),
            P(TP),
            P(TP, None, None),
            P(TP, None),
            P(TP, FS),
            P(TP),
            P(FS, TP),
            P(FS, TP),
            P(TP, FS),
            P(TP),
        ),
        out_specs=P(FS, TP),
        check_vma=False,
    )
```

time: 250 us -> 242 us (0.968)
  starting transfers between devices: 57.1 us -> 38.1 us
  blocking collectives: 81.4 us -> 99.6 us
  local copies, waits for them, and re-layouts: 20.4 us -> 15 us
  waiting for transfers between devices: 41.3 us -> 44.2 us
  Pallas kernels: 26.4 us -> 23.8 us
    all_to_all x1 -> x2, blocking collectives: 10.8 us -> 29 us  [the longest x1 17.4 us: on_device(): lax.all_to_all(pair.reshape(chips, own_rows, width), 'x', 0, 0, tiled=True)]
    ppermute x3, waiting for transfers between devices: 0.01 us -> 14.3 us  [from_each(): lax.ppermute(value, axis, [(i, (i + k) % size) for i in range(size)])]
    all_to_all x1 -> x0, waiting for transfers between devices: 13.3 us -> none  [summed_rows(): return lax.all_to_all(pieces, 'x', 0, 0, tiled=True)]
    ppermute x5 -> x2, starting transfers between devices: 16.4 us -> 4.87 us  [to_partner(): return lax.ppermute(value, 'c', [(0, 1), (1, 0)])]
    all_to_all x1 -> x0, starting transfers between devices: 3.51 us -> none  [summed_rows(): return lax.all_to_all(pieces, 'x', 0, 0, tiled=True)]
    all_to_all x3, starting transfers between devices: 28.8 us -> 25.5 us  [sent_to_all(): return lax.all_to_all(copies, axis, split_axis=0, concat_axis=0, tiled=True)]
    slice x4 -> x0, local copies, waits for them, and re-layouts: 2.96 us -> none  [the longest x1 0.78 us: packed_ffw(): up[:, :cut]]
    pallas_call x2, Pallas kernels: 24 us -> 21.4 us  [the longest x1 14 us: mixer(): pl.pallas_call(body, out_shape=(jax.ShapeDtypeStruct((few, width), BF16),...]
  transfers between devices with their start and end apart: 13 -> 9, of which waited for: 3 -> 5; matrix products, arithmetic and copies ran while one was open for 7% -> 6% of each run, Pallas kernels for 5% -> 3%
where the time goes in v5:
time: 242 us; the launch traced here: 241 us
  blocking collectives  99.6 us (41%)
  waiting for transfers between devices  44.2 us (18%)
  starting transfers between devices  38.1 us (16%)
  Pallas kernels  23.8 us (10%)
  local copies, waits for them, and re-layouts  15 us (6%)
  between operations  13.7 us (6%)
  other arithmetic  3.94 us (2%)
  matrix products  2.73 us (1%)
    all_gather x1, blocking collectives, on_device(): small = lax.all_gather(small, 'z', axis=0, tiled=True)  33 us
    all_to_all x3, starting transfers between devices, sent_to_all(): return lax.all_to_all(copies, axis, split_axis=0, concat_axis=0, tiled=True)  25.5 us
    all_to_all x3, waiting for transfers between devices, sent_to_all(): return lax.all_to_all(copies, axis, split_axis=0, concat_axis=0, tiled=True)  25.1 us
    all_to_all x1, blocking collectives, on_device(): lax.all_to_all(pair.reshape(chips, own_rows, width), 'x', 0, 0, tiled=True)  17.4 us
    ppermute x3, waiting for transfers between devices, from_each(): lax.ppermute(value, axis, [(i, (i + k) % size) for i in range(size)])  14.3 us
    pallas_call x1, Pallas kernels, mixer(): pl.pallas_call(body, out_shape=(jax.ShapeDtypeStruct((few, width), BF16),...  14 us
    all_gather x1, blocking collectives, on_device(): out_x = lax.all_gather(small[:, 2 * sg:], 'x', axis=1, tiled=True)  12.8 us
    all_gather x1, blocking collectives, on_device(): lax.all_gather(jnp.concatenate([gate_weight, up_weight, down_weight.T], a...  12.7 us
  transfers between devices with their start and end apart: 9, of which 5 were waited for; matrix products, arithmetic and copies ran while one was open for 6% of the time, Pallas kernels for 3%

profile of v5, /device:TPU:1, one launch (start us, length us, event | category | flops | bytes accessed | tf_op | source)
XLA Modules:
  0.0 241.1 jit_solution(10255096673289436154)
XLA Ops:
  7.5 12.7 %all_gather.14 = bf16[128,2112]{1,0:T(8,128)(2,1)} all-gather(bf16[32,2112]{1,0:T(8,128)(2,1)S(1)} %concatenate.15), channel_id=1, replica_groups=mesh['z'=16,'y'=4,'x'=4,'c'=2] {'y'}, dimensions={0}, use_global_device_ids=true | all-gather | bytes 675840 | tf_op jit(solution)/shard_map/all_gather | solution.py:254
  20.9 33.0 %all_gather.12 = bf16[512,384]{1,0:T(8,128)(2,1)S(1)} all-gather(bf16[32,384]{1,0:T(8,128)(2,1)S(1)} %pad_maximum_fusion), channel_id=1, replica_groups=mesh['z'=16,'y'=4,'x'=4,'c'=2] {'z'}, dimensions={0}, use_global_device_ids=true | all-gather | bytes 417792 | tf_op jit(solution)/shard_map/all_gather | solution.py:259
  54.1 12.2 %all_to_all.30 = bf16[4,512,256]{2,1,0:T(8,128)(2,1)S(1)} all-to-all(bf16[4,512,256]{2,1,0:T(8,128)(2,1)S(1)} %broadcast_in_dim.20), channel_id=1, replica_groups=mesh['z'=16,'y'=4,'x'=4,'c'=2] {'y'}, dimensions={0} | all-to-all | bytes 2097152 | tf_op jit(solution)/shard_map/all_to_all | solution.py:21
  67.7 17.2 %all-to-all-start.1 = ((bf16[8,512,256]{2,1,0:T(8,128)(2,1)}), bf16[8,512,256]{2,1,0:T(8,128)(2,1)S(1)}, u32[]{:S(2)}, u32[]{:S(2)}) async-start(bf16[8,512,256]{2,1,0:T(8,128)(2,1)} %broadcast_in_dim.21), calls=%async_computation.1 | async-start | bytes 4194304 | tf_op jit(solution)/shard_map/all_to_all | solution.py:21
  86.0 25.1 %all-to-all-done.1.blocks_ref = bf16[8,512,256]{2,1,0:T(8,128)(2,1)S(1)} async-done(((bf16[8,512,256]{2,1,0:T(8,128)(2,1)}), bf16[8,512,256]{2,1,0:T(8,128)(2,1)S(1)}, u32[]{:S(2)}, u32[]{:S(2)}) %all-to-all-start.1) | async-done | bytes 2097184 | tf_op jit(solution)/shard_map/all_to_all | solution.py:21
  112.4 3.0 %copy.26 = bf16[512,8,256]{0,2,1:T(8,128)(2,1)S(1)} copy(bf16[512,8,256]{2,0,1:T(8,128)(2,1)} %bitcast.54) | data formatting | bytes 4194304 | tf_op jit(solution)/shard_map/transpose | solution.py:266
  116.7 4.8 %all-to-all-start.2 = ((f32[8,3,512]{2,1,0:T(4,128)}), f32[8,3,512]{2,1,0:T(4,128)}, u32[]{:S(2)}, u32[]{:S(2)}) async-start(f32[8,3,512]{2,1,0:T(4,128)} %broadcast_in_dim.22), calls=%async_computation.2 | async-start | bytes 131072 | tf_op jit(solution)/shard_map/all_to_all | solution.py:21
  121.5 12.8 %all_gather.13 = bf16[512,512]{1,0:T(8,128)(2,1)} all-gather(bf16[512,128]{1,0:T(8,128)(2,1)S(1)} %slice-done), channel_id=1, replica_groups=mesh['z'=16,'y'=4,'x'=4,'c'=2] {'x'}, dimensions={1}, use_global_device_ids=true | all-gather | bytes 655360 | tf_op jit(solution)/shard_map/all_gather | solution.py:263
  134.2 2.8 %collective-permute-start.2 = (bf16[512,512]{1,0:T(8,128)(2,1)}, bf16[512,512]{1,0:T(8,128)(2,1)}, u32[]{:S(2)}, u32[]{:S(2)}) collective-permute-start(bf16[512,512]{1,0:T(8,128)(2,1)} %all_gather.13), channel_id=1, source_target_pairs={{0,24},{8,0},{16,8},{24,16},{1,25},{9,1},{17,9},{25,17},{2,26},{10... | collective-permute-start | bytes 1572872 | tf_op jit(solution)/shard_map/ppermute | solution.py:227
  137.1 3.1 %collective-permute-start.1 = (bf16[512,512]{1,0:T(8,128)(2,1)}, bf16[512,512]{1,0:T(8,128)(2,1)}, u32[]{:S(2)}, u32[]{:S(2)}) collective-permute-start(bf16[512,512]{1,0:T(8,128)(2,1)} %all_gather.13), channel_id=1, source_target_pairs={{0,16},{8,24},{16,0},{24,8},{1,17},{9,25},{17,1},{25,9},{2,18},{10... | collective-permute-start | bytes 1572872 | tf_op jit(solution)/shard_map/ppermute | solution.py:227
  140.1 1.9 collective-permute-start
  143.2 1.6 fusion
  147.4 3.5 %all-to-all-start.3 = ((bf16[4,512,128]{2,1,0:T(8,128)(2,1)}), bf16[4,512,128]{2,1,0:T(8,128)(2,1)S(1)}, u32[]{:S(2)}, u32[]{:S(2)}) async-start(bf16[4,512,128]{2,1,0:T(8,128)(2,1)} %broadcast_in_dim.24), calls=%async_computation.3 | async-start | bytes 1048576 | tf_op jit(solution)/shard_map/all_to_all | solution.py:21
  152.0 13.9 %collective-permute-done = bf16[512,512]{1,0:T(8,128)(2,1)} collective-permute-done((bf16[512,512]{1,0:T(8,128)(2,1)}, bf16[512,512]{1,0:T(8,128)(2,1)}, u32[]{:S(2)}, u32[]{:S(2)}) %collective-permute-start) | collective-permute-done | bytes 524320 | tf_op jit(solution)/shard_map/ppermute | solution.py:227
  166.6 7.4 %projected.1.own_ref = bf16[512,2048]{1,0:T(8,128)(2,1)} custom-call(s32[3]{0:T(128)} %pad_add_fusion.place_ref, bf16[4,512,128]{2,1,0:T(8,128)(2,1)} %copy-done.2, bf16[16,32,512]{2,1,0:T(8,128)(2,1)} %bitcast.23.rest_0_, bf16[16,32,512]{2,1,0:T(8,128)(2,1)} %bitcast.24.rest_1_, bf16[16,32,512]{2,1,0:T(8,128)(2,1)} %bitcast.25.rest_2_, ...), custom_call_target="tpu_custom_call" | custom-call | flops 1073741824 | bytes 6291456 | tf_op jit(solution)/shard_map/projected/pallas_call | solution.py:105
  174.1 2.6 %collective-permute-start.3 = (bf16[512,2048]{1,0:T(8,128)(2,1)}, bf16[512,2048]{1,0:T(8,128)(2,1)S(1)}, u32[]{:S(2)}, u32[]{:S(2)}) collective-permute-start(bf16[512,2048]{1,0:T(8,128)(2,1)} %projected.1.own_ref), channel_id=1, source_target_pairs={{0,1},{1,0},{2,3},{3,2},{4,5},{5,4},{6,7},{7,6},{8,9},{9,8},{10,11... | collective-permute-start | bytes 6291464 | tf_op jit(solution)/shard_map/ppermute | solution.py:25
  178.2 2.3 collective-permute-done.3.other_ref
  181.8 14.0 %mixer.1 = (bf16[64,2048]{1,0:T(8,128)(2,1)}, bf16[256,2048]{1,0:T(8,128)(2,1)}, bf16[256,2048]{1,0:T(8,128)(2,1)}) custom-call(s32[3]{0:T(128)} %pad_add_fusion.place_ref, bf16[512,2048]{1,0:T(8,128)(2,1)} %projected.1.own_ref, bf16[512,2048]{1,0:T(8,128)(2,1)} %copy-done.9, bf16[8,512,256]{2,1,0:T(8,128)(2,1)} %copy-done, f32[1,2048]{1,0:T(1,128)} %bitcast.69, ...), custom_call_target="tpu_custom_call" | custom-call | flops 4429185024 | bytes 18874368 | tf_op jit(solution)/shard_map/mixer/pallas_call | solution.py:200
  195.8 2.3 collective-permute-start.4
  198.1 2.5 %collective-permute-done.4 = bf16[256,2048]{1,0:T(8,128)(2,1)S(1)} collective-permute-done((bf16[256,2048]{1,0:T(8,128)(2,1)}, bf16[256,2048]{1,0:T(8,128)(2,1)S(1)}, u32[]{:S(2)}, u32[]{:S(2)}) %collective-permute-start.4) | collective-permute-done | bytes 1048608 | tf_op jit(solution)/shard_map/ppermute | solution.py:25
  200.6 1.6 add_convert_fusion
  202.2 17.4 %all_to_all.31.pieces_ref = bf16[4,64,2048]{2,1,0:T(8,128)(2,1)} all-to-all(bf16[4,64,2048]{2,1,0:T(8,128)(2,1)S(1)} %bitcast.55), channel_id=1, replica_groups=mesh['z'=16,'y'=4,'x'=4,'c'=2] {'x'}, dimensions={0} | all-to-all | bytes 2097152 | tf_op jit(solution)/shard_map/all_to_all | solution.py:299
  219.6 2.4 %last_norm.1 = bf16[8,64,256]{2,1,0:T(8,128)(2,1)} custom-call(bf16[4,64,2048]{2,1,0:T(8,128)(2,1)} %all_to_all.31.pieces_ref, bf16[64,2048]{1,0:T(8,128)(2,1)} %get-tuple-element.10.base_ref, f32[1,2048]{1,0:T(1,128)} %bitcast.63), custom_call_target="tpu_custom_call" | custom-call | tf_op jit(solution)/shard_map/last_norm/pallas_call | solution.py:51
  222.0 11.5 %all_to_all.32 = bf16[8,64,256]{2,1,0:T(8,128)(2,1)S(1)} all-to-all(bf16[8,64,256]{2,1,0:T(8,128)(2,1)} %last_norm.1), channel_id=1, replica_groups=mesh['z'=16,'y'=4,'x'=4,'c'=2] {'x','c'}, dimensions={0} | all-to-all | bytes 524288 | tf_op jit(solution)/shard_map/all_to_all | solution.py:301
  (53 shorter events, 15.9 us)
Async XLA Ops:
  6.5 174.0 %all-gather.2.cloned.1.call-start = ((), (), s32[]{:S(2)}) async-start(), calls=%async_computation.6 | async-start | bytes 9469952 | tf_op jit(solution)/shard_map/all_gather | solution.py:255
  20.9 45.3 %copy-start.4 = (bf16[512,256]{1,0:T(8,128)(2,1)S(1)}, bf16[512,256]{1,0:T(8,128)(2,1)}, u32[]{:S(2)}) copy-start(bf16[512,256]{1,0:T(8,128)(2,1)} %param.12) | copy-start | bytes 786436
  53.9 31.0 %copy-start.3 = (bf16[512,384]{1,0:T(8,128)(2,1)}, bf16[512,384]{1,0:T(8,128)(2,1)S(1)}, u32[]{:S(2)}) copy-start(bf16[512,384]{1,0:T(8,128)(2,1)S(1)} %all_gather.12) | copy-start | bytes 1179652
  67.7 17.2 %copy-start.5 = (f32[256]{0:T(256)S(1)}, f32[256]{0:T(256)}, u32[]{:S(2)}) copy-start(f32[256]{0:T(256)} %param.23) | copy-start | bytes 3076
  67.7 17.2 %copy-start.6 = (f32[256]{0:T(256)S(1)}, f32[256]{0:T(256)}, u32[]{:S(2)}) copy-start(f32[256]{0:T(256)} %param.19) | copy-start | bytes 3076
  67.7 43.4 %all-to-all-start.1 = ((bf16[8,512,256]{2,1,0:T(8,128)(2,1)}), bf16[8,512,256]{2,1,0:T(8,128)(2,1)S(1)}, u32[]{:S(2)}, u32[]{:S(2)}) async-start(bf16[8,512,256]{2,1,0:T(8,128)(2,1)} %broadcast_in_dim.21), calls=%async_computation.1 | async-start | bytes 4194304 | tf_op jit(solution)/shard_map/all_to_all | solution.py:21
  111.1 1.3 copy-start
  112.4 3.0 %copy-start.1 = (bf16[16,4,32,256]{3,2,1,0:T(8,128)(2,1)S(1)}, bf16[16,4,32,256]{3,2,1,0:T(8,128)(2,1)}, u32[]{:S(2)}) copy-start(bf16[16,4,32,256]{3,2,1,0:T(8,128)(2,1)} %copy.25) | copy-start | bytes 3145732
  115.4 6.1 %slice-start = ((bf16[512,384]{1,0:T(8,128)(2,1)}), bf16[512,128]{1,0:T(8,128)(2,1)S(1)}, s32[]{:S(2)}) async-start(bf16[512,384]{1,0:T(8,128)(2,1)} %copy-done.3), calls=%async_computation.7 | async-start | bytes 262144 | tf_op jit(solution)/shard_map/slice | solution.py:263
  115.4 27.5 %copy-start.7 = (f32[128]{0:T(128)S(1)}, f32[128]{0:T(128)}, u32[]{:S(2)}) copy-start(f32[128]{0:T(128)} %param.15) | copy-start | bytes 1540
  115.4 27.7 %copy-start.8 = (f32[1,128]{1,0:T(1,128)S(1)}, f32[1,128]{1,0:T(1,128)}, u32[]{:S(2)}) copy-start(f32[1,128]{1,0:T(1,128)} %param.17) | copy-start | bytes 1540
  116.7 25.4 %all-to-all-start.2 = ((f32[8,3,512]{2,1,0:T(4,128)}), f32[8,3,512]{2,1,0:T(4,128)}, u32[]{:S(2)}, u32[]{:S(2)}) async-start(f32[8,3,512]{2,1,0:T(4,128)} %broadcast_in_dim.22), calls=%async_computation.2 | async-start | bytes 131072 | tf_op jit(solution)/shard_map/all_to_all | solution.py:21
  134.2 17.3 %collective-permute-start.2 = (bf16[512,512]{1,0:T(8,128)(2,1)}, bf16[512,512]{1,0:T(8,128)(2,1)}, u32[]{:S(2)}, u32[]{:S(2)}) collective-permute-start(bf16[512,512]{1,0:T(8,128)(2,1)} %all_gather.13), channel_id=1, source_target_pairs={{0,24},{8,0},{16,8},{24,16},{1,25},{9,1},{17,9},{25,17},{2,26},{10... | collective-permute-start | bytes 1572872 | tf_op jit(solution)/shard_map/ppermute | solution.py:227
  137.1 14.9 %collective-permute-start.1 = (bf16[512,512]{1,0:T(8,128)(2,1)}, bf16[512,512]{1,0:T(8,128)(2,1)}, u32[]{:S(2)}, u32[]{:S(2)}) collective-permute-start(bf16[512,512]{1,0:T(8,128)(2,1)} %all_gather.13), channel_id=1, source_target_pairs={{0,16},{8,24},{16,0},{24,8},{1,17},{9,25},{17,1},{25,9},{2,18},{10... | collective-permute-start | bytes 1572872 | tf_op jit(solution)/shard_map/ppermute | solution.py:227
  140.1 25.7 %collective-permute-start = (bf16[512,512]{1,0:T(8,128)(2,1)}, bf16[512,512]{1,0:T(8,128)(2,1)}, u32[]{:S(2)}, u32[]{:S(2)}) collective-permute-start(bf16[512,512]{1,0:T(8,128)(2,1)} %all_gather.13), channel_id=1, source_target_pairs={{0,8},{8,16},{16,24},{24,0},{1,9},{9,17},{17,25},{25,1},{2,10},{10... | collective-permute-start | bytes 1572872 | tf_op jit(solution)/shard_map/ppermute | solution.py:227
  147.4 18.4 %all-to-all-start.3 = ((bf16[4,512,128]{2,1,0:T(8,128)(2,1)}), bf16[4,512,128]{2,1,0:T(8,128)(2,1)S(1)}, u32[]{:S(2)}, u32[]{:S(2)}) async-start(bf16[4,512,128]{2,1,0:T(8,128)(2,1)} %broadcast_in_dim.24), calls=%async_computation.3 | async-start | bytes 1048576 | tf_op jit(solution)/shard_map/all_to_all | solution.py:21
  165.8 0.8 copy-start.2
  174.1 6.4 %collective-permute-start.3 = (bf16[512,2048]{1,0:T(8,128)(2,1)}, bf16[512,2048]{1,0:T(8,128)(2,1)S(1)}, u32[]{:S(2)}, u32[]{:S(2)}) collective-permute-start(bf16[512,2048]{1,0:T(8,128)(2,1)} %projected.1.own_ref), channel_id=1, source_target_pairs={{0,1},{1,0},{2,3},{3,2},{4,5},{5,4},{6,7},{7,6},{8,9},{9,8},{10,11... | collective-permute-start | bytes 6291464 | tf_op jit(solution)/shard_map/ppermute | solution.py:25
  180.5 1.3 copy-start.9
  195.8 4.8 %collective-permute-start.4 = (bf16[256,2048]{1,0:T(8,128)(2,1)}, bf16[256,2048]{1,0:T(8,128)(2,1)S(1)}, u32[]{:S(2)}, u32[]{:S(2)}) collective-permute-start(bf16[256,2048]{1,0:T(8,128)(2,1)} %get-tuple-element.9), channel_id=1, source_target_pairs={{0,1},{1,0},{2,3},{3,2},{4,5},{5,4},{6,7},{7,6},{8,9},{9,8},{10,11... | collective-permute-start | bytes 3145736 | tf_op jit(solution)/shard_map/ppermute | solution.py:25
Sparse Core Ops, SparseCore 0:
  20.3 119.2 all-gather.1

commit v6 on v5

--- a/solution.py
+++ b/solution.py
@@ -30,6 +30,14 @@
     mean = jnp.sum(vals, axis=1, keepdims=True) / count
     square = jnp.sum(vals * vals, axis=1, keepdims=True) / count
     return (vals - mean) * lax.rsqrt(square - mean * mean + EPS) * gain
+
+
+def in_vmem(value):
+    return pltpu.with_memory_space_constraint(value, pltpu.VMEM)
+
+
+def in_hbm(value):
+    return pltpu.with_memory_space_constraint(value, pltpu.HBM)
 
 
 def whole_vmem():
@@ -50,11 +58,11 @@
 
     return pl.pallas_call(
         body,
-        out_shape=jax.ShapeDtypeStruct((parts, rows, width // parts), BF16),
+        out_shape=pltpu.VMEM((parts, rows, width // parts), BF16),
         in_specs=[whole_vmem()] * 3,
         out_specs=whole_vmem(),
         name="last_norm",
-    )(pieces, base, gain.reshape(1, width))
+    )(in_vmem(pieces), in_vmem(base), gain.reshape(1, width))
 
 
 def projected(place, gated, pieces):
@@ -71,12 +79,8 @@
 
     def body(place_ref, gated_ref, *rest):
         pieces = rest[:peers]
-        out_ref, weights, left, left_sems, sems = rest[peers:]
+        out_ref, weights, left, sems = rest[peers:]
         y = place_ref[2]
-        first = []
-        for k in range(chips):
-            first.append(pltpu.make_async_copy(gated_ref.at[k], left.at[:, pl.ds(k * channels, channels)], left_sems.at[k]))
-            first[k].start()
         copies = []
         for j in range(steps):
             at_z = pl.ds(j * deep, deep)
@@ -88,8 +92,8 @@
         for some in copies[:ahead]:
             for c in some:
                 c.start()
-        for c in first:
-            c.wait()
+        for k in range(chips):
+            left[:, k * channels : (k + 1) * channels] = gated_ref[k]
         for j in range(steps):
             for c in copies[j]:
                 c.wait()
@@ -105,17 +109,16 @@
     return pl.pallas_call(
         body,
         out_shape=jax.ShapeDtypeStruct((rows, width), BF16),
-        in_specs=[pl.BlockSpec(memory_space=pltpu.SMEM)] + [anywhere] * (1 + peers),
+        in_specs=[pl.BlockSpec(memory_space=pltpu.SMEM), whole_vmem()] + [anywhere] * peers,
         out_specs=whole_vmem(),
         scratch_shapes=[
             pltpu.VMEM((zs, peers, depth, wide), BF16),
             pltpu.VMEM((rows, chips * channels), BF16),
-            pltpu.SemaphoreType.DMA((chips,)),
             pltpu.SemaphoreType.DMA((steps, peers)),
         ],
         cost_estimate=pl.CostEstimate(flops=2 * rows * width * wide, bytes_accessed=6 << 20, transcendentals=0),
         name="projected",
-    )(place, gated, *given)
+    )(in_hbm(place), in_vmem(gated), *given)
 
 
 def mixer(place, own, other, blocks, gain, ffw, ff):
@@ -132,7 +135,7 @@
 
     def body(place_ref, own_ref, other_ref, blocks_ref, gain_ref, ffw_ref, mine_ref, keep_ref, give_ref, *rest):
         weights = rest[:chunks]
-        base, low, high, vals, left, acc, in_sems, sems = rest[chunks:]
+        base, low, vals, left, acc, in_sems, sems = rest[chunks:]
         core = place_ref[0]
         me = place_ref[1]
         inputs = []
@@ -141,8 +144,7 @@
             inputs.append(
                 [
                     pltpu.make_async_copy(own_ref.at[:, at], low.at[j], in_sems.at[j, 0]),
-                    pltpu.make_async_copy(other_ref.at[:, at], high.at[j], in_sems.at[j, 1]),
-                    pltpu.make_async_copy(blocks_ref.at[j], base.at[j], in_sems.at[j, 2]),
+                    pltpu.make_async_copy(blocks_ref.at[j], base.at[j], in_sems.at[j, 1]),
                 ]
             )
             for c in inputs[j]:
@@ -158,7 +160,8 @@
         for j in range(parts):
             for c in inputs[j]:
                 c.wait()
-            mix = (low[j].astype(F32) + high[j].astype(F32)).astype(BF16)
+            high = other_ref[:, j * feats : (j + 1) * feats]
+            mix = (low[j].astype(F32) + high.astype(F32)).astype(BF16)
             these = ALPHA * base[j].astype(F32) + mix.astype(F32)
             vals[j] = these
             total += jnp.sum(these, axis=1, keepdims=True)
@@ -196,30 +199,30 @@
         def _():
             out(1)
 
-    anywhere = pl.BlockSpec(memory_space=pl.ANY)
+    anywhere = pl.BlockSpec(memory_space=pltpu.HBM)
     return pl.pallas_call(
         body,
         out_shape=(
-            jax.ShapeDtypeStruct((few, width), BF16),
-            jax.ShapeDtypeStruct((half, width), BF16),
-            jax.ShapeDtypeStruct((half, width), BF16),
+            pltpu.VMEM((few, width), BF16),
+            pltpu.VMEM((half, width), BF16),
+            pltpu.VMEM((half, width), BF16),
         ),
-        in_specs=[pl.BlockSpec(memory_space=pltpu.SMEM), anywhere, anywhere, anywhere, whole_vmem(), anywhere],
+        in_specs=[pl.BlockSpec(memory_space=pltpu.SMEM), anywhere, whole_vmem(), anywhere, whole_vmem(), anywhere],
         out_specs=(whole_vmem(),) * 3,
         scratch_shapes=[
             *(pltpu.VMEM((width, n), BF16) for n in spans),
             pltpu.VMEM((parts, rows, feats), BF16),
             pltpu.VMEM((parts, rows, feats), BF16),
-            pltpu.VMEM((parts, rows, feats), BF16),
             pltpu.VMEM((parts, rows, feats), F32),
             pltpu.VMEM((rows, width), BF16),
             pltpu.VMEM((rows, 2 * ff), F32),
-            pltpu.SemaphoreType.DMA((parts, 3)),
+            pltpu.SemaphoreType.DMA((parts, 2)),
             pltpu.SemaphoreType.DMA((chunks,)),
         ],
         cost_estimate=pl.CostEstimate(flops=6 * rows * width * ff, bytes_accessed=18 << 20, transcendentals=rows * ff),
         name="mixer",
-    )(place, own, other, blocks, gain.reshape(1, width), ffw)
+        compiler_params=pltpu.CompilerParams(vmem_limit_bytes=40 << 20),
+    )(in_hbm(place), in_hbm(own), in_vmem(other), in_hbm(blocks), gain.reshape(1, width), in_hbm(ffw))
 
 
 def from_each(value, axis):
@@ -254,14 +257,15 @@
     ffw = lax.all_gather(jnp.concatenate([gate_weight, up_weight, down_weight.T], axis=1), "y", axis=0, tiled=True)
     ffw = lax.all_gather(ffw, "z", axis=0, tiled=True)
 
-    small = jnp.concatenate([u_weight, v_weight, out_weight.T], axis=1)
+    out_x = lax.all_gather(out_weight.T, "x", axis=1, tiled=True)
+    small = jnp.concatenate([u_weight, v_weight, out_x], axis=1)
     depth = small.shape[0]
     small = lax.all_gather(small, "z", axis=0, tiled=True)
     gates = sent_to_all(small[:, : 2 * sg], "y")
     gates = gates.reshape(gates.shape[0], -1, depth, 2 * sg)
-    gates = jnp.swapaxes(gates, 0, 1).reshape(width, 2 * sg)
-    out_x = lax.all_gather(small[:, 2 * sg :], "x", axis=1, tiled=True)
-    out_rows = from_each(out_x, "y")
+    gates = jnp.swapaxes(gates, 0, 1)
+    gates = gates.reshape(width, 2 * sg)
+    out_rows = from_each(small[:, 2 * sg :], "y")
 
     whole = jnp.moveaxis(blocks, 0, 1).reshape(rows, width)
 

time: 242 us -> 244 us (level)
  blocking collectives: 99.6 us -> 106 us
  Pallas kernels: 23.8 us -> 20.3 us
    all_gather x1, blocking collectives: 33 us -> 42.2 us  [on_device(): small = lax.all_gather(small, 'z', axis=0, tiled=True)]
    all_gather x1, blocking collectives: 12.8 us -> 9.06 us  [on_device(): out_x = lax.all_gather(out_weight.T, 'x', axis=1, tiled=True)]
    pallas_call x2, Pallas kernels: 16.4 us -> 13.3 us  [the longest x1 12.2 us: mixer(): pl.pallas_call(body, out_shape=(pltpu.VMEM((few, width), BF16), pltpu.VME...]
  transfers between devices with their start and end apart: 9 -> 9, of which waited for: 5 -> 5; matrix products, arithmetic and copies ran while one was open for 6% -> 7% of each run, Pallas kernels for 3% -> 3%
where the time goes in v6:
time: 244 us; the launch traced here: 243 us
  blocking collectives  106 us (43%)
  waiting for transfers between devices  43.5 us (18%)
  starting transfers between devices  39 us (16%)
  Pallas kernels  20.3 us (8%)
  local copies, waits for them, and re-layouts  16.3 us (7%)
  between operations  13.6 us (6%)
  matrix products  2.73 us (1%)
    all_gather x1, blocking collectives, on_device(): small = lax.all_gather(small, 'z', axis=0, tiled=True)  42.2 us
    all_to_all x3, starting transfers between devices, sent_to_all(): return lax.all_to_all(copies, axis, split_axis=0, concat_axis=0, tiled=True)  26.3 us
    all_to_all x3, waiting for transfers between devices, sent_to_all(): return lax.all_to_all(copies, axis, split_axis=0, concat_axis=0, tiled=True)  25.2 us
    all_to_all x1, blocking collectives, on_device(): lax.all_to_all(pair.reshape(chips, own_rows, width), 'x', 0, 0, tiled=True)  18.2 us
    ppermute x3, waiting for transfers between devices, from_each(): lax.ppermute(value, axis, [(i, (i + k) % size) for i in range(size)])  13.8 us
    all_to_all x1, blocking collectives, sent_to_all(): return lax.all_to_all(copies, axis, split_axis=0, concat_axis=0, tiled=True)  12.8 us
    all_gather x1, blocking collectives, on_device(): lax.all_gather(jnp.concatenate([gate_weight, up_weight, down_weight.T], a...  12.7 us
    pallas_call x1, Pallas kernels, mixer(): pl.pallas_call(body, out_shape=(pltpu.VMEM((few, width), BF16), pltpu.VME...  12.2 us
  transfers between devices with their start and end apart: 9, of which 5 were waited for; matrix products, arithmetic and copies ran while one was open for 7% of the time, Pallas kernels for 3%

profile of v6, /device:TPU:1, one launch (start us, length us, event | category | flops | bytes accessed | tf_op | source)
XLA Modules:
  0.0 243.0 jit_solution(6895955279873756747)
XLA Ops:
  7.5 12.7 %all_gather.14 = bf16[128,2112]{1,0:T(8,128)(2,1)} all-gather(bf16[32,2112]{1,0:T(8,128)(2,1)S(1)} %concatenate.15), channel_id=1, replica_groups=mesh['z'=16,'y'=4,'x'=4,'c'=2] {'y'}, dimensions={0}, use_global_device_ids=true | all-gather | bytes 675840 | tf_op jit(solution)/shard_map/all_gather | solution.py:257
  20.2 9.1 %all_gather.12 = bf16[32,512]{1,0:T(8,128)(2,1)S(1)} all-gather(bf16[32,128]{1,0:T(8,128)(2,1)} %bitcast.67), channel_id=1, replica_groups=mesh['z'=16,'y'=4,'x'=4,'c'=2] {'x'}, dimensions={1}, use_global_device_ids=true | all-gather | bytes 40960 | tf_op jit(solution)/shard_map/all_gather | solution.py:260
  30.0 42.2 %all_gather.13 = bf16[512,768]{1,0:T(8,128)(2,1)S(1)} all-gather(bf16[32,768]{1,0:T(8,128)(2,1)S(1)} %pad_maximum_fusion), channel_id=1, replica_groups=mesh['z'=16,'y'=4,'x'=4,'c'=2] {'z'}, dimensions={0}, use_global_device_ids=true | all-gather | bytes 835584 | tf_op jit(solution)/shard_map/all_gather | solution.py:263
  73.2 12.8 %all_to_all.30 = bf16[4,512,256]{2,1,0:T(8,128)(2,1)S(1)} all-to-all(bf16[4,512,256]{2,1,0:T(8,128)(2,1)S(1)} %broadcast_in_dim.20), channel_id=1, replica_groups=mesh['z'=16,'y'=4,'x'=4,'c'=2] {'y'}, dimensions={0} | all-to-all | bytes 2097152 | tf_op jit(solution)/shard_map/all_to_all | solution.py:21
  87.4 18.0 %all-to-all-start.1 = ((bf16[8,512,256]{2,1,0:T(8,128)(2,1)}), bf16[8,512,256]{2,1,0:T(8,128)(2,1)S(1)}, u32[]{:S(2)}, u32[]{:S(2)}) async-start(bf16[8,512,256]{2,1,0:T(8,128)(2,1)} %broadcast_in_dim.21), calls=%async_computation.1 | async-start | bytes 4194304 | tf_op jit(solution)/shard_map/all_to_all | solution.py:21
  106.5 25.2 %all-to-all-done.1.blocks_ref = bf16[8,512,256]{2,1,0:T(8,128)(2,1)S(1)} async-done(((bf16[8,512,256]{2,1,0:T(8,128)(2,1)}), bf16[8,512,256]{2,1,0:T(8,128)(2,1)S(1)}, u32[]{:S(2)}, u32[]{:S(2)}) %all-to-all-start.1) | async-done | bytes 2097184 | tf_op jit(solution)/shard_map/all_to_all | solution.py:21
  133.0 3.0 %copy.26 = bf16[512,8,256]{0,2,1:T(8,128)(2,1)S(1)} copy(bf16[512,8,256]{2,0,1:T(8,128)(2,1)} %bitcast.55) | data formatting | bytes 4194304 | tf_op jit(solution)/shard_map/transpose | solution.py:270
  137.2 4.2 %all-to-all-start.2 = ((f32[8,3,512]{2,1,0:T(4,128)}), f32[8,3,512]{2,1,0:T(4,128)S(1)}, u32[]{:S(2)}, u32[]{:S(2)}) async-start(f32[8,3,512]{2,1,0:T(4,128)} %broadcast_in_dim.22), calls=%async_computation.2 | async-start | bytes 131072 | tf_op jit(solution)/shard_map/all_to_all | solution.py:21
  141.4 1.9 slice.46
  143.3 2.8 %collective-permute-start.2 = (bf16[512,512]{1,0:T(8,128)(2,1)}, bf16[512,512]{1,0:T(8,128)(2,1)}, u32[]{:S(2)}, u32[]{:S(2)}) collective-permute-start(bf16[512,512]{1,0:T(8,128)(2,1)} %slice.46), channel_id=1, source_target_pairs={{0,24},{8,0},{16,8},{24,16},{1,25},{9,1},{17,9},{25,17},{2,26},{10... | collective-permute-start | bytes 1572872 | tf_op jit(solution)/shard_map/ppermute | solution.py:230
  146.1 3.1 %collective-permute-start.1 = (bf16[512,512]{1,0:T(8,128)(2,1)}, bf16[512,512]{1,0:T(8,128)(2,1)}, u32[]{:S(2)}, u32[]{:S(2)}) collective-permute-start(bf16[512,512]{1,0:T(8,128)(2,1)} %slice.46), channel_id=1, source_target_pairs={{0,16},{8,24},{16,0},{24,8},{1,17},{9,25},{17,1},{25,9},{2,18},{10... | collective-permute-start | bytes 1572872 | tf_op jit(solution)/shard_map/ppermute | solution.py:230
  149.2 1.9 collective-permute-start
  152.0 1.6 fusion
  156.3 4.2 %all-to-all-start.3 = ((bf16[4,512,128]{2,1,0:T(8,128)(2,1)}), bf16[4,512,128]{2,1,0:T(8,128)(2,1)S(1)}, u32[]{:S(2)}, u32[]{:S(2)}) async-start(bf16[4,512,128]{2,1,0:T(8,128)(2,1)} %broadcast_in_dim.24), calls=%async_computation.3 | async-start | bytes 1048576 | tf_op jit(solution)/shard_map/all_to_all | solution.py:21
  161.1 1.9 collective-permute-done.1
  163.0 11.9 %collective-permute-done = bf16[512,512]{1,0:T(8,128)(2,1)} collective-permute-done((bf16[512,512]{1,0:T(8,128)(2,1)}, bf16[512,512]{1,0:T(8,128)(2,1)}, u32[]{:S(2)}, u32[]{:S(2)}) %collective-permute-start) | collective-permute-done | bytes 524320 | tf_op jit(solution)/shard_map/ppermute | solution.py:230
  174.9 7.0 %projected.1.own_ref = bf16[512,2048]{1,0:T(8,128)(2,1)} custom-call(s32[3]{0:T(128)} %pad_add_fusion.place_ref, bf16[4,512,128]{2,1,0:T(8,128)(2,1)S(1)} %all-to-all-done.3.gated_ref, bf16[16,32,512]{2,1,0:T(8,128)(2,1)} %bitcast.23.rest_0_, bf16[16,32,512]{2,1,0:T(8,128)(2,1)} %bitcast.24.rest_1_, bf16[16,32,512]{2,1,0:T(8,128)(2,1)} %bitcast.25.rest_2_, ...), custom_call_target="tpu_custom_call" | custom-call | flops 1073741824 | bytes 6291456 | tf_op jit(solution)/shard_map/projected/pallas_call | solution.py:109
  181.9 2.6 %collective-permute-start.3 = (bf16[512,2048]{1,0:T(8,128)(2,1)}, bf16[512,2048]{1,0:T(8,128)(2,1)S(1)}, u32[]{:S(2)}, u32[]{:S(2)}) collective-permute-start(bf16[512,2048]{1,0:T(8,128)(2,1)} %projected.1.own_ref), channel_id=1, source_target_pairs={{0,1},{1,0},{2,3},{3,2},{4,5},{5,4},{6,7},{7,6},{8,9},{9,8},{10,11... | collective-permute-start | bytes 6291464 | tf_op jit(solution)/shard_map/ppermute | solution.py:25
  186.0 2.3 collective-permute-done.3.other_ref
  188.3 12.2 %mixer.1 = (bf16[64,2048]{1,0:T(8,128)(2,1)S(1)}, bf16[256,2048]{1,0:T(8,128)(2,1)S(1)}, bf16[256,2048]{1,0:T(8,128)(2,1)S(1)}) custom-call(s32[3]{0:T(128)} %pad_add_fusion.place_ref, bf16[512,2048]{1,0:T(8,128)(2,1)} %projected.1.own_ref, bf16[512,2048]{1,0:T(8,128)(2,1)S(1)} %collective-permute-done.3.other_ref, bf16[8,512,256]{2,1,0:T(8,128)(2,1)} %copy-done, ...), custom_call_target="tpu_custom_call" | custom-call | flops 4429185024 | bytes 18874368 | tf_op jit(solution)/shard_map/mixer/pallas_call | solution.py:203
  200.5 2.3 collective-permute-start.4
  202.8 2.3 collective-permute-done.4
  205.5 18.2 %all_to_all.31.pieces_ref = bf16[4,64,2048]{2,1,0:T(8,128)(2,1)S(1)} all-to-all(bf16[4,64,2048]{2,1,0:T(8,128)(2,1)S(1)} %bitcast.56), channel_id=1, replica_groups=mesh['z'=16,'y'=4,'x'=4,'c'=2] {'x'}, dimensions={0} | all-to-all | bytes 2097152 | tf_op jit(solution)/shard_map/all_to_all | solution.py:303
  224.8 10.7 %all_to_all.32 = bf16[8,64,256]{2,1,0:T(8,128)(2,1)S(1)} all-to-all(bf16[8,64,256]{2,1,0:T(8,128)(2,1)S(1)} %last_norm.1), channel_id=1, replica_groups=mesh['z'=16,'y'=4,'x'=4,'c'=2] {'x','c'}, dimensions={0} | all-to-all | bytes 524288 | tf_op jit(solution)/shard_map/all_to_all | solution.py:305
  (50 shorter events, 15.5 us)
Async XLA Ops:
  6.5 181.7 %all-gather.2.cloned.1.call-start = ((), (), s32[]{:S(2)}) async-start(), calls=%async_computation.6 | async-start | bytes 9469952 | tf_op jit(solution)/shard_map/all_gather | solution.py:258
  72.2 0.9 copy-start.2
  73.1 12.9 %copy-start.3 = (bf16[512,256]{1,0:T(8,128)(2,1)S(1)}, bf16[512,256]{1,0:T(8,128)(2,1)}, u32[]{:S(2)}) copy-start(bf16[512,256]{1,0:T(8,128)(2,1)} %param.12) | copy-start | bytes 786436
  87.4 18.0 %copy-start.5 = (f32[256]{0:T(256)S(1)}, f32[256]{0:T(256)}, u32[]{:S(2)}) copy-start(f32[256]{0:T(256)} %param.23) | copy-start | bytes 3076
  87.4 18.0 %copy-start.6 = (f32[256]{0:T(256)S(1)}, f32[256]{0:T(256)}, u32[]{:S(2)}) copy-start(f32[256]{0:T(256)} %param.19) | copy-start | bytes 3076
  87.4 44.2 %all-to-all-start.1 = ((bf16[8,512,256]{2,1,0:T(8,128)(2,1)}), bf16[8,512,256]{2,1,0:T(8,128)(2,1)S(1)}, u32[]{:S(2)}, u32[]{:S(2)}) async-start(bf16[8,512,256]{2,1,0:T(8,128)(2,1)} %broadcast_in_dim.21), calls=%async_computation.1 | async-start | bytes 4194304 | tf_op jit(solution)/shard_map/all_to_all | solution.py:21
  131.7 1.3 copy-start
  133.0 3.0 %copy-start.1 = (bf16[16,4,32,256]{3,2,1,0:T(8,128)(2,1)S(1)}, bf16[16,4,32,256]{3,2,1,0:T(8,128)(2,1)}, u32[]{:S(2)}) copy-start(bf16[16,4,32,256]{3,2,1,0:T(8,128)(2,1)} %copy.25) | copy-start | bytes 3145732
  136.0 15.8 %copy-start.7 = (f32[128]{0:T(128)S(1)}, f32[128]{0:T(128)}, u32[]{:S(2)}) copy-start(f32[128]{0:T(128)} %param.15) | copy-start | bytes 1540
  136.0 16.0 %copy-start.8 = (f32[1,128]{1,0:T(1,128)S(1)}, f32[1,128]{1,0:T(1,128)}, u32[]{:S(2)}) copy-start(f32[1,128]{1,0:T(1,128)} %param.17) | copy-start | bytes 1540
  137.2 13.9 %all-to-all-start.2 = ((f32[8,3,512]{2,1,0:T(4,128)}), f32[8,3,512]{2,1,0:T(4,128)S(1)}, u32[]{:S(2)}, u32[]{:S(2)}) async-start(f32[8,3,512]{2,1,0:T(4,128)} %broadcast_in_dim.22), calls=%async_computation.2 | async-start | bytes 131072 | tf_op jit(solution)/shard_map/all_to_all | solution.py:21
  143.3 17.8 %collective-permute-start.2 = (bf16[512,512]{1,0:T(8,128)(2,1)}, bf16[512,512]{1,0:T(8,128)(2,1)}, u32[]{:S(2)}, u32[]{:S(2)}) collective-permute-start(bf16[512,512]{1,0:T(8,128)(2,1)} %slice.46), channel_id=1, source_target_pairs={{0,24},{8,0},{16,8},{24,16},{1,25},{9,1},{17,9},{25,17},{2,26},{10... | collective-permute-start | bytes 1572872 | tf_op jit(solution)/shard_map/ppermute | solution.py:230
  146.1 16.9 %collective-permute-start.1 = (bf16[512,512]{1,0:T(8,128)(2,1)}, bf16[512,512]{1,0:T(8,128)(2,1)}, u32[]{:S(2)}, u32[]{:S(2)}) collective-permute-start(bf16[512,512]{1,0:T(8,128)(2,1)} %slice.46), channel_id=1, source_target_pairs={{0,16},{8,24},{16,0},{24,8},{1,17},{9,25},{17,1},{25,9},{2,18},{10... | collective-permute-start | bytes 1572872 | tf_op jit(solution)/shard_map/ppermute | solution.py:230
  149.2 25.7 %collective-permute-start = (bf16[512,512]{1,0:T(8,128)(2,1)}, bf16[512,512]{1,0:T(8,128)(2,1)}, u32[]{:S(2)}, u32[]{:S(2)}) collective-permute-start(bf16[512,512]{1,0:T(8,128)(2,1)} %slice.46), channel_id=1, source_target_pairs={{0,8},{8,16},{16,24},{24,0},{1,9},{9,17},{17,25},{25,1},{2,10},{10... | collective-permute-start | bytes 1572872 | tf_op jit(solution)/shard_map/ppermute | solution.py:230
  151.1 0.6 copy-start.4
  156.3 18.6 %all-to-all-start.3 = ((bf16[4,512,128]{2,1,0:T(8,128)(2,1)}), bf16[4,512,128]{2,1,0:T(8,128)(2,1)S(1)}, u32[]{:S(2)}, u32[]{:S(2)}) async-start(bf16[4,512,128]{2,1,0:T(8,128)(2,1)} %broadcast_in_dim.24), calls=%async_computation.3 | async-start | bytes 1048576 | tf_op jit(solution)/shard_map/all_to_all | solution.py:21
  181.9 6.4 %collective-permute-start.3 = (bf16[512,2048]{1,0:T(8,128)(2,1)}, bf16[512,2048]{1,0:T(8,128)(2,1)S(1)}, u32[]{:S(2)}, u32[]{:S(2)}) collective-permute-start(bf16[512,2048]{1,0:T(8,128)(2,1)} %projected.1.own_ref), channel_id=1, source_target_pairs={{0,1},{1,0},{2,3},{3,2},{4,5},{5,4},{6,7},{7,6},{8,9},{9,8},{10,11... | collective-permute-start | bytes 6291464 | tf_op jit(solution)/shard_map/ppermute | solution.py:25
  200.5 4.6 %collective-permute-start.4 = (bf16[256,2048]{1,0:T(8,128)(2,1)S(1)}, bf16[256,2048]{1,0:T(8,128)(2,1)S(1)}, u32[]{:S(2)}, u32[]{:S(2)}) collective-permute-start(bf16[256,2048]{1,0:T(8,128)(2,1)S(1)} %get-tuple-element.9), channel_id=1, source_target_pairs={{0,1},{1,0},{2,3},{3,2},{4,5},{5,4},{6,7},{7,6},{8,9},{9,8},{10,11... | collective-permute-start | bytes 3145736 | tf_op jit(solution)/shard_map/ppermute | solution.py:25
Sparse Core Ops, SparseCore 0:
  20.3 124.6 all-gather.1

commit v7 on v6

--- a/solution.py
+++ b/solution.py
@@ -69,8 +69,7 @@
     chips, rows, channels = gated.shape
     peers = len(pieces)
     depth = 32
-    zs = pieces[0].shape[0] // depth
-    wide = pieces[0].shape[1]
+    zs = pieces[0].shape[0] // chips // depth
     width = zs * peers * depth
     steps = 8
     deep = zs // steps
@@ -87,7 +86,7 @@
             some = []
             for n in range(peers):
                 at_y = lax.rem(y + peers - n, peers)
-                some.append(pltpu.make_async_copy(pieces[n].at[at_z], weights.at[at_z, at_y], sems.at[j, n]))
+                some.append(pltpu.make_async_copy(pieces[n].at[:, at_z], weights.at[:, at_z, at_y], sems.at[j, n]))
             copies.append(some)
         for some in copies[:ahead]:
             for c in some:
@@ -100,11 +99,12 @@
             if j + ahead < steps:
                 for c in copies[j + ahead]:
                     c.start()
-            right = weights[j * deep : (j + 1) * deep].reshape(span, wide)
+            right = [weights[k, j * deep : (j + 1) * deep].reshape(span, channels) for k in range(chips)]
+            right = jnp.concatenate(right, axis=1)
             part = lax.dot_general(left[...], right, ACROSS, preferred_element_type=F32)
             out_ref[:, j * span : (j + 1) * span] = part.astype(BF16)
 
-    given = [p.reshape(zs, depth, wide) for p in pieces]
+    given = [p.reshape(chips, zs, depth, channels) for p in pieces]
     anywhere = pl.BlockSpec(memory_space=pl.ANY)
     return pl.pallas_call(
         body,
@@ -112,11 +112,11 @@
         in_specs=[pl.BlockSpec(memory_space=pltpu.SMEM), whole_vmem()] + [anywhere] * peers,
         out_specs=whole_vmem(),
         scratch_shapes=[
-            pltpu.VMEM((zs, peers, depth, wide), BF16),
+            pltpu.VMEM((chips, zs, peers, depth, channels), BF16),
             pltpu.VMEM((rows, chips * channels), BF16),
             pltpu.SemaphoreType.DMA((steps, peers)),
         ],
-        cost_estimate=pl.CostEstimate(flops=2 * rows * width * wide, bytes_accessed=6 << 20, transcendentals=0),
+        cost_estimate=pl.CostEstimate(flops=2 * rows * width * chips * channels, bytes_accessed=6 << 20, transcendentals=0),
         name="projected",
     )(in_hbm(place), in_vmem(gated), *given)
 
@@ -257,15 +257,14 @@
     ffw = lax.all_gather(jnp.concatenate([gate_weight, up_weight, down_weight.T], axis=1), "y", axis=0, tiled=True)
     ffw = lax.all_gather(ffw, "z", axis=0, tiled=True)
 
-    out_x = lax.all_gather(out_weight.T, "x", axis=1, tiled=True)
-    small = jnp.concatenate([u_weight, v_weight, out_x], axis=1)
+    small = jnp.concatenate([u_weight, v_weight, out_weight.T], axis=1)
     depth = small.shape[0]
     small = lax.all_gather(small, "z", axis=0, tiled=True)
     gates = sent_to_all(small[:, : 2 * sg], "y")
     gates = gates.reshape(gates.shape[0], -1, depth, 2 * sg)
-    gates = jnp.swapaxes(gates, 0, 1)
-    gates = gates.reshape(width, 2 * sg)
-    out_rows = from_each(small[:, 2 * sg :], "y")
+    gates = jnp.swapaxes(gates, 0, 1).reshape(width, 2 * sg)
+    out_x = lax.all_gather(small[:, 2 * sg :], "x", axis=0, tiled=True)
+    out_rows = from_each(out_x, "y")
 
     whole = jnp.moveaxis(blocks, 0, 1).reshape(rows, width)
 

time: 244 us -> 233 us (0.955)
  blocking collectives: 106 us -> 98 us
  local copies, waits for them, and re-layouts: 16.3 us -> 12.9 us
    all_gather x1, blocking collectives: 42.2 us -> 33 us  [on_device(): small = lax.all_gather(small, 'z', axis=0, tiled=True)]
    all_gather x1, blocking collectives: 9.06 us -> 12.2 us  [on_device(): out_x = lax.all_gather(small[:, 2 * sg:], 'x', axis=0, tiled=True)]
  transfers between devices with their start and end apart: 9 -> 9, of which waited for: 5 -> 5; matrix products, arithmetic and copies ran while one was open for 7% -> 6% of each run, Pallas kernels for 3% -> 3%
where the time goes in v7:
time: 233 us; the launch traced here: 232 us
  blocking collectives  98 us (42%)
  waiting for transfers between devices  43.9 us (19%)
  starting transfers between devices  38.1 us (16%)
  Pallas kernels  20.3 us (9%)
  between operations  13.7 us (6%)
  local copies, waits for them, and re-layouts  12.9 us (6%)
  other arithmetic  2.75 us (1%)
  matrix products  2.73 us (1%)
    all_gather x1, blocking collectives, on_device(): small = lax.all_gather(small, 'z', axis=0, tiled=True)  33 us
    all_to_all x3, starting transfers between devices, sent_to_all(): return lax.all_to_all(copies, axis, split_axis=0, concat_axis=0, tiled=True)  25.5 us
    all_to_all x3, waiting for transfers between devices, sent_to_all(): return lax.all_to_all(copies, axis, split_axis=0, concat_axis=0, tiled=True)  25.1 us
    all_to_all x1, blocking collectives, on_device(): lax.all_to_all(pair.reshape(chips, own_rows, width), 'x', 0, 0, tiled=True)  17.2 us
    ppermute x3, waiting for transfers between devices, from_each(): lax.ppermute(value, axis, [(i, (i + k) % size) for i in range(size)])  14.3 us
    all_gather x1, blocking collectives, on_device(): lax.all_gather(jnp.concatenate([gate_weight, up_weight, down_weight.T], a...  12.7 us
    pallas_call x1, Pallas kernels, mixer(): pl.pallas_call(body, out_shape=(pltpu.VMEM((few, width), BF16), pltpu.VME...  12.2 us
    all_to_all x1, blocking collectives, sent_to_all(): return lax.all_to_all(copies, axis, split_axis=0, concat_axis=0, tiled=True)  12.2 us
  transfers between devices with their start and end apart: 9, of which 5 were waited for; matrix products, arithmetic and copies ran while one was open for 6% of the time, Pallas kernels for 3%

profile of v7, /device:TPU:1, one launch (start us, length us, event | category | flops | bytes accessed | tf_op | source)
XLA Modules:
  0.0 232.4 jit_solution(12663423006368662782)
XLA Ops:
  7.5 12.7 %all_gather.14 = bf16[128,2112]{1,0:T(8,128)(2,1)} all-gather(bf16[32,2112]{1,0:T(8,128)(2,1)S(1)} %concatenate.15), channel_id=1, replica_groups=mesh['z'=16,'y'=4,'x'=4,'c'=2] {'y'}, dimensions={0}, use_global_device_ids=true | all-gather | bytes 675840 | tf_op jit(solution)/shard_map/all_gather | solution.py:257
  20.9 33.0 %all_gather.12 = bf16[512,384]{1,0:T(8,128)(2,1)S(1)} all-gather(bf16[32,384]{1,0:T(8,128)(2,1)S(1)} %pad_maximum_fusion), channel_id=1, replica_groups=mesh['z'=16,'y'=4,'x'=4,'c'=2] {'z'}, dimensions={0}, use_global_device_ids=true | all-gather | bytes 417792 | tf_op jit(solution)/shard_map/all_gather | solution.py:262
  54.1 12.2 %all_to_all.30 = bf16[4,512,256]{2,1,0:T(8,128)(2,1)S(1)} all-to-all(bf16[4,512,256]{2,1,0:T(8,128)(2,1)S(1)} %broadcast_in_dim.20), channel_id=1, replica_groups=mesh['z'=16,'y'=4,'x'=4,'c'=2] {'y'}, dimensions={0} | all-to-all | bytes 2097152 | tf_op jit(solution)/shard_map/all_to_all | solution.py:21
  66.3 1.5 broadcast_in_dim.21
  67.7 17.2 %all-to-all-start.1 = ((bf16[8,512,256]{2,1,0:T(8,128)(2,1)}), bf16[8,512,256]{2,1,0:T(8,128)(2,1)S(1)}, u32[]{:S(2)}, u32[]{:S(2)}) async-start(bf16[8,512,256]{2,1,0:T(8,128)(2,1)} %broadcast_in_dim.21), calls=%async_computation.1 | async-start | bytes 4194304 | tf_op jit(solution)/shard_map/all_to_all | solution.py:21
  86.0 25.1 %all-to-all-done.1.blocks_ref = bf16[8,512,256]{2,1,0:T(8,128)(2,1)S(1)} async-done(((bf16[8,512,256]{2,1,0:T(8,128)(2,1)}), bf16[8,512,256]{2,1,0:T(8,128)(2,1)S(1)}, u32[]{:S(2)}, u32[]{:S(2)}) %all-to-all-start.1) | async-done | bytes 2097184 | tf_op jit(solution)/shard_map/all_to_all | solution.py:21
  111.1 1.3 copy-done
  112.4 3.0 %copy.26 = bf16[512,8,256]{0,2,1:T(8,128)(2,1)S(1)} copy(bf16[512,8,256]{2,0,1:T(8,128)(2,1)} %bitcast.55) | data formatting | bytes 4194304 | tf_op jit(solution)/shard_map/transpose | solution.py:269
  116.7 4.8 %all-to-all-start.2 = ((f32[8,3,512]{2,1,0:T(4,128)}), f32[8,3,512]{2,1,0:T(4,128)}, u32[]{:S(2)}, u32[]{:S(2)}) async-start(f32[8,3,512]{2,1,0:T(4,128)} %broadcast_in_dim.22), calls=%async_computation.2 | async-start | bytes 131072 | tf_op jit(solution)/shard_map/all_to_all | solution.py:21
  121.5 12.2 %all_gather.13 = bf16[2048,128]{1,0:T(8,128)(2,1)} all-gather(bf16[512,128]{1,0:T(8,128)(2,1)S(1)} %slice-done), channel_id=1, replica_groups=mesh['z'=16,'y'=4,'x'=4,'c'=2] {'x'}, dimensions={0}, use_global_device_ids=true | all-gather | bytes 655360 | tf_op jit(solution)/shard_map/all_gather | solution.py:266
  133.7 2.8 %collective-permute-start.2 = (bf16[2048,128]{1,0:T(8,128)(2,1)}, bf16[2048,128]{1,0:T(8,128)(2,1)}, u32[]{:S(2)}, u32[]{:S(2)}) collective-permute-start(bf16[2048,128]{1,0:T(8,128)(2,1)} %all_gather.13), channel_id=1, source_target_pairs={{0,24},{8,0},{16,8},{24,16},{1,25},{9,1},{17,9},{25,17},{2,26},{10... | collective-permute-start | bytes 1572872 | tf_op jit(solution)/shard_map/ppermute | solution.py:230
  136.5 3.1 %collective-permute-start.1 = (bf16[2048,128]{1,0:T(8,128)(2,1)}, bf16[2048,128]{1,0:T(8,128)(2,1)}, u32[]{:S(2)}, u32[]{:S(2)}) collective-permute-start(bf16[2048,128]{1,0:T(8,128)(2,1)} %all_gather.13), channel_id=1, source_target_pairs={{0,16},{8,24},{16,0},{24,8},{1,17},{9,25},{17,1},{25,9},{2,18},{10... | collective-permute-start | bytes 1572872 | tf_op jit(solution)/shard_map/ppermute | solution.py:230
  139.6 1.9 collective-permute-start
  142.6 1.6 fusion
  146.9 3.5 %all-to-all-start.3 = ((bf16[4,512,128]{2,1,0:T(8,128)(2,1)}), bf16[4,512,128]{2,1,0:T(8,128)(2,1)S(1)}, u32[]{:S(2)}, u32[]{:S(2)}) async-start(bf16[4,512,128]{2,1,0:T(8,128)(2,1)} %broadcast_in_dim.24), calls=%async_computation.3 | async-start | bytes 1048576 | tf_op jit(solution)/shard_map/all_to_all | solution.py:21
  151.2 14.1 %collective-permute-done = bf16[2048,128]{1,0:T(8,128)(2,1)} collective-permute-done((bf16[2048,128]{1,0:T(8,128)(2,1)}, bf16[2048,128]{1,0:T(8,128)(2,1)}, u32[]{:S(2)}, u32[]{:S(2)}) %collective-permute-start) | collective-permute-done | bytes 524320 | tf_op jit(solution)/shard_map/ppermute | solution.py:230
  165.3 7.0 %projected.1.own_ref = bf16[512,2048]{1,0:T(8,128)(2,1)} custom-call(s32[3]{0:T(128)} %pad_add_fusion.place_ref, bf16[4,512,128]{2,1,0:T(8,128)(2,1)S(1)} %all-to-all-done.3.gated_ref, bf16[4,16,32,128]{3,2,1,0:T(8,128)(2,1)} %bitcast.23.rest_0_, bf16[4,16,32,128]{3,2,1,0:T(8,128)(2,1)} %bitcast.24.rest_1_, bf16[4,16,32,128]{3,2,1,0:T(8,128)(2,1)} %bitcast.25.rest_2_, ...), custom_call_target="tpu_custom_call" | custom-call | flops 1073741824 | bytes 6291456 | tf_op jit(solution)/shard_map/projected/pallas_call | solution.py:109
  172.3 2.6 %collective-permute-start.3 = (bf16[512,2048]{1,0:T(8,128)(2,1)}, bf16[512,2048]{1,0:T(8,128)(2,1)S(1)}, u32[]{:S(2)}, u32[]{:S(2)}) collective-permute-start(bf16[512,2048]{1,0:T(8,128)(2,1)} %projected.1.own_ref), channel_id=1, source_target_pairs={{0,1},{1,0},{2,3},{3,2},{4,5},{5,4},{6,7},{7,6},{8,9},{9,8},{10,11... | collective-permute-start | bytes 6291464 | tf_op jit(solution)/shard_map/ppermute | solution.py:25
  176.4 2.3 collective-permute-done.3.other_ref
  178.7 12.2 %mixer.1 = (bf16[64,2048]{1,0:T(8,128)(2,1)S(1)}, bf16[256,2048]{1,0:T(8,128)(2,1)S(1)}, bf16[256,2048]{1,0:T(8,128)(2,1)S(1)}) custom-call(s32[3]{0:T(128)} %pad_add_fusion.place_ref, bf16[512,2048]{1,0:T(8,128)(2,1)} %projected.1.own_ref, bf16[512,2048]{1,0:T(8,128)(2,1)S(1)} %collective-permute-done.3.other_ref, bf16[8,512,256]{2,1,0:T(8,128)(2,1)} %copy-done, ...), custom_call_target="tpu_custom_call" | custom-call | flops 4429185024 | bytes 18874368 | tf_op jit(solution)/shard_map/mixer/pallas_call | solution.py:203
  190.9 2.3 collective-permute-start.4
  193.2 2.3 collective-permute-done.4
  195.9 17.2 %all_to_all.31.pieces_ref = bf16[4,64,2048]{2,1,0:T(8,128)(2,1)S(1)} all-to-all(bf16[4,64,2048]{2,1,0:T(8,128)(2,1)S(1)} %bitcast.56), channel_id=1, replica_groups=mesh['z'=16,'y'=4,'x'=4,'c'=2] {'x'}, dimensions={0} | all-to-all | bytes 2097152 | tf_op jit(solution)/shard_map/all_to_all | solution.py:302
  214.2 10.7 %all_to_all.32 = bf16[8,64,256]{2,1,0:T(8,128)(2,1)S(1)} all-to-all(bf16[8,64,256]{2,1,0:T(8,128)(2,1)S(1)} %last_norm.1), channel_id=1, replica_groups=mesh['z'=16,'y'=4,'x'=4,'c'=2] {'x','c'}, dimensions={0} | all-to-all | bytes 524288 | tf_op jit(solution)/shard_map/all_to_all | solution.py:304
  (49 shorter events, 12.4 us)
Async XLA Ops:
  6.5 172.2 %all-gather.2.cloned.1.call-start = ((), (), s32[]{:S(2)}) async-start(), calls=%async_computation.6 | async-start | bytes 9469952 | tf_op jit(solution)/shard_map/all_gather | solution.py:258
  20.9 45.3 %copy-start.3 = (bf16[512,256]{1,0:T(8,128)(2,1)S(1)}, bf16[512,256]{1,0:T(8,128)(2,1)}, u32[]{:S(2)}) copy-start(bf16[512,256]{1,0:T(8,128)(2,1)} %param.12) | copy-start | bytes 786436
  53.9 30.9 %copy-start.2 = (bf16[512,384]{1,0:T(8,128)(2,1)}, bf16[512,384]{1,0:T(8,128)(2,1)S(1)}, u32[]{:S(2)}) copy-start(bf16[512,384]{1,0:T(8,128)(2,1)S(1)} %all_gather.12) | copy-start | bytes 1179652
  67.7 17.2 %copy-start.4 = (f32[256]{0:T(256)S(1)}, f32[256]{0:T(256)}, u32[]{:S(2)}) copy-start(f32[256]{0:T(256)} %param.23) | copy-start | bytes 3076
  67.7 17.2 %copy-start.5 = (f32[256]{0:T(256)S(1)}, f32[256]{0:T(256)}, u32[]{:S(2)}) copy-start(f32[256]{0:T(256)} %param.19) | copy-start | bytes 3076
  67.7 43.4 %all-to-all-start.1 = ((bf16[8,512,256]{2,1,0:T(8,128)(2,1)}), bf16[8,512,256]{2,1,0:T(8,128)(2,1)S(1)}, u32[]{:S(2)}, u32[]{:S(2)}) async-start(bf16[8,512,256]{2,1,0:T(8,128)(2,1)} %broadcast_in_dim.21), calls=%async_computation.1 | async-start | bytes 4194304 | tf_op jit(solution)/shard_map/all_to_all | solution.py:21
  111.1 1.3 copy-start
  112.4 3.0 %copy-start.1 = (bf16[16,4,32,256]{3,2,1,0:T(8,128)(2,1)S(1)}, bf16[16,4,32,256]{3,2,1,0:T(8,128)(2,1)}, u32[]{:S(2)}) copy-start(bf16[16,4,32,256]{3,2,1,0:T(8,128)(2,1)} %copy.25) | copy-start | bytes 3145732
  115.4 6.1 %slice-start = ((bf16[512,384]{1,0:T(8,128)(2,1)}), bf16[512,128]{1,0:T(8,128)(2,1)S(1)}, s32[]{:S(2)}) async-start(bf16[512,384]{1,0:T(8,128)(2,1)} %copy-done.2), calls=%async_computation.7 | async-start | bytes 262144 | tf_op jit(solution)/shard_map/slice | solution.py:266
  115.4 27.0 %copy-start.6 = (f32[128]{0:T(128)S(1)}, f32[128]{0:T(128)}, u32[]{:S(2)}) copy-start(f32[128]{0:T(128)} %param.15) | copy-start | bytes 1540
  115.4 27.2 %copy-start.7 = (f32[1,128]{1,0:T(1,128)S(1)}, f32[1,128]{1,0:T(1,128)}, u32[]{:S(2)}) copy-start(f32[1,128]{1,0:T(1,128)} %param.17) | copy-start | bytes 1540
  116.7 24.8 %all-to-all-start.2 = ((f32[8,3,512]{2,1,0:T(4,128)}), f32[8,3,512]{2,1,0:T(4,128)}, u32[]{:S(2)}, u32[]{:S(2)}) async-start(f32[8,3,512]{2,1,0:T(4,128)} %broadcast_in_dim.22), calls=%async_computation.2 | async-start | bytes 131072 | tf_op jit(solution)/shard_map/all_to_all | solution.py:21
  133.7 17.3 %collective-permute-start.2 = (bf16[2048,128]{1,0:T(8,128)(2,1)}, bf16[2048,128]{1,0:T(8,128)(2,1)}, u32[]{:S(2)}, u32[]{:S(2)}) collective-permute-start(bf16[2048,128]{1,0:T(8,128)(2,1)} %all_gather.13), channel_id=1, source_target_pairs={{0,24},{8,0},{16,8},{24,16},{1,25},{9,1},{17,9},{25,17},{2,26},{10... | collective-permute-start | bytes 1572872 | tf_op jit(solution)/shard_map/ppermute | solution.py:230
  136.5 14.7 %collective-permute-start.1 = (bf16[2048,128]{1,0:T(8,128)(2,1)}, bf16[2048,128]{1,0:T(8,128)(2,1)}, u32[]{:S(2)}, u32[]{:S(2)}) collective-permute-start(bf16[2048,128]{1,0:T(8,128)(2,1)} %all_gather.13), channel_id=1, source_target_pairs={{0,16},{8,24},{16,0},{24,8},{1,17},{9,25},{17,1},{25,9},{2,18},{10... | collective-permute-start | bytes 1572872 | tf_op jit(solution)/shard_map/ppermute | solution.py:230
  139.6 25.7 %collective-permute-start = (bf16[2048,128]{1,0:T(8,128)(2,1)}, bf16[2048,128]{1,0:T(8,128)(2,1)}, u32[]{:S(2)}, u32[]{:S(2)}) collective-permute-start(bf16[2048,128]{1,0:T(8,128)(2,1)} %all_gather.13), channel_id=1, source_target_pairs={{0,8},{8,16},{16,24},{24,0},{1,9},{9,17},{17,25},{25,1},{2,10},{10... | collective-permute-start | bytes 1572872 | tf_op jit(solution)/shard_map/ppermute | solution.py:230
  146.9 18.4 %all-to-all-start.3 = ((bf16[4,512,128]{2,1,0:T(8,128)(2,1)}), bf16[4,512,128]{2,1,0:T(8,128)(2,1)S(1)}, u32[]{:S(2)}, u32[]{:S(2)}) async-start(bf16[4,512,128]{2,1,0:T(8,128)(2,1)} %broadcast_in_dim.24), calls=%async_computation.3 | async-start | bytes 1048576 | tf_op jit(solution)/shard_map/all_to_all | solution.py:21
  172.3 6.4 %collective-permute-start.3 = (bf16[512,2048]{1,0:T(8,128)(2,1)}, bf16[512,2048]{1,0:T(8,128)(2,1)S(1)}, u32[]{:S(2)}, u32[]{:S(2)}) collective-permute-start(bf16[512,2048]{1,0:T(8,128)(2,1)} %projected.1.own_ref), channel_id=1, source_target_pairs={{0,1},{1,0},{2,3},{3,2},{4,5},{5,4},{6,7},{7,6},{8,9},{9,8},{10,11... | collective-permute-start | bytes 6291464 | tf_op jit(solution)/shard_map/ppermute | solution.py:25
  190.9 4.6 %collective-permute-start.4 = (bf16[256,2048]{1,0:T(8,128)(2,1)S(1)}, bf16[256,2048]{1,0:T(8,128)(2,1)S(1)}, u32[]{:S(2)}, u32[]{:S(2)}) collective-permute-start(bf16[256,2048]{1,0:T(8,128)(2,1)S(1)} %get-tuple-element.9), channel_id=1, source_target_pairs={{0,1},{1,0},{2,3},{3,2},{4,5},{5,4},{6,7},{7,6},{8,9},{9,8},{10,11... | collective-permute-start | bytes 3145736 | tf_op jit(solution)/shard_map/ppermute | solution.py:25
Sparse Core Ops, SparseCore 0:
  20.3 119.2 all-gather.1

commit v8 on v7

--- a/solution.py
+++ b/solution.py
@@ -63,6 +63,95 @@
         out_specs=whole_vmem(),
         name="last_norm",
     )(in_vmem(pieces), in_vmem(base), gain.reshape(1, width))
+
+
+def branches(blocks, gates, gains):
+    parts, rows, feats = blocks.shape
+    ys, deep, columns = gates.shape
+    width = parts * feats
+    half = columns // 2
+    depth = 32
+
+    def body(blocks_ref, gates_ref, gains_ref, gated_ref, valued_ref, sums_ref, left, right, sems):
+        copies = []
+        for k in range(parts):
+            copies.append(pltpu.make_async_copy(blocks_ref.at[k], left.at[:, pl.ds(k * feats, feats)], sems.at[k]))
+            copies[k].start()
+        for z in range(deep // depth):
+            for y in range(ys):
+                at = (z * ys + y) * depth
+                right[at : at + depth] = gates_ref[y, z * depth : (z + 1) * depth]
+        for c in copies:
+            c.wait()
+        both = jnp.dot(left[...], right[...], preferred_element_type=F32)
+        gated_ref[...] = jax.nn.gelu(both[:, :half])
+        valued = jax.nn.gelu(both[:, half:])
+        valued_ref[...] = valued
+        turned = valued.T
+        total = jnp.sum(turned, axis=0, keepdims=True)
+        squares = jnp.sum(turned * turned, axis=0, keepdims=True)
+        for k in range(parts):
+            sums_ref[k, 0:1] = total
+            sums_ref[k, 1:2] = squares
+            sums_ref[k, 2:3] = gains_ref[...]
+            sums_ref[k, 3:4] = gains_ref[...]
+
+    return pl.pallas_call(
+        body,
+        out_shape=(
+            pltpu.VMEM((rows, half), F32),
+            pltpu.VMEM((rows, half), F32),
+            pltpu.VMEM((parts, 4, rows), F32),
+        ),
+        in_specs=[pl.BlockSpec(memory_space=pltpu.HBM), whole_vmem(), whole_vmem()],
+        out_specs=(whole_vmem(),) * 3,
+        scratch_shapes=[
+            pltpu.VMEM((rows, width), BF16),
+            pltpu.VMEM((width, columns), BF16),
+            pltpu.SemaphoreType.DMA((parts,)),
+        ],
+        compiler_params=pltpu.CompilerParams(vmem_limit_bytes=24 << 20),
+        cost_estimate=pl.CostEstimate(flops=2 * rows * width * columns, bytes_accessed=4 << 20, transcendentals=2 * rows * columns),
+        name="branches",
+    )(in_hbm(blocks), in_vmem(gates), gains)
+
+
+def gated_copies(known, gated, valued, gain, weight, bias, copies):
+    parts, _, rows = known.shape
+    channels = gated.shape[1]
+    block = weight.shape[1]
+    count = parts * channels
+
+    def body(known_ref, gated_ref, valued_ref, gain_ref, weight_ref, bias_ref, out_ref):
+        sums = known_ref[0]
+        for k in range(1, parts):
+            sums = sums + known_ref[k]
+        mean = sums[0:1] / count
+        square = sums[1:2] / count
+        scale = lax.rsqrt(square - mean * mean + EPS)
+        mean = jnp.broadcast_to(mean, (channels, rows)).T
+        scale = jnp.broadcast_to(scale, (channels, rows)).T
+        normed = ((valued_ref[...] - mean) * scale * gain_ref[...]).astype(BF16)
+        row = lax.broadcasted_iota(jnp.int32, (block, block), 0)
+        column = lax.broadcasted_iota(jnp.int32, (block, block), 1)
+        masked = jnp.where(row >= column, weight_ref[0].astype(F32), 0.0).astype(BF16)
+        offset = jnp.broadcast_to(bias_ref[...], (channels, block)).T
+        for n in range(rows // block):
+            at = slice(n * block, (n + 1) * block)
+            mixed = jnp.dot(masked, normed[at], preferred_element_type=F32) + offset
+            done = (gated_ref[at] * mixed).astype(BF16)
+            for k in range(copies):
+                out_ref[k, at] = done
+
+    return pl.pallas_call(
+        body,
+        out_shape=pltpu.VMEM((copies, rows, channels), BF16),
+        in_specs=[whole_vmem()] * 6,
+        out_specs=whole_vmem(),
+        compiler_params=pltpu.CompilerParams(vmem_limit_bytes=12 << 20),
+        cost_estimate=pl.CostEstimate(flops=2 * rows * block * channels, bytes_accessed=2 << 20, transcendentals=rows),
+        name="gated_copies",
+    )(in_vmem(known), in_vmem(gated), in_vmem(valued), gain.reshape(1, channels), weight, bias)
 
 
 def projected(place, gated, pieces):
@@ -130,7 +219,7 @@
     edges = [0, 384, 768, 1152, 2 * ff, 3 * ff]
     spans = [e - b for b, e in zip(edges, edges[1:])]
     chunks = len(spans)
-    ahead = 2
+    ahead = 3
     step = 256
 
     def body(place_ref, own_ref, other_ref, blocks_ref, gain_ref, ffw_ref, mine_ref, keep_ref, give_ref, *rest):
@@ -258,43 +347,19 @@
     ffw = lax.all_gather(ffw, "z", axis=0, tiled=True)
 
     small = jnp.concatenate([u_weight, v_weight, out_weight.T], axis=1)
-    depth = small.shape[0]
     small = lax.all_gather(small, "z", axis=0, tiled=True)
     gates = sent_to_all(small[:, : 2 * sg], "y")
-    gates = gates.reshape(gates.shape[0], -1, depth, 2 * sg)
-    gates = jnp.swapaxes(gates, 0, 1).reshape(width, 2 * sg)
     out_x = lax.all_gather(small[:, 2 * sg :], "x", axis=0, tiled=True)
     out_rows = from_each(out_x, "y")
 
-    whole = jnp.moveaxis(blocks, 0, 1).reshape(rows, width)
-
-    pre_u = jnp.dot(whole, gates[:, :sg], preferred_element_type=F32)
-    pre_v = jnp.dot(whole, gates[:, sg:], preferred_element_type=F32)
-    gated = jax.nn.gelu(pre_u)
-    valued = jax.nn.gelu(pre_v)
-    sums = jnp.stack([jnp.sum(valued, axis=1), jnp.sum(valued * valued, axis=1)])
-    gains = jnp.concatenate([gain_one, gain_two]).reshape(-1, rows)
-    known = sent_to_all(jnp.concatenate([sums, gains], axis=0), TP)
-    gains = known[:, 2:].reshape(parts, 2, feats)
+    gains = jnp.concatenate([gain_one, gain_two]).reshape(1, rows)
+    gated, valued, sums = branches(blocks, gates, gains)
+    known = lax.all_to_all(sums, TP, 0, 0, tiled=True)
+    gains = known[:, 2].reshape(parts, 2, feats)
     gain_1 = gains[:, 0].reshape(width)
     gain_2 = gains[:, 1].reshape(width)
-    sums = jnp.sum(known[:, :2], axis=0)
-    count = sg * parts
-    mean = sums[0][:, None] / count
-    square = sums[1][:, None] / count
-    normed = (valued - mean) * lax.rsqrt(square - mean * mean + EPS) * sg_gain[None, :]
-    normed = normed.astype(BF16)
-
-    groups = spatial_weight.shape[0]
-    block = spatial_weight.shape[1]
-    shaped = normed.reshape(rows // block, block, groups, sg // groups)
-    lower = jnp.tril(jnp.ones((block, block), jnp.bool_))
-    masked = jnp.where(lower[None], spatial_weight, jnp.zeros_like(spatial_weight))
-    mixed = jnp.einsum("gij,njgd->nigd", masked, shaped, preferred_element_type=F32)
-    mixed = mixed + spatial_bias.T[None, :, :, None]
-    gated_out = (gated * mixed.reshape(rows, sg)).astype(BF16)
-
-    together = sent_to_all(gated_out, "x")
+    copies = gated_copies(known, gated, valued, sg_gain, spatial_weight, spatial_bias, chips)
+    together = lax.all_to_all(copies, "x", 0, 0, tiled=True)
     place = jnp.stack([core, lax.axis_index(TP), lax.axis_index("y")]).astype(jnp.int32)
     own = projected(place, together, out_rows)
     mine, keep, give = mixer(place, own, to_partner(own), blocks, gain_1, ffw, gate_weight.shape[1])

time: 233 us -> 224 us (0.961)
  blocking collectives: 98 us -> 129 us
  waiting for transfers between devices: 43.9 us -> 14.1 us
  local copies, waits for them, and re-layouts: 12.9 us -> 5.95 us
  starting transfers between devices: 38.1 us -> 33.9 us
  Pallas kernels: 20.3 us -> 24.2 us
  matrix products: 2.73 us -> 0 us
    all_to_all x3 -> x1, waiting for transfers between devices: 25.1 us -> 0.01 us  [sent_to_all(): return lax.all_to_all(copies, axis, split_axis=0, concat_axis=0, tiled=True)]
    all_gather x1, blocking collectives: 12.2 us -> 33.8 us  [on_device(): out_x = lax.all_gather(small[:, 2 * sg:], 'x', axis=0, tiled=True)]
    all_to_all x0 -> x1, blocking collectives: none -> 10.2 us  [on_device(): known = lax.all_to_all(sums, TP, 0, 0, tiled=True)]
    ppermute x3, waiting for transfers between devices: 14.3 us -> 4.43 us  [from_each(): lax.ppermute(value, axis, [(i, (i + k) % size) for i in range(size)])]
    all_to_all x3 -> x1, starting transfers between devices: 25.5 us -> 17.2 us  [sent_to_all(): return lax.all_to_all(copies, axis, split_axis=0, concat_axis=0, tiled=True)]
    all_to_all x0 -> x1, waiting for transfers between devices: none -> 4.14 us  [on_device(): together = lax.all_to_all(copies, 'x', 0, 0, tiled=True)]
    transpose x2 -> x0, local copies, waits for them, and re-layouts: 4.05 us -> none  [the longest x1 2.97 us: on_device(): whole = jnp.moveaxis(blocks, 0, 1).reshape(rows, width)]
    pallas_call x0 -> x2, Pallas kernels: none -> 3.64 us  [the longest x1 2.46 us: branches(): pl.pallas_call(body, out_shape=(pltpu.VMEM((rows, half), F32), pltpu.VMEM...]
  transfers between devices with their start and end apart: 9 -> 8, of which waited for: 5 -> 4; matrix products, arithmetic and copies ran while one was open for 6% -> 2% of each run, Pallas kernels for 3% -> 5%
where the time goes in v8:
time: 224 us; the launch traced here: 223 us
  blocking collectives  129 us (58%)
  starting transfers between devices  33.9 us (15%)
  Pallas kernels  24.2 us (11%)
  waiting for transfers between devices  14.1 us (6%)
  between operations  13.6 us (6%)
  local copies, waits for them, and re-layouts  5.95 us (3%)
    all_gather x1, blocking collectives, on_device(): out_x = lax.all_gather(small[:, 2 * sg:], 'x', axis=0, tiled=True)  33.8 us
    all_gather x1, blocking collectives, on_device(): small = lax.all_gather(small, 'z', axis=0, tiled=True)  33 us
    all_to_all x1, blocking collectives, on_device(): lax.all_to_all(pair.reshape(chips, own_rows, width), 'x', 0, 0, tiled=True)  17.2 us
    all_to_all x1, starting transfers between devices, sent_to_all(): return lax.all_to_all(copies, axis, split_axis=0, concat_axis=0, tiled=True)  17.2 us
    all_gather x1, blocking collectives, on_device(): lax.all_gather(jnp.concatenate([gate_weight, up_weight, down_weight.T], a...  12.7 us
    pallas_call x1, Pallas kernels, mixer(): pl.pallas_call(body, out_shape=(pltpu.VMEM((few, width), BF16), pltpu.VME...  12.5 us
    all_to_all x1, blocking collectives, sent_to_all(): return lax.all_to_all(copies, axis, split_axis=0, concat_axis=0, tiled=True)  12.2 us
    all_to_all x1, blocking collectives, on_device(): known = lax.all_to_all(sums, TP, 0, 0, tiled=True)  10.2 us
  transfers between devices with their start and end apart: 8, of which 4 were waited for; matrix products, arithmetic and copies ran while one was open for 2% of the time, Pallas kernels for 5%

profile of v8, /device:TPU:1, one launch (start us, length us, event | category | flops | bytes accessed | tf_op | source)
XLA Modules:
  0.0 222.7 jit_solution(11552183359200946996)
XLA Ops:
  7.5 12.7 %all_gather.14 = bf16[128,2112]{1,0:T(8,128)(2,1)} all-gather(bf16[32,2112]{1,0:T(8,128)(2,1)S(1)} %concatenate.11), channel_id=1, replica_groups=mesh['z'=16,'y'=4,'x'=4,'c'=2] {'y'}, dimensions={0}, use_global_device_ids=true | all-gather | bytes 675840 | tf_op jit(solution)/shard_map/all_gather | solution.py:346
  20.9 33.0 %all_gather.12 = bf16[512,384]{1,0:T(8,128)(2,1)S(1)} all-gather(bf16[32,384]{1,0:T(8,128)(2,1)S(1)} %pad_maximum_fusion), channel_id=1, replica_groups=mesh['z'=16,'y'=4,'x'=4,'c'=2] {'z'}, dimensions={0}, use_global_device_ids=true | all-gather | bytes 417792 | tf_op jit(solution)/shard_map/all_gather | solution.py:350
  54.8 12.2 %all_to_all.30.gates_ref = bf16[4,512,256]{2,1,0:T(8,128)(2,1)S(1)} all-to-all(bf16[4,512,256]{2,1,0:T(8,128)(2,1)S(1)} %broadcast_in_dim.7), channel_id=1, replica_groups=mesh['z'=16,'y'=4,'x'=4,'c'=2] {'y'}, dimensions={0} | all-to-all | bytes 2097152 | tf_op jit(solution)/shard_map/all_to_all | solution.py:21
  67.0 1.5 broadcast_in_dim.6
  68.5 17.2 %all-to-all-start = ((bf16[8,512,256]{2,1,0:T(8,128)(2,1)}), bf16[8,512,256]{2,1,0:T(8,128)(2,1)S(1)}, u32[]{:S(2)}, u32[]{:S(2)}) async-start(bf16[8,512,256]{2,1,0:T(8,128)(2,1)} %broadcast_in_dim.6), calls=%async_computation | async-start | bytes 4194304 | tf_op jit(solution)/shard_map/all_to_all | solution.py:21
  85.7 33.8 %all_gather.13 = bf16[2048,128]{1,0:T(8,128)(2,1)} all-gather(bf16[512,128]{1,0:T(8,128)(2,1)S(1)} %slice-done), channel_id=1, replica_groups=mesh['z'=16,'y'=4,'x'=4,'c'=2] {'x'}, dimensions={0}, use_global_device_ids=true | all-gather | bytes 655360 | tf_op jit(solution)/shard_map/all_gather | solution.py:352
  119.4 2.8 %collective-permute-start.2 = (bf16[2048,128]{1,0:T(8,128)(2,1)}, bf16[2048,128]{1,0:T(8,128)(2,1)}, u32[]{:S(2)}, u32[]{:S(2)}) collective-permute-start(bf16[2048,128]{1,0:T(8,128)(2,1)} %all_gather.13), channel_id=1, source_target_pairs={{0,24},{8,0},{16,8},{24,16},{1,25},{9,1},{17,9},{25,17},{2,26},{10... | collective-permute-start | bytes 1572872 | tf_op jit(solution)/shard_map/ppermute | solution.py:319
  122.2 3.1 %collective-permute-start.1 = (bf16[2048,128]{1,0:T(8,128)(2,1)}, bf16[2048,128]{1,0:T(8,128)(2,1)}, u32[]{:S(2)}, u32[]{:S(2)}) collective-permute-start(bf16[2048,128]{1,0:T(8,128)(2,1)} %all_gather.13), channel_id=1, source_target_pairs={{0,16},{8,24},{16,0},{24,8},{1,17},{9,25},{17,1},{25,9},{2,18},{10... | collective-permute-start | bytes 1572872 | tf_op jit(solution)/shard_map/ppermute | solution.py:319
  125.3 1.9 collective-permute-start
  127.3 1.3 copy-done.3
  128.6 2.5 %branches.1 = (f32[512,128]{1,0:T(8,128)S(1)}, f32[512,128]{1,0:T(8,128)S(1)}, f32[8,4,512]{2,1,0:T(4,128)S(1)}) custom-call(bf16[8,512,256]{2,1,0:T(8,128)(2,1)} %copy-done.3, bf16[4,512,256]{2,1,0:T(8,128)(2,1)S(1)} %all_to_all.30.gates_ref, f32[1,512]{1,0:T(1,128)S(1)} %bitcast.17), custom_call_target="tpu_custom_call" | custom-call | flops 536870912 | bytes 4194304 | tf_op jit(solution)/shard_map/branches/pallas_call | solution.py:99
  131.1 10.2 %all_to_all.31.known_ref = f32[8,4,512]{2,1,0:T(4,128)S(1)} all-to-all(f32[8,4,512]{2,1,0:T(4,128)S(1)} %get-tuple-element.11), channel_id=1, replica_groups=mesh['z'=16,'y'=4,'x'=4,'c'=2] {'x','c'}, dimensions={0} | all-to-all | bytes 131072 | tf_op jit(solution)/shard_map/all_to_all | solution.py:357
  141.4 1.2 gated_copies.1
  142.5 3.5 %all-to-all-start.3 = ((bf16[4,512,128]{2,1,0:T(8,128)(2,1)}), bf16[4,512,128]{2,1,0:T(8,128)(2,1)S(1)}, u32[]{:S(2)}, u32[]{:S(2)}) async-start(bf16[4,512,128]{2,1,0:T(8,128)(2,1)} %gated_copies.1), calls=%async_computation.3 | async-start | bytes 1048576 | tf_op jit(solution)/shard_map/all_to_all | solution.py:362
  146.6 4.4 %collective-permute-done = bf16[2048,128]{1,0:T(8,128)(2,1)} collective-permute-done((bf16[2048,128]{1,0:T(8,128)(2,1)}, bf16[2048,128]{1,0:T(8,128)(2,1)}, u32[]{:S(2)}, u32[]{:S(2)}) %collective-permute-start) | collective-permute-done | bytes 524320 | tf_op jit(solution)/shard_map/ppermute | solution.py:319
  151.0 4.1 %all-to-all-done.3.gated_ref = bf16[4,512,128]{2,1,0:T(8,128)(2,1)S(1)} async-done(((bf16[4,512,128]{2,1,0:T(8,128)(2,1)}), bf16[4,512,128]{2,1,0:T(8,128)(2,1)S(1)}, u32[]{:S(2)}, u32[]{:S(2)}) %all-to-all-start.3) | async-done | bytes 524320 | tf_op jit(solution)/shard_map/all_to_all | solution.py:362
  155.2 7.0 %projected.1.own_ref = bf16[512,2048]{1,0:T(8,128)(2,1)} custom-call(s32[3]{0:T(128)} %pad_add_fusion.place_ref, bf16[4,512,128]{2,1,0:T(8,128)(2,1)S(1)} %all-to-all-done.3.gated_ref, bf16[4,16,32,128]{3,2,1,0:T(8,128)(2,1)} %bitcast.6.rest_0_, bf16[4,16,32,128]{3,2,1,0:T(8,128)(2,1)} %bitcast.7.rest_1_, bf16[4,16,32,128]{3,2,1,0:T(8,128)(2,1)} %bitcast.8.rest_2_, ...), custom_call_target="tpu_custom_call" | custom-call | flops 1073741824 | bytes 6291456 | tf_op jit(solution)/shard_map/projected/pallas_call | solution.py:198
  162.2 3.1 %collective-permute-start.3 = (bf16[512,2048]{1,0:T(8,128)(2,1)}, bf16[512,2048]{1,0:T(8,128)(2,1)S(1)}, u32[]{:S(2)}, u32[]{:S(2)}) collective-permute-start(bf16[512,2048]{1,0:T(8,128)(2,1)} %projected.1.own_ref), channel_id=1, source_target_pairs={{0,1},{1,0},{2,3},{3,2},{4,5},{5,4},{6,7},{7,6},{8,9},{9,8},{10,11... | collective-permute-start | bytes 6291464 | tf_op jit(solution)/shard_map/ppermute | solution.py:25
  166.0 3.3 %collective-permute-done.3.other_ref = bf16[512,2048]{1,0:T(8,128)(2,1)S(1)} collective-permute-done((bf16[512,2048]{1,0:T(8,128)(2,1)}, bf16[512,2048]{1,0:T(8,128)(2,1)S(1)}, u32[]{:S(2)}, u32[]{:S(2)}) %collective-permute-start.3) | collective-permute-done | bytes 2097184 | tf_op jit(solution)/shard_map/ppermute | solution.py:25
  169.3 12.5 %mixer.1 = (bf16[64,2048]{1,0:T(8,128)(2,1)S(1)}, bf16[256,2048]{1,0:T(8,128)(2,1)S(1)}, bf16[256,2048]{1,0:T(8,128)(2,1)S(1)}) custom-call(s32[3]{0:T(128)} %pad_add_fusion.place_ref, bf16[512,2048]{1,0:T(8,128)(2,1)} %projected.1.own_ref, bf16[512,2048]{1,0:T(8,128)(2,1)S(1)} %collective-permute-done.3.other_ref, bf16[8,512,256]{2,1,0:T(8,128)(2,1)} %copy-done.3, ...), custom_call_target="tpu_custom_call" | custom-call | flops 4429185024 | bytes 18874368 | tf_op jit(solution)/shard_map/mixer/pallas_call | solution.py:292
  181.8 2.3 %collective-permute-start.4 = (bf16[256,2048]{1,0:T(8,128)(2,1)S(1)}, bf16[256,2048]{1,0:T(8,128)(2,1)S(1)}, u32[]{:S(2)}, u32[]{:S(2)}) collective-permute-start(bf16[256,2048]{1,0:T(8,128)(2,1)S(1)} %get-tuple-element.15), channel_id=1, source_target_pairs={{0,1},{1,0},{2,3},{3,2},{4,5},{5,4},{6,7},{7,6},{8,9},{9,8},{10,11... | collective-permute-start | bytes 3145736 | tf_op jit(solution)/shard_map/ppermute | solution.py:25
  184.1 2.3 %collective-permute-done.4 = bf16[256,2048]{1,0:T(8,128)(2,1)S(1)} collective-permute-done((bf16[256,2048]{1,0:T(8,128)(2,1)S(1)}, bf16[256,2048]{1,0:T(8,128)(2,1)S(1)}, u32[]{:S(2)}, u32[]{:S(2)}) %collective-permute-start.4) | collective-permute-done | bytes 1048608 | tf_op jit(solution)/shard_map/ppermute | solution.py:25
  186.7 17.2 %all_to_all.32.pieces_ref = bf16[4,64,2048]{2,1,0:T(8,128)(2,1)S(1)} all-to-all(bf16[4,64,2048]{2,1,0:T(8,128)(2,1)S(1)} %bitcast.19), channel_id=1, replica_groups=mesh['z'=16,'y'=4,'x'=4,'c'=2] {'x'}, dimensions={0} | all-to-all | bytes 2097152 | tf_op jit(solution)/shard_map/all_to_all | solution.py:367
  205.1 10.1 %all_to_all.33 = bf16[8,64,256]{2,1,0:T(8,128)(2,1)S(1)} all-to-all(bf16[8,64,256]{2,1,0:T(8,128)(2,1)S(1)} %last_norm.1), channel_id=1, replica_groups=mesh['z'=16,'y'=4,'x'=4,'c'=2] {'x','c'}, dimensions={0} | all-to-all | bytes 524288 | tf_op jit(solution)/shard_map/all_to_all | solution.py:369
  (35 shorter events, 6.0 us)
Async XLA Ops:
  6.5 162.8 %all-gather.2.cloned.1.call-start = ((), (), s32[]{:S(2)}) async-start(), calls=%async_computation.6 | async-start | bytes 9469952 | tf_op jit(solution)/shard_map/all_gather | solution.py:347
  20.9 46.1 %copy-start.5 = (bf16[512,256]{1,0:T(8,128)(2,1)S(1)}, bf16[512,256]{1,0:T(8,128)(2,1)}, u32[]{:S(2)}) copy-start(bf16[512,256]{1,0:T(8,128)(2,1)} %param.12) | copy-start | bytes 786436
  53.9 0.7 copy-start.4
  68.5 17.2 %slice-start = ((bf16[512,384]{1,0:T(8,128)(2,1)}), bf16[512,128]{1,0:T(8,128)(2,1)S(1)}, s32[]{:S(2)}) async-start(bf16[512,384]{1,0:T(8,128)(2,1)} %copy-done.4), calls=%async_computation.7 | async-start | bytes 262144 | tf_op jit(solution)/shard_map/slice | solution.py:352
  68.5 58.8 %copy-start.6 = (f32[256]{0:T(256)S(1)}, f32[256]{0:T(256)}, u32[]{:S(2)}) copy-start(f32[256]{0:T(256)} %param.23) | copy-start | bytes 3076
  68.5 58.8 %copy-start.7 = (f32[256]{0:T(256)S(1)}, f32[256]{0:T(256)}, u32[]{:S(2)}) copy-start(f32[256]{0:T(256)} %param.19) | copy-start | bytes 3076
  68.5 58.8 %all-to-all-start = ((bf16[8,512,256]{2,1,0:T(8,128)(2,1)}), bf16[8,512,256]{2,1,0:T(8,128)(2,1)S(1)}, u32[]{:S(2)}, u32[]{:S(2)}) async-start(bf16[8,512,256]{2,1,0:T(8,128)(2,1)} %broadcast_in_dim.6), calls=%async_computation | async-start | bytes 4194304 | tf_op jit(solution)/shard_map/all_to_all | solution.py:21
  85.6 55.7 %copy-start = (bf16[1,128,128]{2,1,0:T(8,128)(2,1)S(1)}, bf16[1,128,128]{2,1,0:T(8,128)(2,1)}, u32[]{:S(2)}) copy-start(bf16[1,128,128]{2,1,0:T(8,128)(2,1)} %weight_ref.1) | copy-start | bytes 98308
  85.6 55.7 %copy-start.1 = (f32[128]{0:T(128)S(1)}, f32[128]{0:T(128)}, u32[]{:S(2)}) copy-start(f32[128]{0:T(128)} %param.15) | copy-start | bytes 1540
  85.7 55.7 %copy-start.2 = (f32[1,128]{1,0:T(1,128)S(1)}, f32[1,128]{1,0:T(1,128)}, u32[]{:S(2)}) copy-start(f32[1,128]{1,0:T(1,128)} %bias_ref.1) | copy-start | bytes 1540
  119.4 27.2 %collective-permute-start.2 = (bf16[2048,128]{1,0:T(8,128)(2,1)}, bf16[2048,128]{1,0:T(8,128)(2,1)}, u32[]{:S(2)}, u32[]{:S(2)}) collective-permute-start(bf16[2048,128]{1,0:T(8,128)(2,1)} %all_gather.13), channel_id=1, source_target_pairs={{0,24},{8,0},{16,8},{24,16},{1,25},{9,1},{17,9},{25,17},{2,26},{10... | collective-permute-start | bytes 1572872 | tf_op jit(solution)/shard_map/ppermute | solution.py:319
  122.2 24.4 %collective-permute-start.1 = (bf16[2048,128]{1,0:T(8,128)(2,1)}, bf16[2048,128]{1,0:T(8,128)(2,1)}, u32[]{:S(2)}, u32[]{:S(2)}) collective-permute-start(bf16[2048,128]{1,0:T(8,128)(2,1)} %all_gather.13), channel_id=1, source_target_pairs={{0,16},{8,24},{16,0},{24,8},{1,17},{9,25},{17,1},{25,9},{2,18},{10... | collective-permute-start | bytes 1572872 | tf_op jit(solution)/shard_map/ppermute | solution.py:319
  125.3 25.7 %collective-permute-start = (bf16[2048,128]{1,0:T(8,128)(2,1)}, bf16[2048,128]{1,0:T(8,128)(2,1)}, u32[]{:S(2)}, u32[]{:S(2)}) collective-permute-start(bf16[2048,128]{1,0:T(8,128)(2,1)} %all_gather.13), channel_id=1, source_target_pairs={{0,8},{8,16},{16,24},{24,0},{1,9},{9,17},{17,25},{25,1},{2,10},{10... | collective-permute-start | bytes 1572872 | tf_op jit(solution)/shard_map/ppermute | solution.py:319
  127.3 1.3 copy-start.3
  142.5 12.6 %all-to-all-start.3 = ((bf16[4,512,128]{2,1,0:T(8,128)(2,1)}), bf16[4,512,128]{2,1,0:T(8,128)(2,1)S(1)}, u32[]{:S(2)}, u32[]{:S(2)}) async-start(bf16[4,512,128]{2,1,0:T(8,128)(2,1)} %gated_copies.1), calls=%async_computation.3 | async-start | bytes 1048576 | tf_op jit(solution)/shard_map/all_to_all | solution.py:362
  162.2 7.1 %collective-permute-start.3 = (bf16[512,2048]{1,0:T(8,128)(2,1)}, bf16[512,2048]{1,0:T(8,128)(2,1)S(1)}, u32[]{:S(2)}, u32[]{:S(2)}) collective-permute-start(bf16[512,2048]{1,0:T(8,128)(2,1)} %projected.1.own_ref), channel_id=1, source_target_pairs={{0,1},{1,0},{2,3},{3,2},{4,5},{5,4},{6,7},{7,6},{8,9},{9,8},{10,11... | collective-permute-start | bytes 6291464 | tf_op jit(solution)/shard_map/ppermute | solution.py:25
  181.8 4.6 %collective-permute-start.4 = (bf16[256,2048]{1,0:T(8,128)(2,1)S(1)}, bf16[256,2048]{1,0:T(8,128)(2,1)S(1)}, u32[]{:S(2)}, u32[]{:S(2)}) collective-permute-start(bf16[256,2048]{1,0:T(8,128)(2,1)S(1)} %get-tuple-element.15), channel_id=1, source_target_pairs={{0,1},{1,0},{2,3},{3,2},{4,5},{5,4},{6,7},{7,6},{8,9},{9,8},{10,11... | collective-permute-start | bytes 3145736 | tf_op jit(solution)/shard_map/ppermute | solution.py:25
Sparse Core Ops, SparseCore 0:
  20.3 119.2 all-gather.1

commit v9 on v8

--- a/solution.py
+++ b/solution.py
@@ -210,57 +210,102 @@
     )(in_hbm(place), in_vmem(gated), *given)
 
 
-def mixer(place, own, other, blocks, gain, ffw, ff):
+def copies_of(value, count):
+    def body(value_ref, out_ref):
+        for k in range(count):
+            out_ref[k] = value_ref[...]
+
+    return pl.pallas_call(
+        body,
+        out_shape=pltpu.VMEM((count, *value.shape), value.dtype),
+        in_specs=[whole_vmem()],
+        out_specs=whole_vmem(),
+        compiler_params=pltpu.CompilerParams(vmem_limit_bytes=8 << 20),
+        name="copies",
+    )(value)
+
+
+def first_rows(place, own, other, blocks, gain):
     rows, width = own.shape
     parts, _, feats = blocks.shape
-    chips = parts // 2
-    half = rows // 2
     few = rows // parts
-    edges = [0, 384, 768, 1152, 2 * ff, 3 * ff]
-    spans = [e - b for b, e in zip(edges, edges[1:])]
-    chunks = len(spans)
-    ahead = 3
-    step = 256
-
-    def body(place_ref, own_ref, other_ref, blocks_ref, gain_ref, ffw_ref, mine_ref, keep_ref, give_ref, *rest):
-        weights = rest[:chunks]
-        base, low, vals, left, acc, in_sems, sems = rest[chunks:]
-        core = place_ref[0]
+    lanes = 128
+
+    def body(place_ref, own_ref, other_ref, blocks_ref, gain_ref, first_ref, mine_ref, base, low, vals, sems):
         me = place_ref[1]
         inputs = []
         for j in range(parts):
             at = pl.ds(j * feats, feats)
             inputs.append(
                 [
-                    pltpu.make_async_copy(own_ref.at[:, at], low.at[j], in_sems.at[j, 0]),
-                    pltpu.make_async_copy(blocks_ref.at[j], base.at[j], in_sems.at[j, 1]),
+                    pltpu.make_async_copy(own_ref.at[:, at], low.at[j], sems.at[j, 0]),
+                    pltpu.make_async_copy(blocks_ref.at[j], base.at[j], sems.at[j, 1]),
                 ]
             )
             for c in inputs[j]:
                 c.start()
+        total = jnp.zeros((rows, lanes), F32)
+        squares = jnp.zeros((rows, lanes), F32)
+        for j in range(parts):
+            for c in inputs[j]:
+                c.wait()
+            for b in range(0, feats, lanes):
+                at = slice(j * feats + b, j * feats + b + lanes)
+                high = other_ref[:, at]
+                mix = (low[j, :, b : b + lanes].astype(F32) + high.astype(F32)).astype(BF16)
+                these = ALPHA * base[j, :, b : b + lanes].astype(F32) + mix.astype(F32)
+                vals[:, at] = these
+                total += these
+                squares += these * these
+        mean = jnp.sum(total, axis=1, keepdims=True) / width
+        scale = lax.rsqrt(jnp.sum(squares, axis=1, keepdims=True) / width - mean * mean + EPS)
+        for j in range(parts):
+            at = slice(j * feats, (j + 1) * feats)
+            first_ref[:, at] = ((vals[:, at] - mean) * scale * gain_ref[:, at]).astype(BF16)
+        mine_ref[...] = first_ref[pl.ds(pl.multiple_of(me * few, few), few), :]
+
+    hbm = pl.BlockSpec(memory_space=pltpu.HBM)
+    return pl.pallas_call(
+        body,
+        out_shape=(jax.ShapeDtypeStruct((rows, width), BF16), pltpu.VMEM((few, width), BF16)),
+        in_specs=[pl.BlockSpec(memory_space=pltpu.SMEM), hbm, whole_vmem(), hbm, whole_vmem()],
+        out_specs=(whole_vmem(),) * 2,
+        scratch_shapes=[
+            pltpu.VMEM((parts, rows, feats), BF16),
+            pltpu.VMEM((parts, rows, feats), BF16),
+            pltpu.VMEM((rows, width), F32),
+            pltpu.SemaphoreType.DMA((parts, 2)),
+        ],
+        compiler_params=pltpu.CompilerParams(vmem_limit_bytes=16 << 20),
+        cost_estimate=pl.CostEstimate(flops=12 * rows * width, bytes_accessed=6 << 20, transcendentals=rows),
+        name="first_rows",
+    )(in_hbm(place), in_hbm(own), in_vmem(other), in_hbm(blocks), gain.reshape(1, width))
+
+
+def mixer(place, first, ffw, ff):
+    rows, width = first.shape
+    chips = 4
+    half = rows // 2
+    few = half // chips
+    edges = [0, 384, 768, 1152, 2 * ff, 3 * ff]
+    spans = [e - b for b, e in zip(edges, edges[1:])]
+    chunks = len(spans)
+    ahead = 3
+    step = 256
+
+    def body(place_ref, first_ref, ffw_ref, keep_ref, give_ref, *rest):
+        weights = rest[:chunks]
+        left, acc, lead, sems = rest[chunks:]
+        core = place_ref[0]
+        start = pltpu.make_async_copy(first_ref, left, lead.at[0])
+        start.start()
         copies = []
         for n in range(chunks):
             at = pl.ds(edges[n], spans[n])
             copies.append(pltpu.make_async_copy(ffw_ref.at[:, at], weights[n], sems.at[n]))
         for c in copies[:ahead]:
             c.start()
-        total = jnp.zeros((rows, 1), F32)
-        squares = jnp.zeros((rows, 1), F32)
-        for j in range(parts):
-            for c in inputs[j]:
-                c.wait()
-            high = other_ref[:, j * feats : (j + 1) * feats]
-            mix = (low[j].astype(F32) + high.astype(F32)).astype(BF16)
-            these = ALPHA * base[j].astype(F32) + mix.astype(F32)
-            vals[j] = these
-            total += jnp.sum(these, axis=1, keepdims=True)
-            squares += jnp.sum(these * these, axis=1, keepdims=True)
-        mean = total / width
-        scale = lax.rsqrt(squares / width - mean * mean + EPS)
-        for j in range(parts):
-            at = slice(j * feats, (j + 1) * feats)
-            left[:, at] = ((vals[j] - mean) * scale * gain_ref[:, at]).astype(BF16)
-        mine_ref[...] = left[pl.ds(pl.multiple_of(me * few, few), few), :]
+        start.wait()
         for n in range(chunks - 1):
             copies[n].wait()
             if n + ahead < chunks:
@@ -288,30 +333,25 @@
         def _():
             out(1)
 
-    anywhere = pl.BlockSpec(memory_space=pltpu.HBM)
     return pl.pallas_call(
         body,
         out_shape=(
-            pltpu.VMEM((few, width), BF16),
             pltpu.VMEM((half, width), BF16),
             pltpu.VMEM((half, width), BF16),
         ),
-        in_specs=[pl.BlockSpec(memory_space=pltpu.SMEM), anywhere, whole_vmem(), anywhere, whole_vmem(), anywhere],
-        out_specs=(whole_vmem(),) * 3,
+        in_specs=[pl.BlockSpec(memory_space=pltpu.SMEM)] + [pl.BlockSpec(memory_space=pltpu.HBM)] * 2,
+        out_specs=(whole_vmem(),) * 2,
         scratch_shapes=[
             *(pltpu.VMEM((width, n), BF16) for n in spans),
-            pltpu.VMEM((parts, rows, feats), BF16),
-            pltpu.VMEM((parts, rows, feats), BF16),
-            pltpu.VMEM((parts, rows, feats), F32),
             pltpu.VMEM((rows, width), BF16),
             pltpu.VMEM((rows, 2 * ff), F32),
-            pltpu.SemaphoreType.DMA((parts, 2)),
+            pltpu.SemaphoreType.DMA((1,)),
             pltpu.SemaphoreType.DMA((chunks,)),
         ],
         cost_estimate=pl.CostEstimate(flops=6 * rows * width * ff, bytes_accessed=18 << 20, transcendentals=rows * ff),
         name="mixer",
-        compiler_params=pltpu.CompilerParams(vmem_limit_bytes=40 << 20),
-    )(in_hbm(place), in_hbm(own), in_vmem(other), in_hbm(blocks), gain.reshape(1, width), in_hbm(ffw))
+        compiler_params=pltpu.CompilerParams(vmem_limit_bytes=28 << 20),
+    )(in_hbm(place), in_hbm(first), in_hbm(ffw))
 
 
 def from_each(value, axis):
@@ -341,7 +381,7 @@
     sg = u_weight.shape[1]
     own_rows = rows // parts
 
-    blocks = sent_to_all(tokens, TP)
+    blocks = lax.all_to_all(copies_of(tokens, parts), TP, 0, 0, tiled=True)
 
     ffw = lax.all_gather(jnp.concatenate([gate_weight, up_weight, down_weight.T], axis=1), "y", axis=0, tiled=True)
     ffw = lax.all_gather(ffw, "z", axis=0, tiled=True)
@@ -362,7 +402,8 @@
     together = lax.all_to_all(copies, "x", 0, 0, tiled=True)
     place = jnp.stack([core, lax.axis_index(TP), lax.axis_index("y")]).astype(jnp.int32)
     own = projected(place, together, out_rows)
-    mine, keep, give = mixer(place, own, to_partner(own), blocks, gain_1, ffw, gate_weight.shape[1])
+    first, mine = first_rows(place, own, to_partner(own), blocks, gain_1)
+    keep, give = mixer(place, first, ffw, gate_weight.shape[1])
     pair = (keep.astype(F32) + to_partner(give).astype(F32)).astype(BF16)
     pieces = lax.all_to_all(pair.reshape(chips, own_rows, width), "x", 0, 0, tiled=True)
     last = last_norm(pieces, mine, gain_2, parts)

time: 224 us -> 229 us (1.022)
  blocking collectives: 129 us -> 117 us
  waiting for transfers between devices: 14.1 us -> 22.4 us
  Pallas kernels: 24.2 us -> 29.1 us
  starting transfers between devices: 33.9 us -> 37 us
    all_to_all x0 -> x1, starting transfers between devices: none -> 16.2 us  [on_device(): blocks = lax.all_to_all(copies_of(tokens, parts), TP, 0, 0, tiled=True)]
    all_to_all x1, starting transfers between devices: 17.2 us -> 3.51 us  [sent_to_all(): return lax.all_to_all(copies, axis, split_axis=0, concat_axis=0, tiled=True)]
    all_to_all x1 -> x0, blocking collectives: 12.2 us -> none  [sent_to_all(): return lax.all_to_all(copies, axis, split_axis=0, concat_axis=0, tiled=True)]
    all_to_all x1, waiting for transfers between devices: 0.01 us -> 8.29 us  [sent_to_all(): return lax.all_to_all(copies, axis, split_axis=0, concat_axis=0, tiled=True)]
    pallas_call x1 -> x3, Pallas kernels: 12.5 us -> 17.4 us  [the longest x1 10.9 us: mixer(): pl.pallas_call(body, out_shape=(pltpu.VMEM((half, width), BF16), pltpu.VM...]
    ppermute x3, waiting for transfers between devices: 4.43 us -> 2.1 us  [from_each(): lax.ppermute(value, axis, [(i, (i + k) % size) for i in range(size)])]
  transfers between devices with their start and end apart: 8 -> 9, of which waited for: 4 -> 5; matrix products, arithmetic and copies ran while one was open for 2% -> 1% of each run, Pallas kernels for 5% -> 7%
where the time goes in v9:
time: 229 us; the launch traced here: 228 us
  blocking collectives  117 us (51%)
  starting transfers between devices  37 us (16%)
  Pallas kernels  29.1 us (13%)
  waiting for transfers between devices  22.4 us (10%)
  between operations  13.6 us (6%)
  local copies, waits for them, and re-layouts  6.79 us (3%)
    all_gather x1, blocking collectives, on_device(): out_x = lax.all_gather(small[:, 2 * sg:], 'x', axis=0, tiled=True)  33.8 us
    all_gather x1, blocking collectives, on_device(): small = lax.all_gather(small, 'z', axis=0, tiled=True)  33 us
    all_to_all x1, blocking collectives, on_device(): lax.all_to_all(pair.reshape(chips, own_rows, width), 'x', 0, 0, tiled=True)  17.2 us
    all_to_all x1, starting transfers between devices, on_device(): blocks = lax.all_to_all(copies_of(tokens, parts), TP, 0, 0, tiled=True)  16.2 us
    all_gather x1, blocking collectives, on_device(): lax.all_gather(jnp.concatenate([gate_weight, up_weight, down_weight.T], a...  12.7 us
    pallas_call x1, Pallas kernels, mixer(): pl.pallas_call(body, out_shape=(pltpu.VMEM((half, width), BF16), pltpu.VM...  10.9 us
    all_to_all x1, blocking collectives, on_device(): known = lax.all_to_all(sums, TP, 0, 0, tiled=True)  10.3 us
    all_to_all x1, blocking collectives, on_device(): return lax.all_to_all(last, TP, 0, 0, tiled=True).reshape(rows, feats)  10.1 us
  transfers between devices with their start and end apart: 9, of which 5 were waited for; matrix products, arithmetic and copies ran while one was open for 1% of the time, Pallas kernels for 7%

profile of v9, /device:TPU:1, one launch (start us, length us, event | category | flops | bytes accessed | tf_op | source)
XLA Modules:
  0.0 227.7 jit_solution(6059885329165411173)
XLA Ops:
  7.5 12.7 %all_gather.14 = bf16[128,2112]{1,0:T(8,128)(2,1)} all-gather(bf16[32,2112]{1,0:T(8,128)(2,1)S(1)} %concatenate.11), channel_id=1, replica_groups=mesh['z'=16,'y'=4,'x'=4,'c'=2] {'y'}, dimensions={0}, use_global_device_ids=true | all-gather | bytes 675840 | tf_op jit(solution)/shard_map/all_gather | solution.py:386
  20.9 33.0 %all_gather.12 = bf16[512,384]{1,0:T(8,128)(2,1)S(1)} all-gather(bf16[32,384]{1,0:T(8,128)(2,1)S(1)} %pad_maximum_fusion), channel_id=1, replica_groups=mesh['z'=16,'y'=4,'x'=4,'c'=2] {'z'}, dimensions={0}, use_global_device_ids=true | all-gather | bytes 417792 | tf_op jit(solution)/shard_map/all_gather | solution.py:390
  55.8 3.5 %all-to-all-start.1 = ((bf16[4,512,256]{2,1,0:T(8,128)(2,1)}), bf16[4,512,256]{2,1,0:T(8,128)(2,1)S(1)}, u32[]{:S(2)}, u32[]{:S(2)}) async-start(bf16[4,512,256]{2,1,0:T(8,128)(2,1)} %broadcast_in_dim.3), calls=%async_computation.1 | async-start | bytes 2097152 | tf_op jit(solution)/shard_map/all_to_all | solution.py:21
  59.3 1.5 copies.1
  60.8 8.3 %all-to-all-done.1.gates_ref = bf16[4,512,256]{2,1,0:T(8,128)(2,1)S(1)} async-done(((bf16[4,512,256]{2,1,0:T(8,128)(2,1)}), bf16[4,512,256]{2,1,0:T(8,128)(2,1)S(1)}, u32[]{:S(2)}, u32[]{:S(2)}) %all-to-all-start.1) | async-done | bytes 1048608 | tf_op jit(solution)/shard_map/all_to_all | solution.py:21
  69.0 16.2 %all-to-all-start = ((bf16[8,512,256]{2,1,0:T(8,128)(2,1)}), bf16[8,512,256]{2,1,0:T(8,128)(2,1)S(1)}, u32[]{:S(2)}, u32[]{:S(2)}) async-start(bf16[8,512,256]{2,1,0:T(8,128)(2,1)} %copies.1), calls=%async_computation | async-start | bytes 4194304 | tf_op jit(solution)/shard_map/all_to_all | solution.py:384
  85.2 33.8 %all_gather.13 = bf16[2048,128]{1,0:T(8,128)(2,1)} all-gather(bf16[512,128]{1,0:T(8,128)(2,1)S(1)} %slice-done), channel_id=1, replica_groups=mesh['z'=16,'y'=4,'x'=4,'c'=2] {'x'}, dimensions={0}, use_global_device_ids=true | all-gather | bytes 655360 | tf_op jit(solution)/shard_map/all_gather | solution.py:392
  119.0 2.2 collective-permute-start
  121.2 3.7 %collective-permute-start.1 = (bf16[2048,128]{1,0:T(8,128)(2,1)}, bf16[2048,128]{1,0:T(8,128)(2,1)}, u32[]{:S(2)}, u32[]{:S(2)}) collective-permute-start(bf16[2048,128]{1,0:T(8,128)(2,1)} %all_gather.13), channel_id=1, source_target_pairs={{0,16},{8,24},{16,0},{24,8},{1,17},{9,25},{17,1},{25,9},{2,18},{10... | collective-permute-start | bytes 1572872 | tf_op jit(solution)/shard_map/ppermute | solution.py:359
  124.9 2.5 %collective-permute-start.2 = (bf16[2048,128]{1,0:T(8,128)(2,1)}, bf16[2048,128]{1,0:T(8,128)(2,1)}, u32[]{:S(2)}, u32[]{:S(2)}) collective-permute-start(bf16[2048,128]{1,0:T(8,128)(2,1)} %all_gather.13), channel_id=1, source_target_pairs={{0,24},{8,0},{16,8},{24,16},{1,25},{9,1},{17,9},{25,17},{2,26},{10... | collective-permute-start | bytes 1572872 | tf_op jit(solution)/shard_map/ppermute | solution.py:359
  128.8 2.5 %branches.1 = (f32[512,128]{1,0:T(8,128)S(1)}, f32[512,128]{1,0:T(8,128)S(1)}, f32[8,4,512]{2,1,0:T(4,128)S(1)}) custom-call(bf16[8,512,256]{2,1,0:T(8,128)(2,1)} %copy-done.5, bf16[4,512,256]{2,1,0:T(8,128)(2,1)S(1)} %all-to-all-done.1.gates_ref, f32[1,512]{1,0:T(1,128)S(1)} %bitcast.17), custom_call_target="tpu_custom_call" | custom-call | flops 536870912 | bytes 4194304 | tf_op jit(solution)/shard_map/branches/pallas_call | solution.py:99
  131.3 10.3 %all_to_all.30.known_ref = f32[8,4,512]{2,1,0:T(4,128)S(1)} all-to-all(f32[8,4,512]{2,1,0:T(4,128)S(1)} %get-tuple-element.12), channel_id=1, replica_groups=mesh['z'=16,'y'=4,'x'=4,'c'=2] {'x','c'}, dimensions={0} | all-to-all | bytes 131072 | tf_op jit(solution)/shard_map/all_to_all | solution.py:397
  142.7 3.5 %all-to-all-start.3 = ((bf16[4,512,128]{2,1,0:T(8,128)(2,1)}), bf16[4,512,128]{2,1,0:T(8,128)(2,1)S(1)}, u32[]{:S(2)}, u32[]{:S(2)}) async-start(bf16[4,512,128]{2,1,0:T(8,128)(2,1)} %gated_copies.1), calls=%async_computation.3 | async-start | bytes 1048576 | tf_op jit(solution)/shard_map/all_to_all | solution.py:402
  146.9 2.1 collective-permute-done.2
  149.0 6.4 %all-to-all-done.3.gated_ref = bf16[4,512,128]{2,1,0:T(8,128)(2,1)S(1)} async-done(((bf16[4,512,128]{2,1,0:T(8,128)(2,1)}), bf16[4,512,128]{2,1,0:T(8,128)(2,1)S(1)}, u32[]{:S(2)}, u32[]{:S(2)}) %all-to-all-start.3) | async-done | bytes 524320 | tf_op jit(solution)/shard_map/all_to_all | solution.py:402
  155.4 7.0 %projected.1.own_ref = bf16[512,2048]{1,0:T(8,128)(2,1)} custom-call(s32[3]{0:T(128)} %pad_add_fusion.place_ref, bf16[4,512,128]{2,1,0:T(8,128)(2,1)S(1)} %all-to-all-done.3.gated_ref, bf16[4,16,32,128]{3,2,1,0:T(8,128)(2,1)} %bitcast.6.rest_0_, bf16[4,16,32,128]{3,2,1,0:T(8,128)(2,1)} %bitcast.7.rest_1_, bf16[4,16,32,128]{3,2,1,0:T(8,128)(2,1)} %bitcast.8.rest_2_, ...), custom_call_target="tpu_custom_call" | custom-call | flops 1073741824 | bytes 6291456 | tf_op jit(solution)/shard_map/projected/pallas_call | solution.py:198
  162.4 3.1 %collective-permute-start.3 = (bf16[512,2048]{1,0:T(8,128)(2,1)}, bf16[512,2048]{1,0:T(8,128)(2,1)S(1)}, u32[]{:S(2)}, u32[]{:S(2)}) collective-permute-start(bf16[512,2048]{1,0:T(8,128)(2,1)} %projected.1.own_ref), channel_id=1, source_target_pairs={{0,1},{1,0},{2,3},{3,2},{4,5},{5,4},{6,7},{7,6},{8,9},{9,8},{10,11... | collective-permute-start | bytes 6291464 | tf_op jit(solution)/shard_map/ppermute | solution.py:25
  166.2 3.3 %collective-permute-done.3.other_ref = bf16[512,2048]{1,0:T(8,128)(2,1)S(1)} collective-permute-done((bf16[512,2048]{1,0:T(8,128)(2,1)}, bf16[512,2048]{1,0:T(8,128)(2,1)S(1)}, u32[]{:S(2)}, u32[]{:S(2)}) %collective-permute-start.3) | collective-permute-done | bytes 2097184 | tf_op jit(solution)/shard_map/ppermute | solution.py:25
  169.5 5.0 %first_rows.1 = (bf16[512,2048]{1,0:T(8,128)(2,1)S(1)}, bf16[64,2048]{1,0:T(8,128)(2,1)S(1)}) custom-call(s32[3]{0:T(128)} %pad_add_fusion.place_ref, bf16[512,2048]{1,0:T(8,128)(2,1)} %projected.1.own_ref, bf16[512,2048]{1,0:T(8,128)(2,1)S(1)} %collective-permute-done.3.other_ref, bf16[8,512,256]{2,1,0:T(8,128)(2,1)} %copy-done.5, f32[1,2048]{1,0:T(1,128)S(1)} %bitcast.16), custom_call_target="tpu_custom_call" | custom-call | flops 12582912 | bytes 6291456 | tf_op jit(solution)/shard_map/first_rows/pallas_call | solution.py:268
  175.8 10.9 %mixer.1 = (bf16[256,2048]{1,0:T(8,128)(2,1)S(1)}, bf16[256,2048]{1,0:T(8,128)(2,1)S(1)}) custom-call(s32[3]{0:T(128)} %pad_add_fusion.place_ref, bf16[512,2048]{1,0:T(8,128)(2,1)} %copy-done.4, bf16[2048,2112]{1,0:T(8,128)(2,1)} %all-gather.2.cloned.1.call-done.ffw_ref), custom_call_target="tpu_custom_call" | custom-call | flops 4429185024 | bytes 18874368 | tf_op jit(solution)/shard_map/mixer/pallas_call | solution.py:336
  186.7 2.3 collective-permute-start.4
  189.0 2.3 collective-permute-done.4
  191.7 17.2 %all_to_all.31.pieces_ref = bf16[4,64,2048]{2,1,0:T(8,128)(2,1)S(1)} all-to-all(bf16[4,64,2048]{2,1,0:T(8,128)(2,1)S(1)} %bitcast.19), channel_id=1, replica_groups=mesh['z'=16,'y'=4,'x'=4,'c'=2] {'x'}, dimensions={0} | all-to-all | bytes 2097152 | tf_op jit(solution)/shard_map/all_to_all | solution.py:408
  210.0 10.1 %all_to_all.32 = bf16[8,64,256]{2,1,0:T(8,128)(2,1)S(1)} all-to-all(bf16[8,64,256]{2,1,0:T(8,128)(2,1)S(1)} %last_norm.1), channel_id=1, replica_groups=mesh['z'=16,'y'=4,'x'=4,'c'=2] {'x','c'}, dimensions={0} | all-to-all | bytes 524288 | tf_op jit(solution)/shard_map/all_to_all | solution.py:410
  (39 shorter events, 10.9 us)
Async XLA Ops:
  6.5 169.3 %all-gather.2.cloned.1.call-start = ((), (), s32[]{:S(2)}) async-start(), calls=%async_computation.6 | async-start | bytes 9469952 | tf_op jit(solution)/shard_map/all_gather | solution.py:387
  20.9 38.3 %copy-start = (bf16[512,256]{1,0:T(8,128)(2,1)S(1)}, bf16[512,256]{1,0:T(8,128)(2,1)}, u32[]{:S(2)}) copy-start(bf16[512,256]{1,0:T(8,128)(2,1)} %value_ref.1) | copy-start | bytes 786436
  53.9 0.8 copy-start.6
  55.8 13.3 %all-to-all-start.1 = ((bf16[4,512,256]{2,1,0:T(8,128)(2,1)}), bf16[4,512,256]{2,1,0:T(8,128)(2,1)S(1)}, u32[]{:S(2)}, u32[]{:S(2)}) async-start(bf16[4,512,256]{2,1,0:T(8,128)(2,1)} %broadcast_in_dim.3), calls=%async_computation.1 | async-start | bytes 2097152 | tf_op jit(solution)/shard_map/all_to_all | solution.py:21
  60.8 24.5 %slice-start = ((bf16[512,384]{1,0:T(8,128)(2,1)}), bf16[512,128]{1,0:T(8,128)(2,1)S(1)}, s32[]{:S(2)}) async-start(bf16[512,384]{1,0:T(8,128)(2,1)} %copy-done.6), calls=%async_computation.7 | async-start | bytes 262144 | tf_op jit(solution)/shard_map/slice | solution.py:392
  60.8 66.7 %copy-start.7 = (f32[256]{0:T(256)S(1)}, f32[256]{0:T(256)}, u32[]{:S(2)}) copy-start(f32[256]{0:T(256)} %param.23) | copy-start | bytes 3076
  60.8 66.7 %copy-start.8 = (f32[256]{0:T(256)S(1)}, f32[256]{0:T(256)}, u32[]{:S(2)}) copy-start(f32[256]{0:T(256)} %param.19) | copy-start | bytes 3076
  69.0 58.4 %all-to-all-start = ((bf16[8,512,256]{2,1,0:T(8,128)(2,1)}), bf16[8,512,256]{2,1,0:T(8,128)(2,1)S(1)}, u32[]{:S(2)}, u32[]{:S(2)}) async-start(bf16[8,512,256]{2,1,0:T(8,128)(2,1)} %copies.1), calls=%async_computation | async-start | bytes 4194304 | tf_op jit(solution)/shard_map/all_to_all | solution.py:384
  85.2 56.3 %copy-start.1 = (bf16[1,128,128]{2,1,0:T(8,128)(2,1)S(1)}, bf16[1,128,128]{2,1,0:T(8,128)(2,1)}, u32[]{:S(2)}) copy-start(bf16[1,128,128]{2,1,0:T(8,128)(2,1)} %weight_ref.1) | copy-start | bytes 98308
  85.2 56.3 %copy-start.2 = (f32[128]{0:T(128)S(1)}, f32[128]{0:T(128)}, u32[]{:S(2)}) copy-start(f32[128]{0:T(128)} %param.15) | copy-start | bytes 1540
  85.2 56.3 %copy-start.3 = (f32[1,128]{1,0:T(1,128)S(1)}, f32[1,128]{1,0:T(1,128)}, u32[]{:S(2)}) copy-start(f32[1,128]{1,0:T(1,128)} %bias_ref.1) | copy-start | bytes 1540
  119.0 27.9 %collective-permute-start = (bf16[2048,128]{1,0:T(8,128)(2,1)}, bf16[2048,128]{1,0:T(8,128)(2,1)}, u32[]{:S(2)}, u32[]{:S(2)}) collective-permute-start(bf16[2048,128]{1,0:T(8,128)(2,1)} %all_gather.13), channel_id=1, source_target_pairs={{0,8},{8,16},{16,24},{24,0},{1,9},{9,17},{17,25},{25,1},{2,10},{10... | collective-permute-start | bytes 1572872 | tf_op jit(solution)/shard_map/ppermute | solution.py:359
  121.2 25.7 %collective-permute-start.1 = (bf16[2048,128]{1,0:T(8,128)(2,1)}, bf16[2048,128]{1,0:T(8,128)(2,1)}, u32[]{:S(2)}, u32[]{:S(2)}) collective-permute-start(bf16[2048,128]{1,0:T(8,128)(2,1)} %all_gather.13), channel_id=1, source_target_pairs={{0,16},{8,24},{16,0},{24,8},{1,17},{9,25},{17,1},{25,9},{2,18},{10... | collective-permute-start | bytes 1572872 | tf_op jit(solution)/shard_map/ppermute | solution.py:359
  124.9 24.1 %collective-permute-start.2 = (bf16[2048,128]{1,0:T(8,128)(2,1)}, bf16[2048,128]{1,0:T(8,128)(2,1)}, u32[]{:S(2)}, u32[]{:S(2)}) collective-permute-start(bf16[2048,128]{1,0:T(8,128)(2,1)} %all_gather.13), channel_id=1, source_target_pairs={{0,24},{8,0},{16,8},{24,16},{1,25},{9,1},{17,9},{25,17},{2,26},{10... | collective-permute-start | bytes 1572872 | tf_op jit(solution)/shard_map/ppermute | solution.py:359
  127.5 1.3 copy-start.5
  142.7 12.6 %all-to-all-start.3 = ((bf16[4,512,128]{2,1,0:T(8,128)(2,1)}), bf16[4,512,128]{2,1,0:T(8,128)(2,1)S(1)}, u32[]{:S(2)}, u32[]{:S(2)}) async-start(bf16[4,512,128]{2,1,0:T(8,128)(2,1)} %gated_copies.1), calls=%async_computation.3 | async-start | bytes 1048576 | tf_op jit(solution)/shard_map/all_to_all | solution.py:402
  162.4 7.1 %collective-permute-start.3 = (bf16[512,2048]{1,0:T(8,128)(2,1)}, bf16[512,2048]{1,0:T(8,128)(2,1)S(1)}, u32[]{:S(2)}, u32[]{:S(2)}) collective-permute-start(bf16[512,2048]{1,0:T(8,128)(2,1)} %projected.1.own_ref), channel_id=1, source_target_pairs={{0,1},{1,0},{2,3},{3,2},{4,5},{5,4},{6,7},{7,6},{8,9},{9,8},{10,11... | collective-permute-start | bytes 6291464 | tf_op jit(solution)/shard_map/ppermute | solution.py:25
  174.5 1.3 copy-start.4
  186.7 4.6 %collective-permute-start.4 = (bf16[256,2048]{1,0:T(8,128)(2,1)S(1)}, bf16[256,2048]{1,0:T(8,128)(2,1)S(1)}, u32[]{:S(2)}, u32[]{:S(2)}) collective-permute-start(bf16[256,2048]{1,0:T(8,128)(2,1)S(1)} %get-tuple-element.17), channel_id=1, source_target_pairs={{0,1},{1,0},{2,3},{3,2},{4,5},{5,4},{6,7},{7,6},{8,9},{9,8},{10,11... | collective-permute-start | bytes 3145736 | tf_op jit(solution)/shard_map/ppermute | solution.py:25
Sparse Core Ops, SparseCore 0:
  20.3 119.2 all-gather.1
